TPU v7x, 512 devices: a whole 4x8x8 slice. The times are simulated.
512 devices in a mesh: sp: 32 (over z, x), tp: 16 (over y, core).
Axes of the slice: x: 4, y: 8, z: 8, core: 2. Of those that a mesh axis runs over, the one named last changes fastest.
Arguments:
- pool_input: bfloat16 [1024, 12288], P('tp', 'sp'), may hold values from -6 to 6
- pool_gate: bfloat16 [1024, 12288], P('tp', 'sp'), may hold values from -6 to 6
- pool_mix: bfloat16 [4, 256, 256], replicated, may hold values from -0.375 to 0.375
- pool_scale: float32 [1024], replicated, may hold values from 0.1 to 1.9
- out_proj: bfloat16 [1024, 2048], P(None, 'tp'), may hold values from -0.375 to 0.375
- residual: bfloat16 [12288, 2048], P('sp', 'tp'), may hold values from -12 to 12
- norm_gain: float32 [2048], P('tp'), may hold values from 0.1 to 1.9
- routes: int32 [12288, 2], P('sp'), may hold values from 0 to 31, all different within a row; in each aligned block of 384 rows (0 to 383, 384 to 767, ...) at most 36 rows name the same one
- group_logits: float32 [12288, 4], P('sp'), may hold values from -4 to 4
- expert_scores: float32 [12288, 2], P('sp'), may hold values from -4 to 4
- w_gate: bfloat16 [32, 2048, 4096], P('sp', None, 'tp'), may hold values from -0.125 to 0.125
- w_up: bfloat16 [32, 2048, 4096], P('sp', None, 'tp'), may hold values from -0.125 to 0.125
- w_down: bfloat16 [32, 4096, 2048], P('sp', None, 'tp'), may hold values from -0.375 to 0.375
Outputs:
- layer_out: bfloat16 [12288, 2048], P('sp', 'tp')
Inputs may be any that keep to these rules, and one draw needn't show every extreme that they name: `routes`: among the rows of one device (aligned blocks of 384 rows) no expert is named by more than 36 rows, a bound that some block reaches; the 2 experts of a row differ.
All inputs are finite; a program needn't handle non-finite values.
Results may differ from a plain program's by a relative error of at most 0.01.
Values may be sent and summed in bfloat16 or wider, within the bound.
No kernel may reach another device: no remote copies, remote signals or barrier semaphores. Data moves between devices by JAX's collectives and lax.ppermute only.
A program may use at most 64 MiB of HBM per device.

v0:
```python
import jax
import jax.numpy as jnp
from jax import lax
from jax.sharding import PartitionSpec as P

D = 2048
POOL_GROUP = 256
TOP = 2


reach_back = 15
epsilon = 1e-06


def from_behind(value, axis, steps):
    count = lax.axis_size(axis)
    initial, last = (max(0, -steps), min(count, count - steps))
    return lax.ppermute(value, axis, [(source, source + steps) for source in range(initial, last)])


def in_one_piece(arrays, axis, dim, along):
    ends, at = ([], 0)
    for a in arrays[:-1]:
        at += a.shape[along]
        ends.append(at)
    both = jnp.concatenate(arrays, axis=along)
    return tuple(jnp.split(lax.all_gather(both, axis, axis=dim, tiled=True), ends, axis=along))


def from_everyone(value, axis):
    count = lax.axis_size(axis)
    return lax.all_to_all(
        jnp.broadcast_to(value[None], (count, *value.shape)), axis, 0, 0, tiled=True
    )


def over_copies(value, axis):
    return from_everyone(value, axis).sum(axis=0)


def window_terms(extended, first_channel, first_position, group_width):
    length = extended.shape[1] - reach_back
    layered = extended
    stride = 1
    partial_sums = []
    for _ in range(4):
        layered = layered[:, stride:] + layered[:, :-stride]
        stride = stride * 2
        partial_sums.append(layered[:, layered.shape[1] - length :])
    channel = first_channel + jnp.arange(extended.shape[0], dtype=jnp.int32)
    scale_index = channel // group_width
    chosen = partial_sums[3]
    for octave in range(3):
        chosen = jnp.where((scale_index == octave)[:, None], partial_sums[octave], chosen)
    window = (2 ** (scale_index + 1)).astype(jnp.float32)
    positions = (first_position + jnp.arange(length, dtype=jnp.int32) + 1).astype(jnp.float32)
    counted = jnp.minimum(positions[None, :], window[:, None])
    return chosen / counted - extended[:, reach_back:]


def slot_table(row_block, experts, capacity):
    flattened = row_block.reshape(-1)
    onehot = (flattened[:, None] == jnp.arange(experts, dtype=jnp.int32)[None, :]).astype(jnp.int32)
    before = jnp.cumsum(onehot, axis=0) - onehot
    ranked = jnp.sum(before * onehot, axis=1)
    return flattened * capacity + ranked


def route_weights(routes, group_logits, expert_scores, per_group):
    raised = jnp.exp(group_logits)
    group_prob = raised / jnp.sum(raised, axis=1, keepdims=True)
    owning_group = routes // per_group
    groups_iota = jnp.arange(group_logits.shape[1], dtype=jnp.int32)
    picked = jnp.sum(
        jnp.where(
            owning_group[:, :, None] == groups_iota[None, None, :], group_prob[:, None, :], 0.0
        ),
        axis=2,
    )
    lifted = jnp.exp(expert_scores)
    return picked * lifted / jnp.sum(lifted, axis=1, keepdims=True)


def per_device(
    pool_input,
    pool_gate,
    pool_mix,
    pool_scale,
    out_proj,
    residual,
    norm_gain,
    routes,
    group_logits,
    expert_scores,
    w_gate,
    w_up,
    w_down,
):
    channels, length = pool_input.shape
    edge_rows = from_behind(pool_input[:, length - reach_back :], "sp", 1)
    extended = jnp.concatenate([edge_rows, pool_input], axis=1).astype(jnp.float32)
    first_channel = lax.axis_index("tp") * channels
    first_position = lax.axis_index("sp") * length
    pooled = window_terms(extended, first_channel, first_position, POOL_GROUP).astype(jnp.bfloat16)
    gathered, gate_rows = in_one_piece((pooled, pool_gate), "tp", 0, 1)
    scales = pool_mix.shape[0]
    mixed_rows = jnp.einsum(
        "gct,gcd->tgd",
        gathered.reshape(scales, POOL_GROUP, length),
        pool_mix,
        preferred_element_type=jnp.float32,
    ).reshape(length, scales * POOL_GROUP)
    branch = (
        jax.nn.sigmoid(gate_rows.T.astype(jnp.float32)) * mixed_rows * pool_scale[None, :]
    ).astype(jnp.bfloat16)
    hidden_state = (
        residual.astype(jnp.float32) + jnp.dot(branch, out_proj, preferred_element_type=jnp.float32)
    ).astype(jnp.bfloat16)
    state_float = hidden_state.astype(jnp.float32)
    squares = over_copies(jnp.sum(state_float * state_float, axis=1), "tp")
    normed = (state_float * lax.rsqrt(squares / D + epsilon)[:, None] * norm_gain[None, :]).astype(
        jnp.bfloat16
    )
    experts = lax.axis_size("sp") * w_gate.shape[0]
    weights = route_weights(routes, group_logits, expert_scores, experts // group_logits.shape[1])
    capacity = 3 * TOP * length // (2 * experts)
    destination = slot_table(routes, experts, capacity)
    token_index = jnp.arange(length * TOP, dtype=jnp.int32) // TOP
    sources = jnp.full((experts * capacity,), length, jnp.int32).at[destination].set(token_index)
    padded = jnp.concatenate([normed, jnp.zeros((1, normed.shape[1]), jnp.bfloat16)], axis=0)
    arrived = lax.all_to_all(padded[sources], "sp", split_axis=0, concat_axis=0, tiled=True)
    portion = lax.all_gather(arrived, "tp", axis=1, tiled=True)
    rows_gate = w_gate[0]
    rows_up = w_up[0]
    gate_term = jnp.dot(portion, rows_gate, preferred_element_type=jnp.float32)
    up_term = jnp.dot(portion, rows_up, preferred_element_type=jnp.float32)
    activated = (jax.nn.silu(gate_term) * up_term).astype(jnp.bfloat16)
    rows_down = w_down[0]
    result = jnp.dot(
        lax.all_gather(activated, "tp", axis=1, tiled=True),
        rows_down,
        preferred_element_type=jnp.float32,
    ).astype(jnp.bfloat16)
    returned = lax.all_to_all(result, "sp", split_axis=0, concat_axis=0, tiled=True)
    picked = returned[destination].astype(jnp.float32).reshape(length, TOP, returned.shape[1])
    combined = jnp.sum(weights[:, :, None] * picked, axis=1)
    return (state_float + combined).astype(jnp.bfloat16)


def solution(mesh):
    placed = (
        P("tp", "sp"),
        P("tp", "sp"),
        P(),
        P(),
        P(None, "tp"),
        P("sp", "tp"),
        P("tp"),
        P("sp", None),
        P("sp", None),
        P("sp", None),
        P("sp", None, "tp"),
        P("sp", None, "tp"),
        P("sp", None, "tp"),
    )
    return jax.shard_map(
        per_device, mesh=mesh, in_specs=placed, out_specs=P("sp", "tp"), check_vma=False
    )
```

profile of v0, /device:TPU:1, one launch (start us, length us, event | category | flops | bytes accessed | tf_op | source)
XLA Modules:
  0.0 268.6 jit_solution(10977367310961019468)
XLA Ops:
  6.5 0.9 slice.43
  7.4 3.9 %collective-permute-start = (bf16[64,15]{1,0:T(8,128)(2,1)S(1)}, bf16[64,15]{1,0:T(8,128)(2,1)S(1)}, u32[]{:S(2)}, u32[]{:S(2)}) collective-permute-start(bf16[64,15]{1,0:T(8,128)(2,1)S(1)} %slice.43), channel_id=1, source_target_pairs={{0,16},{16,32},{32,48},{48,64},{64,80},{80,96},{96,112},{112,128},... | collective-permute-start | bytes 5768 | tf_op jit(solution)/shard_map/ppermute | solution.py:18
  11.4 0.8 collective-permute-done
  12.2 0.9 maximum_convert_fusion
  13.1 0.1 slice_add_fusion.2
  13.2 0.1 slice_add_fusion.1
  13.3 0.1 slice_add_fusion
  13.4 0.2 fusion.13
  13.6 0.7 pad_maximum_fusion
  14.3 0.1 copy.36
  14.5 0.1 eq.69
  14.6 0.1 eq.65
  14.8 1.7 reduce-window.6
  16.5 0.3 slice_reduce_fusion
  16.9 0.1 copy.35
  17.0 0.2 mul.134
  17.2 0.1 fusion.12
  17.3 3.4 %scatter_custom_fusion = s32[1152]{0:T(1024)S(1)} fusion(s32[768]{0:T(1024)S(1)} %fusion.24, s32[768]{0:T(1024)S(1)} %add_select_fusion, s32[]{:T(128)} %constant.90.clone.1), kind=kCustom, calls=%fused_computation.60 | custom fusion | bytes 4612 | tf_op jit(solution)/shard_map/scatter | solution.py:129
  20.7 42.6 %all-gather.4.cloned.1.call-done = bf16[1024,768]{1,0:T(8,128)(2,1)} async-done(((bf16[64,768]{1,0:T(8,128)(2,1)}), bf16[1024,768]{1,0:T(8,128)(2,1)}) %all-gather.4.cloned.1.call-update) | async-done | bytes 1572880 | tf_op jit(solution)/shard_map/all_gather | solution.py:27
  63.3 1.6 slice-done
  64.9 0.5 fusion.26
  65.5 0.4 fusion.2
  65.9 0.5 copy-done.3
  66.4 0.0 copy-done.4
  66.4 0.5 multiply_reduce_fusion
  66.9 0.6 broadcast_in_dim.69
  67.5 4.9 %all-to-all-start = ((f32[16,1,384]{2,1,0:T(1,128)}), f32[16,1,384]{2,1,0:T(1,128)S(1)}, u32[]{:S(2)}, u32[]{:S(2)}) async-start(f32[16,1,384]{2,1,0:T(1,128)} %broadcast_in_dim.69), calls=%async_computation | async-start | bytes 49152 | tf_op jit(solution)/shard_map/all_to_all | solution.py:32
  72.4 0.0 all-gather.6.cloned.1.call-start
  72.5 7.3 %all-to-all-done = f32[16,1,384]{2,1,0:T(1,128)S(1)} async-done(((f32[16,1,384]{2,1,0:T(1,128)}), f32[16,1,384]{2,1,0:T(1,128)S(1)}, u32[]{:S(2)}, u32[]{:S(2)}) %all-to-all-start) | async-done | bytes 24608 | tf_op jit(solution)/shard_map/all_to_all | solution.py:32
  79.8 0.1 multiply_convert_fusion
  80.0 2.9 %gather_fusion = bf16[1152,128]{1,0:T(8,128)(2,1)S(1)} fusion(bf16[385,128]{1,0:T(8,128)(2,1)S(1)} %concatenate.11, s32[2048]{0:T(1024)S(1)} %pad_clamp_fusion), kind=kCustom, calls=%fused_computation | custom fusion | bytes 594432 | tf_op jit(solution)/shard_map/gather | solution.py:131
  82.9 0.1 all_to_all.21
  83.0 22.5 %all_to_all.30 = bf16[32,36,128]{2,1,0:T(8,128)(2,1)S(1)} all-to-all(bf16[32,36,128]{2,1,0:T(8,128)(2,1)S(1)} %all_to_all.21), channel_id=1, replica_groups=mesh['sp'=32,'tp'=16] {'sp'}, dimensions={0} | all-to-all | bytes 589824 | tf_op jit(solution)/shard_map/all_to_all | solution.py:131
  105.4 0.8 all_to_all.23
  106.2 0.0 all-gather.8.cloned.1.call-start
  106.3 47.4 %all-gather.6.cloned.1.call-done = bf16[1152,2048]{1,0:T(8,128)(2,1)} async-done(((bf16[1152,128]{1,0:T(8,128)(2,1)}), bf16[1152,2048]{1,0:T(8,128)(2,1)}) %all-gather.6.cloned.1.call-update) | async-done | bytes 4718608 | tf_op jit(solution)/shard_map/all_gather | solution.py:132
  153.7 3.9 %fusion.7 = f32[1152,256]{1,0:T(8,128)S(1)} fusion(bf16[1152,2048]{1,0:T(8,128)(2,1)} %all-gather.6.cloned.1.call-done, bf16[1,2048,256]{2,1,0:T(8,128)(2,1)S(1)} %copy-done), kind=kOutput, calls=%fused_computation.14 | convolution fusion | flops 1207959552 | bytes 6946816 | tf_op jit(solution)/shard_map/dot_general | solution.py:135
  157.7 2.3 fusion
  160.1 70.0 %all-gather.8.cloned.1.call-done = bf16[1152,4096]{1,0:T(8,128)(2,1)} async-done(((bf16[1152,256]{1,0:T(8,128)(2,1)}), bf16[1152,4096]{1,0:T(8,128)(2,1)}) %all-gather.8.cloned.1.call-update) | async-done | bytes 9437200 | tf_op jit(solution)/shard_map/all_gather | solution.py:140
  230.0 6.5 %convolution_convert_fusion = bf16[1152,128]{1,0:T(8,128)(2,1)S(1)} fusion(bf16[1152,4096]{1,0:T(8,128)(2,1)} %all-gather.8.cloned.1.call-done, bf16[1,4096,128]{2,1,0:T(8,128)(2,1)} %param.25), kind=kOutput, calls=%fused_computation.5 | convolution fusion | flops 1208107008 | bytes 10780672 | tf_op jit(solution)/shard_map/dot_general | solution.py:139
  236.6 0.8 all_to_all.24
  237.3 8.7 %all-to-all-start.2 = ((bf16[32,36,128]{2,1,0:T(8,128)(2,1)}), bf16[32,36,128]{2,1,0:T(8,128)(2,1)S(1)}, u32[]{:S(2)}, u32[]{:S(2)}) async-start(bf16[32,36,128]{2,1,0:T(8,128)(2,1)} %all_to_all.24), calls=%async_computation.2 | async-start | bytes 655360 | tf_op jit(solution)/shard_map/all_to_all | solution.py:144
  246.1 0.1 copy.33
  246.3 12.6 %all-to-all-done.2 = bf16[32,36,128]{2,1,0:T(8,128)(2,1)S(1)} async-done(((bf16[32,36,128]{2,1,0:T(8,128)(2,1)}), bf16[32,36,128]{2,1,0:T(8,128)(2,1)S(1)}, u32[]{:S(2)}, u32[]{:S(2)}) %all-to-all-start.2) | async-done | bytes 294944 | tf_op jit(solution)/shard_map/all_to_all | solution.py:144
  258.9 0.1 all_to_all.26
  259.0 1.9 gather_fusion.1
  260.8 0.6 fusion.9
  261.4 0.7 add_convert_fusion
  (49 shorter events, 0.4 us)
Async XLA Ops:
  6.5 147.2 %copy-start = (bf16[1,2048,256]{2,1,0:T(8,128)(2,1)S(1)}, bf16[1,2048,256]{2,1,0:T(8,128)(2,1)}, u32[]{:S(2)}) copy-start(bf16[1,2048,256]{2,1,0:T(8,128)(2,1)} %param.23) | copy-start | bytes 3145732
  6.5 7.1 %copy-start.5 = (bf16[64,384]{1,0:T(8,128)(2,1)S(1)}, bf16[64,384]{1,0:T(8,128)(2,1)}, u32[]{:S(2)}) copy-start(bf16[64,384]{1,0:T(8,128)(2,1)} %param.14) | copy-start | bytes 147460
  6.5 7.8 %copy-start.8 = (s32[384,2]{0,1:T(2,128)S(1)}, s32[384,2]{0,1:T(2,128)}, u32[]{:S(2)}) copy-start(s32[384,2]{0,1:T(2,128)} %param.20) | copy-start | bytes 9220
  6.5 56.8 %all-gather.4.cloned.1.call-start = ((), (), s32[]{:S(2)}) async-start(), calls=%async_computation.3 | async-start | bytes 1671168 | tf_op jit(solution)/shard_map/all_gather | solution.py:27
  7.4 4.8 %collective-permute-start = (bf16[64,15]{1,0:T(8,128)(2,1)S(1)}, bf16[64,15]{1,0:T(8,128)(2,1)S(1)}, u32[]{:S(2)}, u32[]{:S(2)}) collective-permute-start(bf16[64,15]{1,0:T(8,128)(2,1)S(1)} %slice.43), channel_id=1, source_target_pairs={{0,16},{16,32},{32,48},{48,64},{64,80},{80,96},{96,112},{112,128},... | collective-permute-start | bytes 5768 | tf_op jit(solution)/shard_map/ppermute | solution.py:18
  14.3 49.0 %copy-start.2 = (bf16[4,256,256]{2,1,0:T(8,128)(2,1)S(1)}, bf16[4,256,256]{2,1,0:T(8,128)(2,1)}, u32[]{:S(2)}) copy-start(bf16[4,256,256]{2,1,0:T(8,128)(2,1)} %param.15) | copy-start | bytes 1572868
  63.3 1.6 slice-start
  63.3 2.1 copy-start.1
  63.3 2.1 copy-start.9
  65.4 1.0 copy-start.3
  65.5 1.0 copy-start.4
  65.5 14.4 %copy-start.10 = (f32[128]{0:T(128)S(1)}, f32[128]{0:T(128)}, u32[]{:S(2)}) copy-start(f32[128]{0:T(128)} %param.19) | copy-start | bytes 1540
  67.5 12.2 %all-to-all-start = ((f32[16,1,384]{2,1,0:T(1,128)}), f32[16,1,384]{2,1,0:T(1,128)S(1)}, u32[]{:S(2)}, u32[]{:S(2)}) async-start(f32[16,1,384]{2,1,0:T(1,128)} %broadcast_in_dim.69), calls=%async_computation | async-start | bytes 49152 | tf_op jit(solution)/shard_map/all_to_all | solution.py:32
  72.4 81.3 %all-gather.6.cloned.1.call-start = ((), (), s32[]{:S(2)}) async-start(), calls=%async_computation.4 | async-start | bytes 5013504 | tf_op jit(solution)/shard_map/all_gather | solution.py:132
  106.2 51.4 %copy-start.12 = (bf16[1,2048,256]{2,1,0:T(8,128)(2,1)S(1)}, bf16[1,2048,256]{2,1,0:T(8,128)(2,1)}, u32[]{:S(2)}) copy-start(bf16[1,2048,256]{2,1,0:T(8,128)(2,1)} %param.24) | copy-start | bytes 3145732
  106.2 123.8 %all-gather.8.cloned.1.call-start = ((), (), s32[]{:S(2)}) async-start(), calls=%async_computation.5 | async-start | bytes 10027008 | tf_op jit(solution)/shard_map/all_gather | solution.py:140
  153.7 3.9 %copy-start.11 = (bf16[1152,2048]{1,0:T(8,128)(2,1)S(1)}, bf16[1152,2048]{1,0:T(8,128)(2,1)}, u32[]{:S(2)}) copy-start(bf16[1152,2048]{1,0:T(8,128)(2,1)} %all-gather.6.cloned.1.call-done) | copy-start | bytes 14155780
  157.6 2.4 copy-start.6
  160.1 86.0 %copy-start.7 = (f32[384,2]{0,1:T(2,128)S(1)}, f32[384,2]{0,1:T(2,128)}, u32[]{:S(2)}) copy-start(f32[384,2]{0,1:T(2,128)} %param.22) | copy-start | bytes 9220
  237.3 21.6 %all-to-all-start.2 = ((bf16[32,36,128]{2,1,0:T(8,128)(2,1)}), bf16[32,36,128]{2,1,0:T(8,128)(2,1)S(1)}, u32[]{:S(2)}, u32[]{:S(2)}) async-start(bf16[32,36,128]{2,1,0:T(8,128)(2,1)} %all_to_all.24), calls=%async_computation.2 | async-start | bytes 655360 | tf_op jit(solution)/shard_map/all_to_all | solution.py:144
Sparse Core Ops, SparseCore 0:
  14.4 48.8 all-gather.3
  106.3 47.3 all-gather.5
  160.1 69.8 all-gather.7
where the time goes:
time: 269 us
  waiting for transfers between devices  181 us (67%)
  blocking collectives  22.5 us (8%)
  starting transfers between devices  17.6 us (7%)
  local copies, waits for them, and re-layouts  14.7 us (5%)
  matrix products  13.7 us (5%)
  between operations  13.5 us (5%)
  other arithmetic  5.95 us (2%)
    all_gather x1, waiting for transfers between devices, per_device(): lax.all_gather(activated, 'tp', axis=1, tiled=True)  70 us
    all_gather x1, waiting for transfers between devices, per_device(): portion = lax.all_gather(arrived, 'tp', axis=1, tiled=True)  47.4 us
    all_gather x1, waiting for transfers between devices, in_one_piece(): lax.all_gather(both, axis, axis=dim, tiled=True)  42.6 us
    all_to_all x1, blocking collectives, per_device(): lax.all_to_all(padded[sources], 'sp', split_axis=0, concat_axis=0, tiled=...  22.5 us
    all_to_all x1, waiting for transfers between devices, per_device(): lax.all_to_all(result, 'sp', split_axis=0, concat_axis=0, tiled=True)  12.6 us
    all_to_all x1, starting transfers between devices, per_device(): lax.all_to_all(result, 'sp', split_axis=0, concat_axis=0, tiled=True)  8.7 us
    all_to_all x1, waiting for transfers between devices, from_everyone(): lax.all_to_all(jnp.broadcast_to(value[None], (count, *value.shape)), axis...  7.3 us
    dot_general x1, matrix products, per_device(): jnp.dot(lax.all_gather(activated, 'tp', axis=1, tiled=True), rows_down, p...  6.52 us
  transfers between devices with their start and end apart: 6, of which 6 were waited for; matrix products, arithmetic and copies ran while one was open for 2% of the time, Pallas kernels for 0%

commit v1 on v0

v1 whole, which is shorter than its diff:
```python
import jax
import jax.numpy as jnp
from jax import lax
from jax.experimental import pallas as pl
from jax.experimental.pallas import tpu as pltpu
from jax.sharding import Mesh, PartitionSpec as P

SPAN = 128
ROW_TILE = 144
GAIN_ROWS = 16
epsilon = 1e-06

TP = ("tg", "tl")


def pool_kernel(where_ref, edge_ref, own_ref, out_ref):
    scale, first = where_ref[0], where_ref[1]
    length = own_ref.shape[1]
    own = own_ref[...].astype(jnp.float32)
    layered = jnp.concatenate([edge_ref[...].astype(jnp.float32), own], axis=1)
    chosen = None
    stride = 1
    for octave in range(4):
        layered = layered + pltpu.roll(layered, stride, 1)
        stride *= 2
        chosen = layered if chosen is None else jnp.where(scale >= octave, layered, chosen)
    window = jnp.left_shift(2, scale)
    position = first + 1 + lax.broadcasted_iota(jnp.int32, own.shape, 1)
    counted = jnp.minimum(position, window).astype(jnp.float32)
    pooled = chosen[:, SPAN : SPAN + length] / counted - own
    out_ref[...] = pooled.astype(out_ref.dtype)


def pool(edge, own, scale, first):
    return pl.pallas_call(
        pool_kernel,
        out_shape=jax.ShapeDtypeStruct(own.shape, jnp.bfloat16),
        in_specs=[
            pl.BlockSpec(memory_space=pltpu.SMEM),
            pl.BlockSpec(memory_space=pltpu.VMEM),
            pl.BlockSpec(memory_space=pltpu.VMEM),
        ],
        name="pool",
    )(jnp.stack([scale, first]), edge, own)


def hidden_kernel(x_ref, extra_ref, gate_ref, up_ref, out_ref):
    parts, rows, width = x_ref.shape
    squares = jnp.zeros((rows, width), jnp.float32)
    scaled = []
    for part in range(parts):
        state = x_ref[part].astype(jnp.float32)
        squares += state * state
        extra = extra_ref[part].astype(jnp.float32)
        gain = extra[0:1] + extra[1:2] + extra[2:3]
        scaled.append((state * gain).astype(jnp.bfloat16))
    rows_in = jnp.concatenate(scaled, axis=1)
    mean = jnp.sum(squares, axis=1, keepdims=True) / (parts * width)
    factor = lax.rsqrt(mean + epsilon)
    gate = jnp.dot(rows_in, gate_ref[0], preferred_element_type=jnp.float32) * factor
    up = jnp.dot(rows_in, up_ref[0], preferred_element_type=jnp.float32) * factor
    out_ref[...] = (jax.nn.silu(gate) * up).astype(out_ref.dtype)


def hidden(everyone, w_gate, w_up, rows):
    parts, _, width = everyone.shape
    units = w_gate.shape[2]
    weight = pl.BlockSpec((1, parts * width, units), lambda i: (0, 0, 0))
    return pl.pallas_call(
        hidden_kernel,
        out_shape=jax.ShapeDtypeStruct((rows, units), jnp.bfloat16),
        grid=(rows // ROW_TILE,),
        in_specs=[
            pl.BlockSpec((parts, ROW_TILE, width), lambda i: (0, i, 0)),
            pl.BlockSpec((parts, GAIN_ROWS, width), lambda i: (0, rows // GAIN_ROWS, 0)),
            weight,
            weight,
        ],
        out_specs=pl.BlockSpec((ROW_TILE, units), lambda i: (i, 0)),
        name="hidden",
    )(everyone, everyone, w_gate, w_up)


def down_kernel(x_ref, down_ref, out_ref):
    rows_in = jnp.concatenate([x_ref[part] for part in range(x_ref.shape[0])], axis=1)
    result = jnp.dot(rows_in, down_ref[0], preferred_element_type=jnp.float32)
    out_ref[...] = result.astype(out_ref.dtype)


def down(everyone, w_down):
    parts, rows, units = everyone.shape
    width = w_down.shape[2]
    return pl.pallas_call(
        down_kernel,
        out_shape=jax.ShapeDtypeStruct((rows, width), jnp.bfloat16),
        grid=(rows // ROW_TILE,),
        in_specs=[
            pl.BlockSpec((parts, ROW_TILE, units), lambda i: (0, i, 0)),
            pl.BlockSpec((1, parts * units, width), lambda i: (0, 0, 0)),
        ],
        out_specs=pl.BlockSpec((ROW_TILE, width), lambda i: (i, 0)),
        name="down",
    )(everyone, w_down)


def combine_kernel(state_ref, slot_ref, weight_ref, returned_ref, out_ref):
    length, slots = state_ref.shape[0], returned_ref.shape[0]
    place = lax.broadcasted_iota(jnp.int32, (length, slots), 1)
    total = jnp.zeros(out_ref.shape, jnp.float32)
    for choice in range(slot_ref.shape[1]):
        pick = jnp.where(place == slot_ref[:, choice : choice + 1], 1.0, 0.0).astype(jnp.bfloat16)
        picked = jnp.dot(pick, returned_ref[...], preferred_element_type=jnp.float32)
        total += weight_ref[:, choice : choice + 1] * picked
    out_ref[...] = (state_ref[...].astype(jnp.float32) + total).astype(out_ref.dtype)


def combine(state, slots, weights, returned):
    return pl.pallas_call(
        combine_kernel,
        out_shape=jax.ShapeDtypeStruct(state.shape, jnp.bfloat16),
        name="combine",
    )(state, slots, weights, returned)


def slot_table(routes, experts, capacity):
    flattened = routes.reshape(-1)
    count = flattened.shape[0]
    onehot = (flattened[:, None] == jnp.arange(experts, dtype=jnp.int32)[None, :]).astype(jnp.bfloat16)
    row = lax.broadcasted_iota(jnp.int32, (count, count), 0)
    column = lax.broadcasted_iota(jnp.int32, (count, count), 1)
    earlier = (column < row).astype(jnp.bfloat16)
    before = jnp.dot(earlier, onehot, preferred_element_type=jnp.float32)
    ranked = jnp.sum(before * onehot.astype(jnp.float32), axis=1).astype(jnp.int32)
    return (flattened * capacity + ranked).reshape(routes.shape)


def route_weights(routes, group_logits, expert_scores, per_group):
    raised = jnp.exp(group_logits)
    group_prob = raised / jnp.sum(raised, axis=1, keepdims=True)
    owning_group = routes // per_group
    groups_iota = jnp.arange(group_logits.shape[1], dtype=jnp.int32)
    picked = jnp.sum(
        jnp.where(owning_group[:, :, None] == groups_iota[None, None, :], group_prob[:, None, :], 0.0),
        axis=2,
    )
    lifted = jnp.exp(expert_scores)
    return picked * lifted / jnp.sum(lifted, axis=1, keepdims=True)


def gain_rows(gain):
    rows, rest = [], gain
    for _ in range(3):
        head = lax.reduce_precision(rest, 8, 7)
        rows.append(head)
        rest = rest - head
    rows += [jnp.zeros_like(gain)] * (GAIN_ROWS - len(rows))
    return jnp.stack(rows).astype(jnp.bfloat16)


def per_device(
    pool_input,
    pool_gate,
    pool_mix,
    pool_scale,
    out_proj,
    residual,
    norm_gain,
    routes,
    group_logits,
    expert_scores,
    w_gate,
    w_up,
    w_down,
):
    channels, length = pool_input.shape
    blocks = lax.axis_size("sp")
    scale, quarter = lax.axis_index("tg"), lax.axis_index("tl")
    own_first = (scale * lax.axis_size("tl") + quarter) * channels
    edge = lax.ppermute(
        pool_input[:, length - SPAN :], "sp", [(i, i + 1) for i in range(blocks - 1)]
    )
    pooled = pool(edge, pool_input, scale, lax.axis_index("sp") * length)
    group = lax.all_gather(pooled, "tl", axis=0, tiled=True)
    mix = lax.dynamic_slice(
        pool_mix, (scale, 0, quarter * channels), (1, pool_mix.shape[1], channels)
    )[0]
    mixed = lax.dot_general(mix, group, (((0,), (0,)), ((), ())), preferred_element_type=jnp.float32)
    own_scale = lax.dynamic_slice(pool_scale, (own_first,), (channels,))
    branch = (jax.nn.sigmoid(pool_gate.astype(jnp.float32)) * mixed * own_scale[:, None]).astype(jnp.bfloat16)
    branches = lax.all_gather(branch, TP, axis=0, tiled=True)
    product = lax.dot_general(
        branches, out_proj, (((0,), (0,)), ((), ())), preferred_element_type=jnp.float32
    )
    state = (residual.astype(jnp.float32) + product).astype(jnp.bfloat16)

    experts = blocks * w_gate.shape[0]
    capacity = 3 * routes.shape[1] * length // (2 * experts)
    slots = slot_table(routes, experts, capacity)
    rows = experts * capacity
    place = jnp.arange(rows, dtype=jnp.int32)[:, None]
    spread = sum((place == slots[:, k][None, :]).astype(jnp.bfloat16) for k in range(slots.shape[1]))
    sent = jnp.dot(spread, state, preferred_element_type=jnp.float32).astype(jnp.bfloat16)
    arrived = lax.all_to_all(
        sent.reshape(blocks, capacity, -1), "sp", split_axis=0, concat_axis=0, tiled=True
    ).reshape(rows, -1)
    carried = jnp.concatenate([arrived, gain_rows(norm_gain)], axis=0)
    everyone = lax.all_gather(carried, TP, axis=0, tiled=False)
    activated = hidden(everyone, w_gate, w_up, rows)
    weights = route_weights(routes, group_logits, expert_scores, experts // group_logits.shape[1])
    units = lax.all_gather(activated, TP, axis=0, tiled=False)
    result = down(units, w_down)
    returned = lax.all_to_all(
        result.reshape(blocks, capacity, -1), "sp", split_axis=0, concat_axis=0, tiled=True
    ).reshape(rows, -1)
    return combine(state, slots, weights, returned)


def solution(mesh):
    fine = Mesh(mesh.devices.reshape(mesh.devices.shape[0], 4, -1), ("sp", *TP))
    placed = (
        P(TP, "sp"),
        P(TP, "sp"),
        P(),
        P(),
        P(None, TP),
        P("sp", TP),
        P(TP),
        P("sp", None),
        P("sp", None),
        P("sp", None),
        P("sp", None, TP),
        P("sp", None, TP),
        P("sp", None, TP),
    )
    return jax.shard_map(
        per_device, mesh=fine, in_specs=placed, out_specs=P("sp", TP), check_vma=False
    )
```

time: 269 us -> 229 us (0.85)
  waiting for transfers between devices: 181 us -> 126 us
  Pallas kernels: 0 us -> 21.5 us
  matrix products: 13.7 us -> 1.56 us
  starting transfers between devices: 17.6 us -> 26.4 us
  local copies, waits for them, and re-layouts: 14.7 us -> 9.69 us
  blocking collectives: 22.5 us -> 26.4 us
  other arithmetic: 5.95 us -> 2.27 us
    all_gather x3 -> x2, waiting for transfers between devices: 160 us -> 102 us  [the longest x1 61.9 us: per_device(): units = lax.all_gather(activated, TP, axis=0, tiled=False)]
    all_gather x0 -> x2, blocking collectives: none -> 26.4 us  [the longest x1 16.6 us: per_device(): branches = lax.all_gather(branch, TP, axis=0, tiled=True)]
    all_to_all x1 -> x0, blocking collectives: 22.5 us -> none  [per_device(): lax.all_to_all(padded[sources], 'sp', split_axis=0, concat_axis=0, tiled=...]
    pallas_call x0 -> x4, Pallas kernels: none -> 21.5 us  [the longest x1 8.78 us: down(): pl.pallas_call(down_kernel, out_shape=jax.ShapeDtypeStruct((rows, width),...]
    dot_general x5 -> x4, matrix products: 13.7 us -> 1.56 us  [the longest x1 0.52 us: per_device(): jnp.dot(spread, state, preferred_element_type=jnp.float32)]
    all_to_all x2, starting transfers between devices: 13.6 us -> 22.4 us  [the longest x1 12.5 us: per_device(): lax.all_to_all(sent.reshape(blocks, capacity, -1), 'sp', split_axis=0, co...]
    gather x2 -> x0, local copies, waits for them, and re-layouts: 4.81 us -> none  [the longest x1 2.93 us: per_device(): padded[sources]]
    all_to_all x2, waiting for transfers between devices: 19.9 us -> 24.7 us  [the longest x1 12.9 us: per_device(): lax.all_to_all(sent.reshape(blocks, capacity, -1), 'sp', split_axis=0, co...]
  transfers between devices with their start and end apart: 6 -> 5, of which waited for: 6 -> 4; matrix products, arithmetic and copies ran while one was open for 2% -> 2% of each run, Pallas kernels for 0% -> 0%
where the time goes in v1:
time: 229 us; the launch traced here: 228 us
  waiting for transfers between devices  126 us (55%)
  starting transfers between devices  26.4 us (12%)
  blocking collectives  26.4 us (12%)
  Pallas kernels  21.5 us (9%)
  between operations  13.7 us (6%)
  local copies, waits for them, and re-layouts  9.69 us (4%)
    all_gather x1, waiting for transfers between devices, per_device(): units = lax.all_gather(activated, TP, axis=0, tiled=False)  61.9 us
    all_gather x1, waiting for transfers between devices, per_device(): everyone = lax.all_gather(carried, TP, axis=0, tiled=False)  39.7 us
    all_gather x1, blocking collectives, per_device(): branches = lax.all_gather(branch, TP, axis=0, tiled=True)  16.6 us
    all_to_all x1, waiting for transfers between devices, per_device(): lax.all_to_all(sent.reshape(blocks, capacity, -1), 'sp', split_axis=0, co...  12.9 us
    all_to_all x1, starting transfers between devices, per_device(): lax.all_to_all(sent.reshape(blocks, capacity, -1), 'sp', split_axis=0, co...  12.5 us
    all_to_all x1, waiting for transfers between devices, per_device(): lax.all_to_all(result.reshape(blocks, capacity, -1), 'sp', split_axis=0,...  11.8 us
    all_to_all x1, starting transfers between devices, per_device(): lax.all_to_all(result.reshape(blocks, capacity, -1), 'sp', split_axis=0,...  9.9 us
    all_gather x1, blocking collectives, per_device(): group = lax.all_gather(pooled, 'tl', axis=0, tiled=True)  9.82 us
  transfers between devices with their start and end apart: 5, of which 4 were waited for; matrix products, arithmetic and copies ran while one was open for 2% of the time, Pallas kernels for 0%

profile of v1, /device:TPU:1, one launch (start us, length us, event | category | flops | bytes accessed | tf_op | source)
XLA Modules:
  0.0 227.8 jit_solution(1842558096719151467)
XLA Ops:
  6.5 0.0 copy-start
  6.5 0.8 slice.9
  7.3 3.9 %collective-permute-start = (bf16[64,128]{1,0:T(8,128)(2,1)S(1)}, bf16[64,128]{1,0:T(8,128)(2,1)S(1)}, u32[]{:S(2)}, u32[]{:S(2)}) collective-permute-start(bf16[64,128]{1,0:T(8,128)(2,1)S(1)} %slice.9), channel_id=1, source_target_pairs={{0,16},{16,32},{32,48},{48,64},{64,80},{80,96},{96,112},{112,128},... | collective-permute-start | bytes 49160 | tf_op jit(solution)/shard_map/ppermute | solution.py:179
  11.2 0.7 and_select_fusion
  12.0 0.8 copy.35
  12.8 0.1 copy.36
  12.9 0.1 eq.58
  13.1 0.0 copy-start.3
  13.1 0.0 copy-start.4
  13.1 0.4 fusion.7
  13.5 0.2 convert_element_type.43
  13.7 0.0 copy-start.1
  13.7 0.3 slice_reduce_fusion.1
  13.9 0.7 pad_add_fusion.where_ref
  14.6 0.8 dynamic_slice.7
  15.4 0.0 collective-permute-done.edge_ref
  15.4 0.6 copy-done.6
  16.0 1.8 pool.1
  17.8 9.8 %all_gather.18 = bf16[256,384]{1,0:T(8,128)(2,1)S(1)} all-gather(bf16[64,384]{1,0:T(8,128)(2,1)} %pool.1), channel_id=1, replica_groups=mesh['sp'=32,'tg'=4,'tl'=4] {'tl'}, dimensions={0}, use_global_device_ids=true | all-gather | bytes 245760 | tf_op jit(solution)/shard_map/all_gather | solution.py:183
  27.6 0.0 copy-done
  27.6 0.0 copy-done.9
  27.6 0.3 fusion.6
  27.9 16.6 %all_gather.19 = bf16[1024,384]{1,0:T(8,128)(2,1)S(1)} all-gather(bf16[64,384]{1,0:T(8,128)(2,1)S(1)} %fusion.6), channel_id=1, replica_groups=mesh['sp'=32,'tg'=4,'tl'=4] {'tg','tl'}, dimensions={0}, use_global_device_ids=true | all-gather | bytes 835584 | tf_op jit(solution)/shard_map/all_gather | solution.py:190
  44.5 0.4 fusion.3.state_ref
  44.9 0.0 copy-start.8
  45.0 0.5 convolution_convert_fusion
  45.5 0.8 reshape.24
  46.3 12.5 %all-to-all-start = ((bf16[32,36,128]{2,1,0:T(8,128)(2,1)}), bf16[32,36,128]{2,1,0:T(8,128)(2,1)S(1)}, u32[]{:S(2)}, u32[]{:S(2)}) async-start(bf16[32,36,128]{2,1,0:T(8,128)(2,1)} %reshape.24), calls=%async_computation | async-start | bytes 655360 | tf_op jit(solution)/shard_map/all_to_all | solution.py:203
  58.8 0.0 all-gather.5.cloned.1.call-start
  58.8 0.0 copy-done.8
  58.8 12.9 %all-to-all-done = bf16[32,36,128]{2,1,0:T(8,128)(2,1)S(1)} async-done(((bf16[32,36,128]{2,1,0:T(8,128)(2,1)}), bf16[32,36,128]{2,1,0:T(8,128)(2,1)S(1)}, u32[]{:S(2)}, u32[]{:S(2)}) %all-to-all-start) | async-done | bytes 294944 | tf_op jit(solution)/shard_map/all_to_all | solution.py:203
  71.7 0.1 reshape.25
  71.8 2.5 %concatenate.4 = bf16[1168,128]{1,0:T(8,128)(2,1)} concatenate(bf16[1152,128]{1,0:T(8,128)(2,1)S(1)} %reshape.25, bf16[1,128]{1,0:T(2,128)(2,1)S(1)} %get-tuple-element.13, bf16[1,128]{1,0:T(2,128)(2,1)S(1)} %get-tuple-element.12, bf16[1,128]{1,0:T(2,128)(2,1)S(1)} %get-tuple-element.11, bf16[1,128]{1,0:T(2,128)(2,1)S(1)} %stack_broadcast_in_dim.3, bf16[4,128]{1,0:T(4,128)(2,1)S(1)} %stack.35, ...), dimensions={0} | concatenate | bytes 598016 | tf_op jit(solution)/shard_map/concatenate | solution.py:206
  74.3 0.0 all-gather.5.cloned.1.call-update
  74.3 0.0 all-gather.7.cloned.1.call-start
  74.4 39.7 %all-gather.5.cloned.1.call-done = bf16[18688,128]{1,0:T(8,128)(2,1)} async-done(((bf16[1168,128]{1,0:T(8,128)(2,1)}), bf16[18688,128]{1,0:T(8,128)(2,1)}) %all-gather.5.cloned.1.call-update) | async-done | bytes 4784144 | tf_op jit(solution)/shard_map/all_gather | solution.py:207
  114.1 8.4 %hidden.1 = bf16[1152,256]{1,0:T(8,128)(2,1)} custom-call(bf16[16,1168,128]{2,1,0:T(8,128)(2,1)} %bitcast.17, bf16[16,1168,128]{2,1,0:T(8,128)(2,1)} %bitcast.18, bf16[1,2048,256]{2,1,0:T(8,128)(2,1)} %gate_ref.1, bf16[1,2048,256]{2,1,0:T(8,128)(2,1)} %up_ref.1), custom_call_target="tpu_custom_call" | custom-call | tf_op jit(solution)/shard_map/hidden/pallas_call | solution.py:69
  122.5 0.0 all-gather.7.cloned.1.call-update
  122.5 0.0 copy-done.5
  122.5 61.9 %all-gather.7.cloned.1.call-done = bf16[18432,256]{1,0:T(8,128)(2,1)} async-done(((bf16[1152,256]{1,0:T(8,128)(2,1)}), bf16[18432,256]{1,0:T(8,128)(2,1)}) %all-gather.7.cloned.1.call-update) | async-done | bytes 9437200 | tf_op jit(solution)/shard_map/all_gather | solution.py:210
  184.4 8.8 %down.1 = bf16[1152,128]{1,0:T(8,128)(2,1)} custom-call(bf16[16,1152,256]{2,1,0:T(8,128)(2,1)} %bitcast.19, bf16[1,4096,128]{2,1,0:T(8,128)(2,1)} %down_ref.1), custom_call_target="tpu_custom_call" | custom-call | tf_op jit(solution)/shard_map/down/pallas_call | solution.py:93
  193.2 1.7 reshape.26
  194.9 9.9 %all-to-all-start.1 = ((bf16[32,36,128]{2,1,0:T(8,128)(2,1)}), bf16[32,36,128]{2,1,0:T(8,128)(2,1)S(1)}, u32[]{:S(2)}, u32[]{:S(2)}) async-start(bf16[32,36,128]{2,1,0:T(8,128)(2,1)} %reshape.26), calls=%async_computation.1 | async-start | bytes 655360 | tf_op jit(solution)/shard_map/all_to_all | solution.py:212
  204.9 0.1 copy.37
  205.0 0.8 broadcast_divide_fusion.weight_ref
  205.9 11.8 %all-to-all-done.1 = bf16[32,36,128]{2,1,0:T(8,128)(2,1)S(1)} async-done(((bf16[32,36,128]{2,1,0:T(8,128)(2,1)}), bf16[32,36,128]{2,1,0:T(8,128)(2,1)S(1)}, u32[]{:S(2)}, u32[]{:S(2)}) %all-to-all-start.1) | async-done | bytes 294944 | tf_op jit(solution)/shard_map/all_to_all | solution.py:212
  217.7 0.8 reshape.27.returned_ref
  218.5 2.5 %combine.1 = bf16[384,128]{1,0:T(8,128)(2,1)} custom-call(bf16[384,128]{1,0:T(8,128)(2,1)} %copy-done.2, s32[384,2]{1,0:T(8,128)} %copy-done.1, f32[384,2]{1,0:T(8,128)} %broadcast_divide_fusion.weight_ref, bf16[1152,128]{1,0:T(8,128)(2,1)} %reshape.27.returned_ref), custom_call_target="tpu_custom_call" | custom-call | tf_op jit(solution)/shard_map/combine/pallas_call | solution.py:118
  (20 shorter events, 0.1 us)
Async XLA Ops:
  6.5 21.1 %copy-start = (bf16[4,256,256]{2,1,0:T(8,128)(2,1)S(1)}, bf16[4,256,256]{2,1,0:T(8,128)(2,1)}, u32[]{:S(2)}) copy-start(bf16[4,256,256]{2,1,0:T(8,128)(2,1)} %param.15) | copy-start | bytes 1572868
  6.5 21.1 %copy-start.9 = (bf16[64,384]{1,0:T(8,128)(2,1)S(1)}, bf16[64,384]{1,0:T(8,128)(2,1)}, u32[]{:S(2)}) copy-start(bf16[64,384]{1,0:T(8,128)(2,1)} %param.14) | copy-start | bytes 147460
  7.3 8.0 %collective-permute-start = (bf16[64,128]{1,0:T(8,128)(2,1)S(1)}, bf16[64,128]{1,0:T(8,128)(2,1)S(1)}, u32[]{:S(2)}, u32[]{:S(2)}) collective-permute-start(bf16[64,128]{1,0:T(8,128)(2,1)S(1)} %slice.9), channel_id=1, source_target_pairs={{0,16},{16,32},{32,48},{48,64},{64,80},{80,96},{96,112},{112,128},... | collective-permute-start | bytes 49160 | tf_op jit(solution)/shard_map/ppermute | solution.py:179
  13.1 31.4 %copy-start.3 = (bf16[1024,128]{1,0:T(8,128)(2,1)S(1)}, bf16[1024,128]{1,0:T(8,128)(2,1)}, u32[]{:S(2)}) copy-start(bf16[1024,128]{1,0:T(8,128)(2,1)} %param.17) | copy-start | bytes 786436
  13.1 31.4 %copy-start.4 = (bf16[384,128]{1,0:T(8,128)(2,1)S(1)}, bf16[384,128]{1,0:T(8,128)(2,1)}, u32[]{:S(2)}) copy-start(bf16[384,128]{1,0:T(8,128)(2,1)} %param.18) | copy-start | bytes 294916
  13.7 31.8 %copy-start.1 = (s32[384,2]{1,0:T(8,128)}, s32[384,2]{1,0:T(8,128)S(1)}, u32[]{:S(2)}) copy-start(s32[384,2]{1,0:T(8,128)S(1)} %add.32.slot_ref) | copy-start | bytes 9220
  15.4 0.6 copy-start.6
  44.9 26.8 %copy-start.2 = (bf16[384,128]{1,0:T(8,128)(2,1)}, bf16[384,128]{1,0:T(8,128)(2,1)S(1)}, u32[]{:S(2)}) copy-start(bf16[384,128]{1,0:T(8,128)(2,1)S(1)} %fusion.3.state_ref) | copy-start | bytes 294916
  44.9 13.9 %copy-start.8 = (f32[128]{0:T(128)S(1)}, f32[128]{0:T(128)}, u32[]{:S(2)}) copy-start(f32[128]{0:T(128)} %param.19) | copy-start | bytes 1540
  46.3 25.4 %all-to-all-start = ((bf16[32,36,128]{2,1,0:T(8,128)(2,1)}), bf16[32,36,128]{2,1,0:T(8,128)(2,1)S(1)}, u32[]{:S(2)}, u32[]{:S(2)}) async-start(bf16[32,36,128]{2,1,0:T(8,128)(2,1)} %reshape.24), calls=%async_computation | async-start | bytes 655360 | tf_op jit(solution)/shard_map/all_to_all | solution.py:203
  58.8 55.3 %all-gather.5.cloned.1.call-start = ((), (), s32[]{:S(2)}) async-start(), calls=%async_computation.2 | async-start | bytes 5083136 | tf_op jit(solution)/shard_map/all_gather | solution.py:207
  74.3 110.1 %all-gather.7.cloned.1.call-start = ((), (), s32[]{:S(2)}) async-start(), calls=%async_computation.3 | async-start | bytes 10027008 | tf_op jit(solution)/shard_map/all_gather | solution.py:210
  114.1 8.4 %copy-start.5 = (f32[384,4]{0,1:T(4,128)S(1)}, f32[384,4]{0,1:T(4,128)}, u32[]{:S(2)}) copy-start(f32[384,4]{0,1:T(4,128)} %param.21) | copy-start | bytes 18436
  184.4 20.5 %copy-start.7 = (f32[384,2]{0,1:T(2,128)S(1)}, f32[384,2]{0,1:T(2,128)}, u32[]{:S(2)}) copy-start(f32[384,2]{0,1:T(2,128)} %param.22) | copy-start | bytes 9220
  194.9 22.8 %all-to-all-start.1 = ((bf16[32,36,128]{2,1,0:T(8,128)(2,1)}), bf16[32,36,128]{2,1,0:T(8,128)(2,1)S(1)}, u32[]{:S(2)}, u32[]{:S(2)}) async-start(bf16[32,36,128]{2,1,0:T(8,128)(2,1)} %reshape.26), calls=%async_computation.1 | async-start | bytes 655360 | tf_op jit(solution)/shard_map/all_to_all | solution.py:212
Sparse Core Ops, SparseCore 0:
  74.5 39.5 all-gather.4
  122.6 61.7 all-gather.6

commit v2 on v1

v2 whole, which is shorter than its diff:
```python
import jax
import jax.numpy as jnp
from jax import lax
from jax.experimental import pallas as pl
from jax.experimental.pallas import tpu as pltpu
from jax.sharding import Mesh, PartitionSpec as P

SPAN = 128
GAIN_ROWS = 16
TOGETHER = 2
epsilon = 1e-06

X_PIECES = (1152,)
U_PIECES = (1152,)

TP = ("tg", "tl")


def vmem(mib):
    return pltpu.CompilerParams(vmem_limit_bytes=mib << 20)


def padded(rows):
    return -(-rows // 8) * 8


def pool_kernel(edge_ref, own_ref, out_ref):
    length = own_ref.shape[1]
    scale = lax.axis_index("tg")
    first = lax.axis_index("sp") * length
    own = own_ref[...].astype(jnp.float32)
    layered = jnp.concatenate([edge_ref[...].astype(jnp.float32), own], axis=1)
    chosen = None
    stride = 1
    for octave in range(4):
        layered = layered + pltpu.roll(layered, stride, 1)
        stride *= 2
        chosen = layered if chosen is None else jnp.where(scale >= octave, layered, chosen)
    window = jnp.left_shift(2, scale)
    position = first + 1 + lax.broadcasted_iota(jnp.int32, own.shape, 1)
    counted = jnp.minimum(position, window).astype(jnp.float32)
    pooled = chosen[:, SPAN : SPAN + length] / counted - own
    out_ref[...] = pooled.astype(out_ref.dtype)


def pool(edge, own):
    return pl.pallas_call(
        pool_kernel,
        out_shape=jax.ShapeDtypeStruct(own.shape, jnp.bfloat16),
        compiler_params=vmem(4),
        name="pool",
    )(edge, own)


def slot_kernel(experts, pitch, routes_ref, out_ref):
    choices, length = routes_ref.shape
    number = lax.broadcasted_iota(jnp.int32, (experts, length), 0)
    named = [(number == routes_ref[k : k + 1, :]).astype(jnp.float32) for k in range(choices)]
    earlier = lax.broadcasted_iota(jnp.int32, (length, length), 0) < lax.broadcasted_iota(
        jnp.int32, (length, length), 1
    )
    before = jnp.dot(
        sum(named).astype(jnp.bfloat16),
        jnp.where(earlier, 1.0, 0.0).astype(jnp.bfloat16),
        preferred_element_type=jnp.float32,
    )
    for k in range(choices):
        rank = jnp.sum(before * named[k], axis=0, keepdims=True).astype(jnp.int32)
        out_ref[k : k + 1, :] = routes_ref[k : k + 1, :] * pitch + rank


def slot_table(routes, experts, pitch):
    def kernel(routes_ref, out_ref):
        slot_kernel(experts, pitch, routes_ref, out_ref)

    return pl.pallas_call(
        kernel,
        out_shape=jax.ShapeDtypeStruct(routes.shape, jnp.int32),
        compiler_params=vmem(8),
        name="slots",
    )(routes)


def dispatch_kernel(state_ref, slot_ref, out_ref):
    blocks, capacity, _ = out_ref.shape
    pitch = padded(capacity)
    place = lax.broadcasted_iota(jnp.int32, (blocks * pitch, state_ref.shape[0]), 0)
    chosen = place == slot_ref[0:1, :]
    for k in range(1, slot_ref.shape[0]):
        chosen = chosen | (place == slot_ref[k : k + 1, :])
    spread = jnp.where(chosen, 1.0, 0.0).astype(jnp.bfloat16)
    rows = jnp.dot(spread, state_ref[...], preferred_element_type=jnp.float32)
    for block in range(blocks):
        out_ref[block] = rows[block * pitch : block * pitch + capacity].astype(out_ref.dtype)


def dispatch(state, slots, blocks, capacity):
    return pl.pallas_call(
        dispatch_kernel,
        out_shape=jax.ShapeDtypeStruct((blocks, capacity, state.shape[1]), jnp.bfloat16),
        compiler_params=vmem(12),
        name="dispatch",
    )(state, slots)


def compact_kernel(arrived_ref, gain_ref, *refs):
    outs, rows_ref = refs[:-1], refs[-1]
    blocks, capacity, _ = arrived_ref.shape
    for block in range(blocks):
        rows_ref[block * capacity : (block + 1) * capacity] = arrived_ref[block].astype(jnp.float32)
    start = 0
    for out_ref, count in zip(outs, X_PIECES):
        out_ref[0:count] = rows_ref[start : start + count].astype(jnp.bfloat16)
        start += count
    outs[-1][count : count + GAIN_ROWS] = gain_ref[...]


def compact(arrived, gains):
    rows, width = arrived.shape[0] * arrived.shape[1], arrived.shape[2]
    counts = (*X_PIECES[:-1], X_PIECES[-1] + GAIN_ROWS)
    return pl.pallas_call(
        compact_kernel,
        out_shape=[jax.ShapeDtypeStruct((count, width), jnp.bfloat16) for count in counts],
        scratch_shapes=[pltpu.VMEM((rows, width), jnp.float32)],
        compiler_params=vmem(8),
        name="compact",
    )(arrived, gains)


def hidden_kernel(*refs):
    pieces, count = len(X_PIECES), len(U_PIECES)
    x_refs, (extra_ref, gate_ref, up_ref) = refs[:pieces], refs[pieces : pieces + 3]
    outs = refs[pieces + 3 : pieces + 3 + count]
    squares_ref, gate_sum, up_sum = refs[pieces + 3 + count :]
    step, steps = pl.program_id(0), pl.num_programs(0)
    width = squares_ref.shape[1]

    @pl.when(step == 0)
    def _():
        squares_ref[...] = jnp.zeros_like(squares_ref)
        gate_sum[...] = jnp.zeros_like(gate_sum)
        up_sum[...] = jnp.zeros_like(up_sum)

    gains = []
    for part in range(TOGETHER):
        extra = extra_ref[part].astype(jnp.float32)
        gains.append(extra[0:1] + extra[1:2] + extra[2:3])
    start = 0
    for x_ref in x_refs:
        here = pl.ds(start, x_ref.shape[1])
        start += x_ref.shape[1]
        squares, scaled = squares_ref[here, :], []
        for part in range(TOGETHER):
            state = x_ref[part].astype(jnp.float32)
            squares += state * state
            scaled.append((state * gains[part]).astype(jnp.bfloat16))
        squares_ref[here, :] = squares
        rows_in = jnp.concatenate(scaled, axis=1)
        gate_sum[here, :] += jnp.dot(rows_in, gate_ref[0], preferred_element_type=jnp.float32)
        up_sum[here, :] += jnp.dot(rows_in, up_ref[0], preferred_element_type=jnp.float32)

    @pl.when(step == steps - 1)
    def _():
        begin = 0
        for out_ref in outs:
            there = pl.ds(begin, out_ref.shape[0])
            begin += out_ref.shape[0]
            mean = jnp.sum(squares_ref[there, :], axis=1, keepdims=True) / (steps * TOGETHER * width)
            factor = lax.rsqrt(mean + epsilon)
            gate, up = gate_sum[there, :] * factor, up_sum[there, :] * factor
            out_ref[...] = (jax.nn.silu(gate) * up).astype(out_ref.dtype)


def hidden(everyone, w_gate, w_up):
    parts, _, width = everyone[-1].shape
    rows, units = sum(X_PIECES), w_gate.shape[2]
    weight = pl.BlockSpec((1, TOGETHER * width, units), lambda i: (0, i, 0))
    last = X_PIECES[-1] // GAIN_ROWS
    return pl.pallas_call(
        hidden_kernel,
        out_shape=[jax.ShapeDtypeStruct((count, units), jnp.bfloat16) for count in U_PIECES],
        grid=(parts // TOGETHER,),
        in_specs=[
            *[pl.BlockSpec((TOGETHER, count, width), lambda i: (i, 0, 0)) for count in X_PIECES],
            pl.BlockSpec((TOGETHER, GAIN_ROWS, width), lambda i: (i, last, 0)),
            weight,
            weight,
        ],
        out_specs=[pl.BlockSpec((count, units), lambda i: (0, 0)) for count in U_PIECES],
        scratch_shapes=[
            pltpu.VMEM((rows, width), jnp.float32),
            pltpu.VMEM((rows, units), jnp.float32),
            pltpu.VMEM((rows, units), jnp.float32),
        ],
        name="hidden",
    )(*everyone, everyone[-1], w_gate, w_up)


def down_kernel(*refs):
    pieces = len(U_PIECES)
    u_refs, (down_ref, out_ref, total_ref) = refs[:pieces], refs[pieces:]
    step, steps = pl.program_id(0), pl.num_programs(0)

    @pl.when(step == 0)
    def _():
        total_ref[...] = jnp.zeros_like(total_ref)

    start = 0
    for u_ref in u_refs:
        here = pl.ds(start, u_ref.shape[1])
        start += u_ref.shape[1]
        rows_in = jnp.concatenate([u_ref[part] for part in range(TOGETHER)], axis=1)
        total_ref[here, :] += jnp.dot(rows_in, down_ref[0], preferred_element_type=jnp.float32)

    @pl.when(step == steps - 1)
    def _():
        blocks, capacity, _ = out_ref.shape
        for block in range(blocks):
            out_ref[block] = total_ref[block * capacity : (block + 1) * capacity].astype(out_ref.dtype)


def down(everyone, w_down, blocks, capacity):
    parts, _, units = everyone[-1].shape
    width = w_down.shape[2]
    return pl.pallas_call(
        down_kernel,
        out_shape=jax.ShapeDtypeStruct((blocks, capacity, width), jnp.bfloat16),
        grid=(parts // TOGETHER,),
        in_specs=[
            *[pl.BlockSpec((TOGETHER, count, units), lambda i: (i, 0, 0)) for count in U_PIECES],
            pl.BlockSpec((1, TOGETHER * units, width), lambda i: (0, i, 0)),
        ],
        out_specs=pl.BlockSpec((blocks, capacity, width), lambda i: (0, 0, 0)),
        scratch_shapes=[pltpu.VMEM((blocks * capacity, width), jnp.float32)],
        name="down",
    )(*everyone, w_down)


def combine_kernel(state_ref, slot_ref, weight_ref, returned_ref, out_ref, rows_ref):
    blocks, capacity, _ = returned_ref.shape
    pitch = padded(capacity)
    rows_ref[...] = jnp.zeros_like(rows_ref)
    for block in range(blocks):
        rows_ref[block * pitch : block * pitch + capacity] = returned_ref[block].astype(jnp.float32)
    rows = rows_ref[...].astype(jnp.bfloat16)
    place = lax.broadcasted_iota(jnp.int32, (state_ref.shape[0], blocks * pitch), 1)
    total = jnp.zeros(out_ref.shape, jnp.float32)
    for choice in range(slot_ref.shape[1]):
        pick = jnp.where(place == slot_ref[:, choice : choice + 1], 1.0, 0.0).astype(jnp.bfloat16)
        picked = jnp.dot(pick, rows, preferred_element_type=jnp.float32)
        total += weight_ref[:, choice : choice + 1] * picked
    out_ref[...] = (state_ref[...].astype(jnp.float32) + total).astype(out_ref.dtype)


def combine(state, slots, weights, returned):
    blocks, capacity, width = returned.shape
    return pl.pallas_call(
        combine_kernel,
        out_shape=jax.ShapeDtypeStruct(state.shape, jnp.bfloat16),
        scratch_shapes=[pltpu.VMEM((blocks * padded(capacity), width), jnp.float32)],
        compiler_params=vmem(12),
        name="combine",
    )(state, slots, weights, returned)


def route_weights(routes, group_logits, expert_scores, per_group):
    raised = jnp.exp(group_logits)
    group_prob = raised / jnp.sum(raised, axis=1, keepdims=True)
    owning_group = routes // per_group
    groups_iota = jnp.arange(group_logits.shape[1], dtype=jnp.int32)
    picked = jnp.sum(
        jnp.where(owning_group[:, :, None] == groups_iota[None, None, :], group_prob[:, None, :], 0.0),
        axis=2,
    )
    lifted = jnp.exp(expert_scores)
    return picked * lifted / jnp.sum(lifted, axis=1, keepdims=True)


def gain_rows(gain):
    row = lax.broadcasted_iota(jnp.int32, (GAIN_ROWS, gain.shape[0]), 0)
    rows, rest = jnp.zeros(row.shape, jnp.float32), gain[None, :]
    for k in range(3):
        head = lax.reduce_precision(rest, 8, 7)
        rows = jnp.where(row == k, head, rows)
        rest = rest - head
    return rows.astype(jnp.bfloat16)


def per_device(
    pool_input,
    pool_gate,
    pool_mix,
    pool_scale,
    out_proj,
    residual,
    norm_gain,
    routes,
    group_logits,
    expert_scores,
    w_gate,
    w_up,
    w_down,
):
    channels, length = pool_input.shape
    blocks = lax.axis_size("sp")
    experts = blocks * w_gate.shape[0]
    capacity = 3 * routes.shape[1] * length // (2 * experts)
    scale, quarter = lax.axis_index("tg"), lax.axis_index("tl")
    own_first = (scale * lax.axis_size("tl") + quarter) * channels
    edge = lax.ppermute(
        pool_input[:, length - SPAN :], "sp", [(i, i + 1) for i in range(blocks - 1)]
    )
    slots = slot_table(routes.T, experts, padded(capacity))
    gains = gain_rows(norm_gain)
    pooled = pool(edge, pool_input)
    group = lax.all_gather(pooled, "tl", axis=0, tiled=True)
    mix = lax.dynamic_slice(
        pool_mix, (scale, 0, quarter * channels), (1, pool_mix.shape[1], channels)
    )[0]
    mixed = lax.dot_general(mix, group, (((0,), (0,)), ((), ())), preferred_element_type=jnp.float32)
    own_scale = lax.dynamic_slice(pool_scale, (own_first,), (channels,))
    branch = (jax.nn.sigmoid(pool_gate.astype(jnp.float32)) * mixed * own_scale[:, None]).astype(jnp.bfloat16)
    branches = lax.all_gather(branch, TP, axis=0, tiled=True)
    product = lax.dot_general(
        branches, out_proj, (((0,), (0,)), ((), ())), preferred_element_type=jnp.float32
    )
    state = (residual.astype(jnp.float32) + product).astype(jnp.bfloat16)

    sent = dispatch(state, slots, blocks, capacity)
    arrived = lax.all_to_all(sent, "sp", split_axis=0, concat_axis=0, tiled=True)
    everyone = [lax.all_gather(piece, TP, axis=0, tiled=False) for piece in compact(arrived, gains)]
    activated = hidden(everyone, w_gate, w_up)
    units = [lax.all_gather(piece, TP, axis=0, tiled=False) for piece in activated]
    result = down(units, w_down, blocks, capacity)
    returned = lax.all_to_all(result, "sp", split_axis=0, concat_axis=0, tiled=True)
    weights = route_weights(routes, group_logits, expert_scores, experts // group_logits.shape[1])
    return combine(state, slots.T, weights, returned)


def solution(mesh):
    fine = Mesh(mesh.devices.reshape(mesh.devices.shape[0], 4, -1), ("sp", *TP))
    placed = (
        P(TP, "sp"),
        P(TP, "sp"),
        P(),
        P(),
        P(None, TP),
        P("sp", TP),
        P(TP),
        P("sp", None),
        P("sp", None),
        P("sp", None),
        P("sp", None, TP),
        P("sp", None, TP),
        P("sp", None, TP),
    )
    return jax.shard_map(
        per_device, mesh=fine, in_specs=placed, out_specs=P("sp", TP), check_vma=False
    )
```

time: 229 us -> 223 us (0.974)
  local copies, waits for them, and re-layouts: 9.69 us -> 3.32 us
    reshape x4 -> x0, local copies, waits for them, and re-layouts: 3.35 us -> none  [the longest x1 1.74 us: per_device(): result.reshape(blocks, capacity, -1)]
    concatenate x1 -> x0, local copies, waits for them, and re-layouts: 2.5 us -> none  [per_device(): carried = jnp.concatenate([arrived, gain_rows(norm_gain)], axis=0)]
    pallas_call x2 -> x5, Pallas kernels: 17.2 us -> 19.4 us  [the longest x1 8.64 us: hidden(): pl.pallas_call(hidden_kernel, out_shape=[jax.ShapeDtypeStruct((count, uni...]
  transfers between devices with their start and end apart: 5 -> 5, of which waited for: 4 -> 4; matrix products, arithmetic and copies ran while one was open for 2% -> 1% of each run, Pallas kernels for 0% -> 0%
where the time goes in v2:
time: 223 us; the launch traced here: 222 us
  waiting for transfers between devices  126 us (57%)
  starting transfers between devices  28.1 us (13%)
  blocking collectives  26.3 us (12%)
  Pallas kernels  21.2 us (10%)
  between operations  13.6 us (6%)
  local copies, waits for them, and re-layouts  3.32 us (1%)
  matrix products  2.44 us (1%)
    all_gather x2, waiting for transfers between devices, per_device(): lax.all_gather(piece, TP, axis=0, tiled=False)  101 us
    all_gather x1, blocking collectives, per_device(): branches = lax.all_gather(branch, TP, axis=0, tiled=True)  16.6 us
    all_to_all x1, starting transfers between devices, per_device(): lax.all_to_all(sent, 'sp', split_axis=0, concat_axis=0, tiled=True)  14.2 us
    all_to_all x1, waiting for transfers between devices, per_device(): lax.all_to_all(result, 'sp', split_axis=0, concat_axis=0, tiled=True)  12.5 us
    all_to_all x1, waiting for transfers between devices, per_device(): lax.all_to_all(sent, 'sp', split_axis=0, concat_axis=0, tiled=True)  12.1 us
    all_to_all x1, starting transfers between devices, per_device(): lax.all_to_all(result, 'sp', split_axis=0, concat_axis=0, tiled=True)  9.91 us
    all_gather x1, blocking collectives, per_device(): group = lax.all_gather(pooled, 'tl', axis=0, tiled=True)  9.63 us
    pallas_call x1, Pallas kernels, hidden(): pl.pallas_call(hidden_kernel, out_shape=[jax.ShapeDtypeStruct((count, uni...  8.64 us
  transfers between devices with their start and end apart: 5, of which 4 were waited for; matrix products, arithmetic and copies ran while one was open for 1% of the time, Pallas kernels for 0%

profile of v2, /device:TPU:1, one launch (start us, length us, event | category | flops | bytes accessed | tf_op | source)
XLA Modules:
  0.0 221.9 jit_solution(6459752322602308409)
XLA Ops:
  6.5 0.0 copy-start
  6.5 0.0 copy-start.3
  6.5 0.0 copy-start.4
  6.5 0.8 slice.3
  7.3 3.9 %collective-permute-start = (bf16[64,128]{1,0:T(8,128)(2,1)S(1)}, bf16[64,128]{1,0:T(8,128)(2,1)S(1)}, u32[]{:S(2)}, u32[]{:S(2)}) collective-permute-start(bf16[64,128]{1,0:T(8,128)(2,1)S(1)} %slice.3), channel_id=1, source_target_pairs={{0,16},{16,32},{32,48},{48,64},{64,80},{80,96},{96,112},{112,128},... | collective-permute-start | bytes 49160 | tf_op jit(solution)/shard_map/ppermute | solution.py:310
  11.3 0.0 copy-start.2
  11.3 0.7 copy-done.2
  12.0 0.2 slots.1.slot_ref
  12.1 0.8 dynamic_slice.7
  12.9 0.0 collective-permute-done.edge_ref
  12.9 0.0 copy-start.1
  12.9 0.8 copy-done.1
  13.7 0.4 pool.1
  14.1 9.6 %all_gather.18 = bf16[256,384]{1,0:T(8,128)(2,1)S(1)} all-gather(bf16[64,384]{1,0:T(8,128)(2,1)S(1)} %pool.1), channel_id=1, replica_groups=mesh['sp'=32,'tg'=4,'tl'=4] {'tl'}, dimensions={0}, use_global_device_ids=true | all-gather | bytes 245760 | tf_op jit(solution)/shard_map/all_gather | solution.py:316
  23.7 0.0 copy-done
  23.7 1.1 fusion.2
  24.8 16.6 %all_gather.19 = bf16[1024,384]{1,0:T(8,128)(2,1)S(1)} all-gather(bf16[64,384]{1,0:T(8,128)(2,1)S(1)} %fusion.2), channel_id=1, replica_groups=mesh['sp'=32,'tg'=4,'tl'=4] {'tg','tl'}, dimensions={0}, use_global_device_ids=true | all-gather | bytes 835584 | tf_op jit(solution)/shard_map/all_gather | solution.py:323
  41.4 1.4 fusion.state_ref
  42.8 1.3 dispatch.1
  44.1 14.2 %all-to-all-start = ((bf16[32,36,128]{2,1,0:T(8,128)(2,1)}), bf16[32,36,128]{2,1,0:T(8,128)(2,1)S(1)}, u32[]{:S(2)}, u32[]{:S(2)}) async-start(bf16[32,36,128]{2,1,0:T(8,128)(2,1)} %dispatch.1), calls=%async_computation | async-start | bytes 655360 | tf_op jit(solution)/shard_map/all_to_all | solution.py:330
  58.3 0.0 all-gather.5.cloned.1.call-start
  58.3 0.7 subtract_reduce-precision_fusion
  59.0 0.1 select_convert_fusion.gain_ref
  59.1 12.1 %all-to-all-done.arrived_ref = bf16[32,36,128]{2,1,0:T(8,128)(2,1)S(1)} async-done(((bf16[32,36,128]{2,1,0:T(8,128)(2,1)}), bf16[32,36,128]{2,1,0:T(8,128)(2,1)S(1)}, u32[]{:S(2)}, u32[]{:S(2)}) %all-to-all-start) | async-done | bytes 294944 | tf_op jit(solution)/shard_map/all_to_all | solution.py:330
  71.2 0.8 compact.1
  72.0 0.0 all-gather.5.cloned.1.call-update
  72.0 0.0 all-gather.7.cloned.1.call-start
  72.0 39.7 %all-gather.5.cloned.1.call-done = bf16[18688,128]{1,0:T(8,128)(2,1)} async-done(((bf16[1168,128]{1,0:T(8,128)(2,1)}), bf16[18688,128]{1,0:T(8,128)(2,1)}) %all-gather.5.cloned.1.call-update) | async-done | bytes 4784144 | tf_op jit(solution)/shard_map/all_gather | solution.py:331
  111.7 0.0 copy-start.5
  111.7 8.6 %hidden.1 = bf16[1152,256]{1,0:T(8,128)(2,1)} custom-call(bf16[16,1168,128]{2,1,0:T(8,128)(2,1)} %bitcast.12, bf16[16,1168,128]{2,1,0:T(8,128)(2,1)} %bitcast.13, bf16[1,2048,256]{2,1,0:T(8,128)(2,1)} %refs_2_.1, bf16[1,2048,256]{2,1,0:T(8,128)(2,1)} %refs_3_.1), custom_call_target="tpu_custom_call" | custom-call | tf_op jit(solution)/shard_map/hidden/pallas_call | solution.py:179
  120.4 0.0 all-gather.7.cloned.1.call-update
  120.4 0.1 copy.24
  120.5 0.0 copy-done.4
  120.6 0.0 copy-done.3
  120.6 61.7 %all-gather.7.cloned.1.call-done = bf16[18432,256]{1,0:T(8,128)(2,1)} async-done(((bf16[1152,256]{1,0:T(8,128)(2,1)}), bf16[18432,256]{1,0:T(8,128)(2,1)}) %all-gather.7.cloned.1.call-update) | async-done | bytes 9437200 | tf_op jit(solution)/shard_map/all_gather | solution.py:333
  182.3 8.6 %down.1 = bf16[32,36,128]{2,1,0:T(8,128)(2,1)} custom-call(bf16[16,1152,256]{2,1,0:T(8,128)(2,1)} %bitcast.14, bf16[1,4096,128]{2,1,0:T(8,128)(2,1)} %refs_1_.1), custom_call_target="tpu_custom_call" | custom-call | tf_op jit(solution)/shard_map/down/pallas_call | solution.py:225
  190.9 9.9 %all-to-all-start.1 = ((bf16[32,36,128]{2,1,0:T(8,128)(2,1)}), bf16[32,36,128]{2,1,0:T(8,128)(2,1)S(1)}, u32[]{:S(2)}, u32[]{:S(2)}) async-start(bf16[32,36,128]{2,1,0:T(8,128)(2,1)} %down.1), calls=%async_computation.1 | async-start | bytes 655360 | tf_op jit(solution)/shard_map/all_to_all | solution.py:335
  200.8 0.0 copy-done.5
  200.9 0.1 copy.25
  201.0 0.1 broadcast_divide_fusion.weight_ref
  201.1 12.5 %all-to-all-done.1.returned_ref = bf16[32,36,128]{2,1,0:T(8,128)(2,1)S(1)} async-done(((bf16[32,36,128]{2,1,0:T(8,128)(2,1)}), bf16[32,36,128]{2,1,0:T(8,128)(2,1)S(1)}, u32[]{:S(2)}, u32[]{:S(2)}) %all-to-all-start.1) | async-done | bytes 294944 | tf_op jit(solution)/shard_map/all_to_all | solution.py:335
  213.7 1.4 combine.1
  (7 shorter events, 0.1 us)
Async XLA Ops:
  6.5 17.2 %copy-start = (bf16[4,256,256]{2,1,0:T(8,128)(2,1)S(1)}, bf16[4,256,256]{2,1,0:T(8,128)(2,1)}, u32[]{:S(2)}) copy-start(bf16[4,256,256]{2,1,0:T(8,128)(2,1)} %param.15) | copy-start | bytes 1572868
  6.5 114.0 %copy-start.3 = (s32[384,2]{0,1:T(2,128)S(1)}, s32[384,2]{0,1:T(2,128)}, u32[]{:S(2)}) copy-start(s32[384,2]{0,1:T(2,128)} %param.20) | copy-start | bytes 9220
  6.5 114.0 %copy-start.4 = (f32[384,4]{0,1:T(4,128)S(1)}, f32[384,4]{0,1:T(4,128)}, u32[]{:S(2)}) copy-start(f32[384,4]{0,1:T(4,128)} %param.21) | copy-start | bytes 18436
  7.3 5.6 %collective-permute-start = (bf16[64,128]{1,0:T(8,128)(2,1)S(1)}, bf16[64,128]{1,0:T(8,128)(2,1)S(1)}, u32[]{:S(2)}, u32[]{:S(2)}) collective-permute-start(bf16[64,128]{1,0:T(8,128)(2,1)S(1)} %slice.3), channel_id=1, source_target_pairs={{0,16},{16,32},{32,48},{48,64},{64,80},{80,96},{96,112},{112,128},... | collective-permute-start | bytes 49160 | tf_op jit(solution)/shard_map/ppermute | solution.py:310
  11.3 0.7 copy-start.2
  12.9 0.8 copy-start.1
  44.1 27.1 %all-to-all-start = ((bf16[32,36,128]{2,1,0:T(8,128)(2,1)}), bf16[32,36,128]{2,1,0:T(8,128)(2,1)S(1)}, u32[]{:S(2)}, u32[]{:S(2)}) async-start(bf16[32,36,128]{2,1,0:T(8,128)(2,1)} %dispatch.1), calls=%async_computation | async-start | bytes 655360 | tf_op jit(solution)/shard_map/all_to_all | solution.py:330
  58.3 53.5 %all-gather.5.cloned.1.call-start = ((), (), s32[]{:S(2)}) async-start(), calls=%async_computation.2 | async-start | bytes 5083136 | tf_op jit(solution)/shard_map/all_gather | solution.py:331
  72.0 110.3 %all-gather.7.cloned.1.call-start = ((), (), s32[]{:S(2)}) async-start(), calls=%async_computation.3 | async-start | bytes 10027008 | tf_op jit(solution)/shard_map/all_gather | solution.py:333
  111.7 89.1 %copy-start.5 = (f32[384,2]{0,1:T(2,128)S(1)}, f32[384,2]{0,1:T(2,128)}, u32[]{:S(2)}) copy-start(f32[384,2]{0,1:T(2,128)} %param.22) | copy-start | bytes 9220
  190.9 22.8 %all-to-all-start.1 = ((bf16[32,36,128]{2,1,0:T(8,128)(2,1)}), bf16[32,36,128]{2,1,0:T(8,128)(2,1)S(1)}, u32[]{:S(2)}, u32[]{:S(2)}) async-start(bf16[32,36,128]{2,1,0:T(8,128)(2,1)} %down.1), calls=%async_computation.1 | async-start | bytes 655360 | tf_op jit(solution)/shard_map/all_to_all | solution.py:335
Sparse Core Ops, SparseCore 0:
  72.1 39.5 all-gather.4
  120.5 61.7 all-gather.6

commit v3 on v2

--- a/solution.py
+++ b/solution.py
@@ -10,8 +10,8 @@
 TOGETHER = 2
 epsilon = 1e-06
 
-X_PIECES = (1152,)
-U_PIECES = (1152,)
+X_PIECES = (720, 208, 224)
+U_PIECES = (864, 96, 96, 96)
 
 TP = ("tg", "tl")
 

time: 223 us -> 227 us (1.018)
  blocking collectives: 26.3 us -> 135 us
  waiting for transfers between devices: 126 us -> 24.8 us
  starting transfers between devices: 28.1 us -> 24.2 us
    all_gather x0 -> x5, blocking collectives: none -> 109 us  [per_device(): lax.all_gather(piece, TP, axis=0, tiled=False)]
    all_gather x2, waiting for transfers between devices: 101 us -> 0.01 us  [per_device(): lax.all_gather(piece, TP, axis=0, tiled=False)]
    all_to_all x1, starting transfers between devices: 9.91 us -> 6.02 us  [per_device(): lax.all_to_all(result, 'sp', split_axis=0, concat_axis=0, tiled=True)]
  transfers between devices with their start and end apart: 5 -> 5, of which waited for: 4 -> 2; matrix products, arithmetic and copies ran while one was open for 1% -> 1% of each run, Pallas kernels for 0% -> 0%
where the time goes in v3:
time: 227 us; the launch traced here: 226 us
  blocking collectives  135 us (59%)
  waiting for transfers between devices  24.8 us (11%)
  starting transfers between devices  24.2 us (11%)
  Pallas kernels  21.3 us (9%)
  between operations  13.6 us (6%)
  local copies, waits for them, and re-layouts  3.31 us (1%)
  matrix products  2.46 us (1%)
    all_gather x5, blocking collectives, per_device(): lax.all_gather(piece, TP, axis=0, tiled=False)  109 us
    all_gather x1, blocking collectives, per_device(): branches = lax.all_gather(branch, TP, axis=0, tiled=True)  16.6 us
    all_to_all x1, starting transfers between devices, per_device(): lax.all_to_all(sent, 'sp', split_axis=0, concat_axis=0, tiled=True)  14.2 us
    all_to_all x1, waiting for transfers between devices, per_device(): lax.all_to_all(result, 'sp', split_axis=0, concat_axis=0, tiled=True)  12.6 us
    all_to_all x1, waiting for transfers between devices, per_device(): lax.all_to_all(sent, 'sp', split_axis=0, concat_axis=0, tiled=True)  12.1 us
    all_gather x1, blocking collectives, per_device(): group = lax.all_gather(pooled, 'tl', axis=0, tiled=True)  9.63 us
    pallas_call x1, Pallas kernels, hidden(): pl.pallas_call(hidden_kernel, out_shape=[jax.ShapeDtypeStruct((count, uni...  8.7 us
    pallas_call x1, Pallas kernels, down(): pl.pallas_call(down_kernel, out_shape=jax.ShapeDtypeStruct((blocks, capac...  8.61 us
  transfers between devices with their start and end apart: 5, of which 2 were waited for; matrix products, arithmetic and copies ran while one was open for 1% of the time, Pallas kernels for 0%

profile of v3, /device:TPU:1, one launch (start us, length us, event | category | flops | bytes accessed | tf_op | source)
XLA Modules:
  0.0 225.8 jit_solution(14051285773798548079)
XLA Ops:
  6.5 0.0 copy-start
  6.5 0.8 slice.3
  7.3 3.9 %collective-permute-start = (bf16[64,128]{1,0:T(8,128)(2,1)S(1)}, bf16[64,128]{1,0:T(8,128)(2,1)S(1)}, u32[]{:S(2)}, u32[]{:S(2)}) collective-permute-start(bf16[64,128]{1,0:T(8,128)(2,1)S(1)} %slice.3), channel_id=1, source_target_pairs={{0,16},{16,32},{32,48},{48,64},{64,80},{80,96},{96,112},{112,128},... | collective-permute-start | bytes 49160 | tf_op jit(solution)/shard_map/ppermute | solution.py:310
  11.3 0.0 copy-start.2
  11.3 0.7 copy-done.2
  11.9 0.2 slots.1.slot_ref
  12.1 0.8 dynamic_slice.7
  12.9 0.0 collective-permute-done.edge_ref
  12.9 0.0 copy-start.1
  12.9 0.8 copy-done.1
  13.7 0.4 pool.1
  14.1 9.6 %all_gather.48 = bf16[256,384]{1,0:T(8,128)(2,1)S(1)} all-gather(bf16[64,384]{1,0:T(8,128)(2,1)S(1)} %pool.1), channel_id=1, replica_groups=mesh['sp'=32,'tg'=4,'tl'=4] {'tl'}, dimensions={0}, use_global_device_ids=true | all-gather | bytes 245760 | tf_op jit(solution)/shard_map/all_gather | solution.py:316
  23.7 0.0 copy-done
  23.7 1.1 fusion.2
  24.8 0.0 copy-start.4
  24.8 0.0 copy-start.3
  24.8 16.6 %all_gather.49 = bf16[1024,384]{1,0:T(8,128)(2,1)S(1)} all-gather(bf16[64,384]{1,0:T(8,128)(2,1)S(1)} %fusion.2), channel_id=1, replica_groups=mesh['sp'=32,'tg'=4,'tl'=4] {'tg','tl'}, dimensions={0}, use_global_device_ids=true | all-gather | bytes 835584 | tf_op jit(solution)/shard_map/all_gather | solution.py:323
  41.4 1.4 fusion.state_ref
  42.8 1.3 dispatch.1
  44.1 14.2 %all-to-all-start = ((bf16[32,36,128]{2,1,0:T(8,128)(2,1)}), bf16[32,36,128]{2,1,0:T(8,128)(2,1)S(1)}, u32[]{:S(2)}, u32[]{:S(2)}) async-start(bf16[32,36,128]{2,1,0:T(8,128)(2,1)} %dispatch.1), calls=%async_computation | async-start | bytes 655360 | tf_op jit(solution)/shard_map/all_to_all | solution.py:330
  58.3 0.0 all-gather.10.cloned.1.call-start
  58.3 0.7 subtract_reduce-precision_fusion
  59.0 0.1 select_convert_fusion.gain_ref
  59.1 12.1 %all-to-all-done.arrived_ref = bf16[32,36,128]{2,1,0:T(8,128)(2,1)S(1)} async-done(((bf16[32,36,128]{2,1,0:T(8,128)(2,1)}), bf16[32,36,128]{2,1,0:T(8,128)(2,1)S(1)}, u32[]{:S(2)}, u32[]{:S(2)}) %all-to-all-start) | async-done | bytes 294944 | tf_op jit(solution)/shard_map/all_to_all | solution.py:330
  71.2 0.7 compact.1
  71.9 0.0 all-gather.10.cloned.1.call-update
  72.0 0.0 all-gather.12.cloned.1.call-start
  72.0 21.1 %all-gather.1 = bf16[3328,128]{1,0:T(8,128)(2,1)} all-gather(bf16[208,128]{1,0:T(8,128)(2,1)S(1)} %get-tuple-element.13), channel_id=3, replica_groups=mesh['sp'=32,'tg'=4,'tl'=4] {'tg','tl'}, dimensions={0}, use_global_device_ids=true | all-gather | bytes 905216 | tf_op jit(solution)/shard_map/all_gather | solution.py:331
  93.1 23.8 %all-gather.2 = bf16[3840,128]{1,0:T(8,128)(2,1)} all-gather(bf16[240,128]{1,0:T(8,128)(2,1)S(1)} %get-tuple-element.14), channel_id=4, replica_groups=mesh['sp'=32,'tg'=4,'tl'=4] {'tg','tl'}, dimensions={0}, use_global_device_ids=true | all-gather | bytes 1044480 | tf_op jit(solution)/shard_map/all_gather | solution.py:331
  116.9 0.0 all-gather.10.cloned.1.call-done
  116.9 8.7 %hidden.1 = (bf16[864,256]{1,0:T(8,128)(2,1)}, bf16[96,256]{1,0:T(8,128)(2,1)}, bf16[96,256]{1,0:T(8,128)(2,1)}, bf16[96,256]{1,0:T(8,128)(2,1)}) custom-call(bf16[16,720,128]{2,1,0:T(8,128)(2,1)} %bitcast.24, bf16[16,208,128]{2,1,0:T(8,128)(2,1)} %bitcast.20, bf16[16,240,128]{2,1,0:T(8,128)(2,1)} %bitcast.17, bf16[16,240,128]{2,1,0:T(8,128)(2,1)} %bitcast.18, ...), custom_call_target="tpu_custom_call" | custom-call | tf_op jit(solution)/shard_map/hidden/pallas_call | solution.py:179
  125.6 0.0 all-gather.12.cloned.1.call-update
  125.6 0.0 copy-start.5
  125.6 0.1 copy.24
  125.8 0.0 copy-done.4
  125.8 0.0 copy-done.3
  125.8 20.5 %all-gather.4 = bf16[1536,256]{1,0:T(8,128)(2,1)} all-gather(bf16[96,256]{1,0:T(8,128)(2,1)} %get-tuple-element.16), channel_id=6, replica_groups=mesh['sp'=32,'tg'=4,'tl'=4] {'tg','tl'}, dimensions={0}, use_global_device_ids=true | all-gather | bytes 835584 | tf_op jit(solution)/shard_map/all_gather | solution.py:333
  146.3 25.4 %all-gather.5 = bf16[1536,256]{1,0:T(8,128)(2,1)} all-gather(bf16[96,256]{1,0:T(8,128)(2,1)} %get-tuple-element.17), channel_id=7, replica_groups=mesh['sp'=32,'tg'=4,'tl'=4] {'tg','tl'}, dimensions={0}, use_global_device_ids=true | all-gather | bytes 835584 | tf_op jit(solution)/shard_map/all_gather | solution.py:333
  171.7 18.2 %all-gather.6 = bf16[1536,256]{1,0:T(8,128)(2,1)} all-gather(bf16[96,256]{1,0:T(8,128)(2,1)} %get-tuple-element.18), channel_id=8, replica_groups=mesh['sp'=32,'tg'=4,'tl'=4] {'tg','tl'}, dimensions={0}, use_global_device_ids=true | all-gather | bytes 835584 | tf_op jit(solution)/shard_map/all_gather | solution.py:333
  190.0 0.0 all-gather.12.cloned.1.call-done
  190.0 8.6 %down.1 = bf16[32,36,128]{2,1,0:T(8,128)(2,1)} custom-call(bf16[16,864,256]{2,1,0:T(8,128)(2,1)} %bitcast.19, bf16[16,96,256]{2,1,0:T(8,128)(2,1)} %bitcast.21, bf16[16,96,256]{2,1,0:T(8,128)(2,1)} %bitcast.22, bf16[16,96,256]{2,1,0:T(8,128)(2,1)} %bitcast.23, bf16[1,4096,128]{2,1,0:T(8,128)(2,1)} %refs_4_.3), custom_call_target="tpu_custom_call" | custom-call | tf_op jit(solution)/shard_map/down/pallas_call | solution.py:225
  198.6 6.0 %all-to-all-start.1 = ((bf16[32,36,128]{2,1,0:T(8,128)(2,1)}), bf16[32,36,128]{2,1,0:T(8,128)(2,1)S(1)}, u32[]{:S(2)}, u32[]{:S(2)}) async-start(bf16[32,36,128]{2,1,0:T(8,128)(2,1)} %down.1), calls=%async_computation.1 | async-start | bytes 655360 | tf_op jit(solution)/shard_map/all_to_all | solution.py:335
  204.7 0.0 copy-done.5
  204.7 0.1 copy.25
  204.8 0.1 broadcast_divide_fusion.weight_ref
  205.0 12.6 %all-to-all-done.1.returned_ref = bf16[32,36,128]{2,1,0:T(8,128)(2,1)S(1)} async-done(((bf16[32,36,128]{2,1,0:T(8,128)(2,1)}), bf16[32,36,128]{2,1,0:T(8,128)(2,1)S(1)}, u32[]{:S(2)}, u32[]{:S(2)}) %all-to-all-start.1) | async-done | bytes 294944 | tf_op jit(solution)/shard_map/all_to_all | solution.py:335
  217.6 1.4 combine.1
  (7 shorter events, 0.1 us)
Async XLA Ops:
  6.5 17.2 %copy-start = (bf16[4,256,256]{2,1,0:T(8,128)(2,1)S(1)}, bf16[4,256,256]{2,1,0:T(8,128)(2,1)}, u32[]{:S(2)}) copy-start(bf16[4,256,256]{2,1,0:T(8,128)(2,1)} %param.15) | copy-start | bytes 1572868
  7.3 5.6 %collective-permute-start = (bf16[64,128]{1,0:T(8,128)(2,1)S(1)}, bf16[64,128]{1,0:T(8,128)(2,1)S(1)}, u32[]{:S(2)}, u32[]{:S(2)}) collective-permute-start(bf16[64,128]{1,0:T(8,128)(2,1)S(1)} %slice.3), channel_id=1, source_target_pairs={{0,16},{16,32},{32,48},{48,64},{64,80},{80,96},{96,112},{112,128},... | collective-permute-start | bytes 49160 | tf_op jit(solution)/shard_map/ppermute | solution.py:310
  11.3 0.7 copy-start.2
  12.9 0.8 copy-start.1
  24.8 101.0 %copy-start.4 = (f32[384,4]{0,1:T(4,128)S(1)}, f32[384,4]{0,1:T(4,128)}, u32[]{:S(2)}) copy-start(f32[384,4]{0,1:T(4,128)} %param.21) | copy-start | bytes 18436
  24.8 101.0 %copy-start.3 = (s32[384,2]{0,1:T(2,128)S(1)}, s32[384,2]{0,1:T(2,128)}, u32[]{:S(2)}) copy-start(s32[384,2]{0,1:T(2,128)} %param.20) | copy-start | bytes 9220
  44.1 27.1 %all-to-all-start = ((bf16[32,36,128]{2,1,0:T(8,128)(2,1)}), bf16[32,36,128]{2,1,0:T(8,128)(2,1)S(1)}, u32[]{:S(2)}, u32[]{:S(2)}) async-start(bf16[32,36,128]{2,1,0:T(8,128)(2,1)} %dispatch.1), calls=%async_computation | async-start | bytes 655360 | tf_op jit(solution)/shard_map/all_to_all | solution.py:330
  58.3 58.6 %all-gather.10.cloned.1.call-start = ((), (), s32[]{:S(2)}) async-start(), calls=%async_computation.2 | async-start | bytes 3133440 | tf_op jit(solution)/shard_map/all_gather | solution.py:331
  72.0 118.0 %all-gather.12.cloned.1.call-start = ((), (), s32[]{:S(2)}) async-start(), calls=%async_computation.3 | async-start | bytes 7520256 | tf_op jit(solution)/shard_map/all_gather | solution.py:333
  125.6 79.1 %copy-start.5 = (f32[384,2]{0,1:T(2,128)S(1)}, f32[384,2]{0,1:T(2,128)}, u32[]{:S(2)}) copy-start(f32[384,2]{0,1:T(2,128)} %param.22) | copy-start | bytes 9220
  198.6 19.0 %all-to-all-start.1 = ((bf16[32,36,128]{2,1,0:T(8,128)(2,1)}), bf16[32,36,128]{2,1,0:T(8,128)(2,1)S(1)}, u32[]{:S(2)}, u32[]{:S(2)}) async-start(bf16[32,36,128]{2,1,0:T(8,128)(2,1)} %down.1), calls=%async_computation.1 | async-start | bytes 655360 | tf_op jit(solution)/shard_map/all_to_all | solution.py:335
Sparse Core Ops, SparseCore 0:
  72.1 38.7 all-gather.9
  125.7 51.1 all-gather.11

commit v4 on v2

--- a/solution.py
+++ b/solution.py
@@ -7,11 +7,12 @@
 
 SPAN = 128
 GAIN_ROWS = 16
-TOGETHER = 2
+TOGETHER = 4
+DOWN_TOGETHER = 2
 epsilon = 1e-06
 
 X_PIECES = (1152,)
-U_PIECES = (1152,)
+U_PIECES = (928, 112, 112)
 
 TP = ("tg", "tl")
 
@@ -127,111 +128,149 @@
     )(arrived, gains)
 
 
+def parts_of(hbm_refs, buffers, sems, part):
+    return [
+        pltpu.make_async_copy(hbm.at[part], buffer.at[part], sems.at[part, piece])
+        for piece, (hbm, buffer) in enumerate(zip(hbm_refs, buffers))
+    ]
+
+
 def hidden_kernel(*refs):
     pieces, count = len(X_PIECES), len(U_PIECES)
-    x_refs, (extra_ref, gate_ref, up_ref) = refs[:pieces], refs[pieces : pieces + 3]
-    outs = refs[pieces + 3 : pieces + 3 + count]
-    squares_ref, gate_sum, up_sum = refs[pieces + 3 + count :]
-    step, steps = pl.program_id(0), pl.num_programs(0)
-    width = squares_ref.shape[1]
-
-    @pl.when(step == 0)
-    def _():
-        squares_ref[...] = jnp.zeros_like(squares_ref)
-        gate_sum[...] = jnp.zeros_like(gate_sum)
-        up_sum[...] = jnp.zeros_like(up_sum)
-
-    gains = []
-    for part in range(TOGETHER):
-        extra = extra_ref[part].astype(jnp.float32)
-        gains.append(extra[0:1] + extra[1:2] + extra[2:3])
-    start = 0
-    for x_ref in x_refs:
-        here = pl.ds(start, x_ref.shape[1])
-        start += x_ref.shape[1]
-        squares, scaled = squares_ref[here, :], []
-        for part in range(TOGETHER):
-            state = x_ref[part].astype(jnp.float32)
-            squares += state * state
-            scaled.append((state * gains[part]).astype(jnp.bfloat16))
-        squares_ref[here, :] = squares
-        rows_in = jnp.concatenate(scaled, axis=1)
-        gate_sum[here, :] += jnp.dot(rows_in, gate_ref[0], preferred_element_type=jnp.float32)
-        up_sum[here, :] += jnp.dot(rows_in, up_ref[0], preferred_element_type=jnp.float32)
-
-    @pl.when(step == steps - 1)
-    def _():
-        begin = 0
-        for out_ref in outs:
-            there = pl.ds(begin, out_ref.shape[0])
-            begin += out_ref.shape[0]
-            mean = jnp.sum(squares_ref[there, :], axis=1, keepdims=True) / (steps * TOGETHER * width)
-            factor = lax.rsqrt(mean + epsilon)
-            gate, up = gate_sum[there, :] * factor, up_sum[there, :] * factor
-            out_ref[...] = (jax.nn.silu(gate) * up).astype(out_ref.dtype)
+    x_hbm, (gate_hbm, up_hbm) = refs[:pieces], refs[pieces : pieces + 2]
+    outs, scratch = refs[pieces + 2 : pieces + 2 + count], refs[pieces + 2 + count :]
+    x_refs, (gate_ref, up_ref, squares_ref, gate_sum, up_sum, x_sems, w_sems) = scratch[:pieces], scratch[pieces:]
+    parts, width = x_refs[0].shape[0], x_refs[0].shape[2]
+    depth = TOGETHER * width
+    chunks = parts // TOGETHER
+
+    def weights_of(chunk):
+        here = pl.ds(chunk * depth, depth)
+        return [
+            pltpu.make_async_copy(hbm.at[0, here], ref.at[here], w_sems.at[chunk, k])
+            for k, (hbm, ref) in enumerate(((gate_hbm, gate_ref), (up_hbm, up_ref)))
+        ]
+
+    copies = []
+    for chunk in range(chunks):
+        here = weights_of(chunk)
+        for part in range(chunk * TOGETHER, (chunk + 1) * TOGETHER):
+            here += parts_of(x_hbm, x_refs, x_sems, part)
+        for copy in here:
+            copy.start()
+        copies.append(here)
+    for chunk in range(chunks):
+        for copy in copies[chunk]:
+            copy.wait()
+        mine = range(chunk * TOGETHER, (chunk + 1) * TOGETHER)
+        gains = []
+        for part in mine:
+            extra = x_refs[-1][part, pl.ds(X_PIECES[-1], GAIN_ROWS), :].astype(jnp.float32)
+            gains.append(extra[0:1] + extra[1:2] + extra[2:3])
+        start = 0
+        for x_ref, rows in zip(x_refs, X_PIECES):
+            here = pl.ds(start, rows)
+            start += rows
+            squares, scaled = None, []
+            for part, gain in zip(mine, gains):
+                state = x_ref[part, pl.ds(0, rows), :].astype(jnp.float32)
+                squares = state * state if squares is None else squares + state * state
+                scaled.append((state * gain).astype(jnp.bfloat16))
+            rows_in = jnp.concatenate(scaled, axis=1)
+            deep = pl.ds(chunk * depth, depth)
+            gate = jnp.dot(rows_in, gate_ref[deep, :], preferred_element_type=jnp.float32)
+            up = jnp.dot(rows_in, up_ref[deep, :], preferred_element_type=jnp.float32)
+            if chunk == 0:
+                squares_ref[here, :], gate_sum[here, :], up_sum[here, :] = squares, gate, up
+            else:
+                squares_ref[here, :] += squares
+                gate_sum[here, :] += gate
+                up_sum[here, :] += up
+    begin = 0
+    for out_ref in outs:
+        there = pl.ds(begin, out_ref.shape[0])
+        begin += out_ref.shape[0]
+        mean = jnp.sum(squares_ref[there, :], axis=1, keepdims=True) / (parts * width)
+        factor = lax.rsqrt(mean + epsilon)
+        gate, up = gate_sum[there, :] * factor, up_sum[there, :] * factor
+        out_ref[...] = (jax.nn.silu(gate) * up).astype(out_ref.dtype)
 
 
 def hidden(everyone, w_gate, w_up):
     parts, _, width = everyone[-1].shape
     rows, units = sum(X_PIECES), w_gate.shape[2]
-    weight = pl.BlockSpec((1, TOGETHER * width, units), lambda i: (0, i, 0))
-    last = X_PIECES[-1] // GAIN_ROWS
+    hbm = pl.BlockSpec(memory_space=pltpu.HBM)
     return pl.pallas_call(
         hidden_kernel,
         out_shape=[jax.ShapeDtypeStruct((count, units), jnp.bfloat16) for count in U_PIECES],
-        grid=(parts // TOGETHER,),
-        in_specs=[
-            *[pl.BlockSpec((TOGETHER, count, width), lambda i: (i, 0, 0)) for count in X_PIECES],
-            pl.BlockSpec((TOGETHER, GAIN_ROWS, width), lambda i: (i, last, 0)),
-            weight,
-            weight,
-        ],
-        out_specs=[pl.BlockSpec((count, units), lambda i: (0, 0)) for count in U_PIECES],
+        in_specs=[hbm] * (len(everyone) + 2),
         scratch_shapes=[
+            *[pltpu.VMEM(piece.shape, piece.dtype) for piece in everyone],
+            pltpu.VMEM(w_gate.shape[1:], w_gate.dtype),
+            pltpu.VMEM(w_up.shape[1:], w_up.dtype),
             pltpu.VMEM((rows, width), jnp.float32),
             pltpu.VMEM((rows, units), jnp.float32),
             pltpu.VMEM((rows, units), jnp.float32),
+            pltpu.SemaphoreType.DMA((parts, len(everyone))),
+            pltpu.SemaphoreType.DMA((parts // TOGETHER, 2)),
         ],
         name="hidden",
-    )(*everyone, everyone[-1], w_gate, w_up)
+    )(*everyone, w_gate, w_up)
 
 
 def down_kernel(*refs):
     pieces = len(U_PIECES)
-    u_refs, (down_ref, out_ref, total_ref) = refs[:pieces], refs[pieces:]
-    step, steps = pl.program_id(0), pl.num_programs(0)
-
-    @pl.when(step == 0)
-    def _():
-        total_ref[...] = jnp.zeros_like(total_ref)
-
-    start = 0
-    for u_ref in u_refs:
-        here = pl.ds(start, u_ref.shape[1])
-        start += u_ref.shape[1]
-        rows_in = jnp.concatenate([u_ref[part] for part in range(TOGETHER)], axis=1)
-        total_ref[here, :] += jnp.dot(rows_in, down_ref[0], preferred_element_type=jnp.float32)
-
-    @pl.when(step == steps - 1)
-    def _():
-        blocks, capacity, _ = out_ref.shape
-        for block in range(blocks):
-            out_ref[block] = total_ref[block * capacity : (block + 1) * capacity].astype(out_ref.dtype)
+    u_hbm, (down_hbm, out_ref), scratch = refs[:pieces], refs[pieces : pieces + 2], refs[pieces + 2 :]
+    u_refs, (down_ref, total_ref, u_sems, w_sems) = scratch[:pieces], scratch[pieces:]
+    parts, _, units = u_refs[0].shape
+    depth = DOWN_TOGETHER * units
+    chunks = parts // DOWN_TOGETHER
+    copies = []
+    for chunk in range(chunks):
+        deep = pl.ds(chunk * depth, depth)
+        here = [pltpu.make_async_copy(down_hbm.at[0, deep], down_ref.at[deep], w_sems.at[chunk])]
+        for part in range(chunk * DOWN_TOGETHER, (chunk + 1) * DOWN_TOGETHER):
+            here += parts_of(u_hbm, u_refs, u_sems, part)
+        for copy in here:
+            copy.start()
+        copies.append(here)
+    for chunk in range(chunks):
+        for copy in copies[chunk]:
+            copy.wait()
+        start = 0
+        for u_ref in u_refs:
+            here = pl.ds(start, u_ref.shape[1])
+            start += u_ref.shape[1]
+            rows_in = jnp.concatenate(
+                [u_ref[part] for part in range(chunk * DOWN_TOGETHER, (chunk + 1) * DOWN_TOGETHER)], axis=1
+            )
+            product = jnp.dot(
+                rows_in, down_ref[pl.ds(chunk * depth, depth), :], preferred_element_type=jnp.float32
+            )
+            if chunk == 0:
+                total_ref[here, :] = product
+            else:
+                total_ref[here, :] += product
+    blocks, capacity, _ = out_ref.shape
+    for block in range(blocks):
+        out_ref[block] = total_ref[block * capacity : (block + 1) * capacity].astype(out_ref.dtype)
 
 
 def down(everyone, w_down, blocks, capacity):
-    parts, _, units = everyone[-1].shape
+    parts = everyone[0].shape[0]
     width = w_down.shape[2]
+    hbm = pl.BlockSpec(memory_space=pltpu.HBM)
     return pl.pallas_call(
         down_kernel,
         out_shape=jax.ShapeDtypeStruct((blocks, capacity, width), jnp.bfloat16),
-        grid=(parts // TOGETHER,),
-        in_specs=[
-            *[pl.BlockSpec((TOGETHER, count, units), lambda i: (i, 0, 0)) for count in U_PIECES],
-            pl.BlockSpec((1, TOGETHER * units, width), lambda i: (0, i, 0)),
+        in_specs=[hbm] * (len(everyone) + 1),
+        scratch_shapes=[
+            *[pltpu.VMEM(piece.shape, piece.dtype) for piece in everyone],
+            pltpu.VMEM(w_down.shape[1:], w_down.dtype),
+            pltpu.VMEM((blocks * capacity, width), jnp.float32),
+            pltpu.SemaphoreType.DMA((parts, len(everyone))),
+            pltpu.SemaphoreType.DMA((parts // DOWN_TOGETHER,)),
         ],
-        out_specs=pl.BlockSpec((blocks, capacity, width), lambda i: (0, 0, 0)),
-        scratch_shapes=[pltpu.VMEM((blocks * capacity, width), jnp.float32)],
         name="down",
     )(*everyone, w_down)
 

time: 223 us -> 218 us (0.978)
  waiting for transfers between devices: 126 us -> 76.7 us
  blocking collectives: 26.3 us -> 72.5 us
    all_gather x2, waiting for transfers between devices: 101 us -> 52 us  [per_device(): lax.all_gather(piece, TP, axis=0, tiled=False)]
    all_gather x0 -> x2, blocking collectives: none -> 46.2 us  [per_device(): lax.all_gather(piece, TP, axis=0, tiled=False)]
    pallas_call x1, Pallas kernels: 8.64 us -> 5.9 us  [hidden(): pl.pallas_call(hidden_kernel, out_shape=[jax.ShapeDtypeStruct((count, uni...]
where the time goes in v4:
time: 218 us; the launch traced here: 217 us
  waiting for transfers between devices  76.7 us (35%)
  blocking collectives  72.5 us (33%)
  starting transfers between devices  28.1 us (13%)
  Pallas kernels  19.6 us (9%)
  between operations  13.6 us (6%)
  local copies, waits for them, and re-layouts  3.33 us (2%)
  matrix products  2.44 us (1%)
    all_gather x2, waiting for transfers between devices, per_device(): lax.all_gather(piece, TP, axis=0, tiled=False)  52 us
    all_gather x2, blocking collectives, per_device(): lax.all_gather(piece, TP, axis=0, tiled=False)  46.2 us
    all_gather x1, blocking collectives, per_device(): branches = lax.all_gather(branch, TP, axis=0, tiled=True)  16.6 us
    all_to_all x1, starting transfers between devices, per_device(): lax.all_to_all(sent, 'sp', split_axis=0, concat_axis=0, tiled=True)  14.2 us
    all_to_all x1, waiting for transfers between devices, per_device(): lax.all_to_all(result, 'sp', split_axis=0, concat_axis=0, tiled=True)  12.5 us
    all_to_all x1, waiting for transfers between devices, per_device(): lax.all_to_all(sent, 'sp', split_axis=0, concat_axis=0, tiled=True)  12.1 us
    all_to_all x1, starting transfers between devices, per_device(): lax.all_to_all(result, 'sp', split_axis=0, concat_axis=0, tiled=True)  9.91 us
    pallas_call x1, Pallas kernels, down(): pl.pallas_call(down_kernel, out_shape=jax.ShapeDtypeStruct((blocks, capac...  9.7 us
  transfers between devices with their start and end apart: 5, of which 4 were waited for; matrix products, arithmetic and copies ran while one was open for 1% of the time, Pallas kernels for 0%

profile of v4, /device:TPU:1, one launch (start us, length us, event | category | flops | bytes accessed | tf_op | source)
XLA Modules:
  0.0 217.2 jit_solution(9965983058257139744)
XLA Ops:
  6.5 0.0 copy-start
  6.5 0.0 copy-start.3
  6.5 0.0 copy-start.4
  6.5 0.8 slice.3
  7.3 3.9 %collective-permute-start = (bf16[64,128]{1,0:T(8,128)(2,1)S(1)}, bf16[64,128]{1,0:T(8,128)(2,1)S(1)}, u32[]{:S(2)}, u32[]{:S(2)}) collective-permute-start(bf16[64,128]{1,0:T(8,128)(2,1)S(1)} %slice.3), channel_id=1, source_target_pairs={{0,16},{16,32},{32,48},{48,64},{64,80},{80,96},{96,112},{112,128},... | collective-permute-start | bytes 49160 | tf_op jit(solution)/shard_map/ppermute | solution.py:349
  11.3 0.0 copy-start.2
  11.3 0.7 copy-done.2
  12.0 0.2 slots.1.slot_ref
  12.1 0.8 dynamic_slice.7
  12.9 0.0 collective-permute-done.edge_ref
  12.9 0.0 copy-start.1
  12.9 0.8 copy-done.1
  13.7 0.4 pool.1
  14.1 9.6 %all_gather.30 = bf16[256,384]{1,0:T(8,128)(2,1)S(1)} all-gather(bf16[64,384]{1,0:T(8,128)(2,1)S(1)} %pool.1), channel_id=1, replica_groups=mesh['sp'=32,'tg'=4,'tl'=4] {'tl'}, dimensions={0}, use_global_device_ids=true | all-gather | bytes 245760 | tf_op jit(solution)/shard_map/all_gather | solution.py:355
  23.7 0.0 copy-done
  23.7 1.1 fusion.2
  24.8 16.6 %all_gather.31 = bf16[1024,384]{1,0:T(8,128)(2,1)S(1)} all-gather(bf16[64,384]{1,0:T(8,128)(2,1)S(1)} %fusion.2), channel_id=1, replica_groups=mesh['sp'=32,'tg'=4,'tl'=4] {'tg','tl'}, dimensions={0}, use_global_device_ids=true | all-gather | bytes 835584 | tf_op jit(solution)/shard_map/all_gather | solution.py:362
  41.4 1.4 fusion.state_ref
  42.8 1.3 dispatch.1
  44.1 14.2 %all-to-all-start = ((bf16[32,36,128]{2,1,0:T(8,128)(2,1)}), bf16[32,36,128]{2,1,0:T(8,128)(2,1)S(1)}, u32[]{:S(2)}, u32[]{:S(2)}) async-start(bf16[32,36,128]{2,1,0:T(8,128)(2,1)} %dispatch.1), calls=%async_computation | async-start | bytes 655360 | tf_op jit(solution)/shard_map/all_to_all | solution.py:369
  58.3 0.0 all-gather.7.cloned.1.call-start
  58.3 0.7 subtract_reduce-precision_fusion
  59.0 0.1 select_convert_fusion.gain_ref
  59.1 12.1 %all-to-all-done.arrived_ref = bf16[32,36,128]{2,1,0:T(8,128)(2,1)S(1)} async-done(((bf16[32,36,128]{2,1,0:T(8,128)(2,1)}), bf16[32,36,128]{2,1,0:T(8,128)(2,1)S(1)}, u32[]{:S(2)}, u32[]{:S(2)}) %all-to-all-start) | async-done | bytes 294944 | tf_op jit(solution)/shard_map/all_to_all | solution.py:369
  71.2 0.8 compact.1
  72.0 0.0 all-gather.7.cloned.1.call-update
  72.0 0.0 all-gather.9.cloned.1.call-start
  72.0 39.7 %all-gather.7.cloned.1.call-done = bf16[18688,128]{1,0:T(8,128)(2,1)} async-done(((bf16[1168,128]{1,0:T(8,128)(2,1)}), bf16[18688,128]{1,0:T(8,128)(2,1)}) %all-gather.7.cloned.1.call-update) | async-done | bytes 4784144 | tf_op jit(solution)/shard_map/all_gather | solution.py:370
  111.7 5.9 %hidden.1 = (bf16[928,256]{1,0:T(8,128)(2,1)}, bf16[112,256]{1,0:T(8,128)(2,1)}, bf16[112,256]{1,0:T(8,128)(2,1)}) custom-call(bf16[16,1168,128]{2,1,0:T(8,128)(2,1)} %bitcast.15, bf16[1,2048,256]{2,1,0:T(8,128)(2,1)} %refs_1_.1, bf16[1,2048,256]{2,1,0:T(8,128)(2,1)} %refs_2_.1), custom_call_target="tpu_custom_call" | custom-call | tf_op jit(solution)/shard_map/hidden/pallas_call | solution.py:203
  117.6 0.0 copy-start.5
  117.7 0.0 all-gather.9.cloned.1.call-update
  117.7 0.1 copy.24
  117.8 0.0 copy-done.4
  117.9 0.0 copy-done.3
  117.9 21.9 %all-gather.2 = bf16[1792,256]{1,0:T(8,128)(2,1)} all-gather(bf16[112,256]{1,0:T(8,128)(2,1)} %get-tuple-element.9), channel_id=4, replica_groups=mesh['sp'=32,'tg'=4,'tl'=4] {'tg','tl'}, dimensions={0}, use_global_device_ids=true | all-gather | bytes 974848 | tf_op jit(solution)/shard_map/all_gather | solution.py:372
  139.8 24.3 %all-gather.3 = bf16[1792,256]{1,0:T(8,128)(2,1)} all-gather(bf16[112,256]{1,0:T(8,128)(2,1)} %get-tuple-element.10), channel_id=5, replica_groups=mesh['sp'=32,'tg'=4,'tl'=4] {'tg','tl'}, dimensions={0}, use_global_device_ids=true | all-gather | bytes 974848 | tf_op jit(solution)/shard_map/all_gather | solution.py:372
  164.1 12.3 %all-gather.9.cloned.1.call-done = bf16[14848,256]{1,0:T(8,128)(2,1)} async-done(((bf16[928,256]{1,0:T(8,128)(2,1)}), bf16[14848,256]{1,0:T(8,128)(2,1)}) %all-gather.9.cloned.1.call-update) | async-done | bytes 7602192 | tf_op jit(solution)/shard_map/all_gather | solution.py:372
  176.5 9.7 %down.1 = bf16[32,36,128]{2,1,0:T(8,128)(2,1)} custom-call(bf16[16,928,256]{2,1,0:T(8,128)(2,1)} %bitcast.14, bf16[16,112,256]{2,1,0:T(8,128)(2,1)} %bitcast.16, bf16[16,112,256]{2,1,0:T(8,128)(2,1)} %bitcast.17, bf16[1,4096,128]{2,1,0:T(8,128)(2,1)} %refs_3_.1), custom_call_target="tpu_custom_call" | custom-call | tf_op jit(solution)/shard_map/down/pallas_call | solution.py:263
  186.2 9.9 %all-to-all-start.1 = ((bf16[32,36,128]{2,1,0:T(8,128)(2,1)}), bf16[32,36,128]{2,1,0:T(8,128)(2,1)S(1)}, u32[]{:S(2)}, u32[]{:S(2)}) async-start(bf16[32,36,128]{2,1,0:T(8,128)(2,1)} %down.1), calls=%async_computation.1 | async-start | bytes 655360 | tf_op jit(solution)/shard_map/all_to_all | solution.py:374
  196.1 0.0 copy-done.5
  196.2 0.1 copy.25
  196.3 0.1 broadcast_divide_fusion.weight_ref
  196.4 12.5 %all-to-all-done.1.returned_ref = bf16[32,36,128]{2,1,0:T(8,128)(2,1)S(1)} async-done(((bf16[32,36,128]{2,1,0:T(8,128)(2,1)}), bf16[32,36,128]{2,1,0:T(8,128)(2,1)S(1)}, u32[]{:S(2)}, u32[]{:S(2)}) %all-to-all-start.1) | async-done | bytes 294944 | tf_op jit(solution)/shard_map/all_to_all | solution.py:374
  209.0 1.4 combine.1
  (7 shorter events, 0.1 us)
Async XLA Ops:
  6.5 17.2 %copy-start = (bf16[4,256,256]{2,1,0:T(8,128)(2,1)S(1)}, bf16[4,256,256]{2,1,0:T(8,128)(2,1)}, u32[]{:S(2)}) copy-start(bf16[4,256,256]{2,1,0:T(8,128)(2,1)} %param.15) | copy-start | bytes 1572868
  6.5 111.3 %copy-start.3 = (s32[384,2]{0,1:T(2,128)S(1)}, s32[384,2]{0,1:T(2,128)}, u32[]{:S(2)}) copy-start(s32[384,2]{0,1:T(2,128)} %param.20) | copy-start | bytes 9220
  6.5 111.3 %copy-start.4 = (f32[384,4]{0,1:T(4,128)S(1)}, f32[384,4]{0,1:T(4,128)}, u32[]{:S(2)}) copy-start(f32[384,4]{0,1:T(4,128)} %param.21) | copy-start | bytes 18436
  7.3 5.6 %collective-permute-start = (bf16[64,128]{1,0:T(8,128)(2,1)S(1)}, bf16[64,128]{1,0:T(8,128)(2,1)S(1)}, u32[]{:S(2)}, u32[]{:S(2)}) collective-permute-start(bf16[64,128]{1,0:T(8,128)(2,1)S(1)} %slice.3), channel_id=1, source_target_pairs={{0,16},{16,32},{32,48},{48,64},{64,80},{80,96},{96,112},{112,128},... | collective-permute-start | bytes 49160 | tf_op jit(solution)/shard_map/ppermute | solution.py:349
  11.3 0.7 copy-start.2
  12.9 0.8 copy-start.1
  44.1 27.1 %all-to-all-start = ((bf16[32,36,128]{2,1,0:T(8,128)(2,1)}), bf16[32,36,128]{2,1,0:T(8,128)(2,1)S(1)}, u32[]{:S(2)}, u32[]{:S(2)}) async-start(bf16[32,36,128]{2,1,0:T(8,128)(2,1)} %dispatch.1), calls=%async_computation | async-start | bytes 655360 | tf_op jit(solution)/shard_map/all_to_all | solution.py:369
  58.3 53.5 %all-gather.7.cloned.1.call-start = ((), (), s32[]{:S(2)}) async-start(), calls=%async_computation.2 | async-start | bytes 5083136 | tf_op jit(solution)/shard_map/all_gather | solution.py:370
  72.0 104.5 %all-gather.9.cloned.1.call-start = ((), (), s32[]{:S(2)}) async-start(), calls=%async_computation.3 | async-start | bytes 8077312 | tf_op jit(solution)/shard_map/all_gather | solution.py:372
  117.6 78.5 %copy-start.5 = (f32[384,2]{0,1:T(2,128)S(1)}, f32[384,2]{0,1:T(2,128)}, u32[]{:S(2)}) copy-start(f32[384,2]{0,1:T(2,128)} %param.22) | copy-start | bytes 9220
  186.2 22.8 %all-to-all-start.1 = ((bf16[32,36,128]{2,1,0:T(8,128)(2,1)}), bf16[32,36,128]{2,1,0:T(8,128)(2,1)S(1)}, u32[]{:S(2)}, u32[]{:S(2)}) async-start(bf16[32,36,128]{2,1,0:T(8,128)(2,1)} %down.1), calls=%async_computation.1 | async-start | bytes 655360 | tf_op jit(solution)/shard_map/all_to_all | solution.py:374
Sparse Core Ops, SparseCore 0:
  72.1 39.5 all-gather.6
  117.8 58.6 all-gather.8

commit v5 on v4

v5 whole, which is shorter than its diff:
```python
import jax
import jax.numpy as jnp
from jax import lax
from jax.experimental import pallas as pl
from jax.experimental.pallas import tpu as pltpu
from jax.sharding import Mesh, PartitionSpec as P

SPAN = 128
GAIN_ROWS = 16
TOGETHER = 2
AHEAD = 2
DOWN_AHEAD = 4
ROWS = 288
epsilon = 1e-06

LINE = ("tg", "yl")
SCALE = ("yl", "core")
TP = (*LINE, "core")


def vmem(mib):
    return pltpu.CompilerParams(vmem_limit_bytes=mib << 20)


def padded(rows):
    return -(-rows // 8) * 8


def pool_kernel(edge_ref, own_ref, out_ref):
    length = own_ref.shape[1]
    scale = lax.axis_index("tg")
    first = lax.axis_index("sp") * length
    own = own_ref[...].astype(jnp.float32)
    layered = jnp.concatenate([edge_ref[...].astype(jnp.float32), own], axis=1)
    chosen = None
    stride = 1
    for octave in range(4):
        layered = layered + pltpu.roll(layered, stride, 1)
        stride *= 2
        chosen = layered if chosen is None else jnp.where(scale >= octave, layered, chosen)
    window = jnp.left_shift(2, scale)
    position = first + 1 + lax.broadcasted_iota(jnp.int32, own.shape, 1)
    counted = jnp.minimum(position, window).astype(jnp.float32)
    pooled = chosen[:, SPAN : SPAN + length] / counted - own
    out_ref[...] = pooled.astype(out_ref.dtype)


def pool(edge, own):
    return pl.pallas_call(
        pool_kernel,
        out_shape=jax.ShapeDtypeStruct(own.shape, jnp.bfloat16),
        compiler_params=vmem(4),
        name="pool",
    )(edge, own)


def slot_kernel(experts, pitch, routes_ref, out_ref):
    choices, length = routes_ref.shape
    number = lax.broadcasted_iota(jnp.int32, (experts, length), 0)
    named = [(number == routes_ref[k : k + 1, :]).astype(jnp.float32) for k in range(choices)]
    earlier = lax.broadcasted_iota(jnp.int32, (length, length), 0) < lax.broadcasted_iota(
        jnp.int32, (length, length), 1
    )
    before = jnp.dot(
        sum(named).astype(jnp.bfloat16),
        jnp.where(earlier, 1.0, 0.0).astype(jnp.bfloat16),
        preferred_element_type=jnp.float32,
    )
    for k in range(choices):
        rank = jnp.sum(before * named[k], axis=0, keepdims=True).astype(jnp.int32)
        out_ref[k : k + 1, :] = routes_ref[k : k + 1, :] * pitch + rank


def slot_table(routes, experts, pitch):
    def kernel(routes_ref, out_ref):
        slot_kernel(experts, pitch, routes_ref, out_ref)

    return pl.pallas_call(
        kernel,
        out_shape=jax.ShapeDtypeStruct(routes.shape, jnp.int32),
        compiler_params=vmem(8),
        name="slots",
    )(routes)


def dispatch_kernel(pitch, own_ref, other_ref, slot_ref, out_ref):
    blocks, share, _ = out_ref.shape
    core, stride = lax.axis_index("core"), padded(share)
    first = core == 0
    own, other = own_ref[...].astype(jnp.float32), other_ref[...].astype(jnp.float32)
    state = jnp.concatenate([jnp.where(first, own, other), jnp.where(first, other, own)], axis=1)
    count = lax.broadcasted_iota(jnp.int32, (stride, own_ref.shape[0]), 0) + core * share
    place = jnp.concatenate([count + block * pitch for block in range(blocks)], axis=0)
    chosen = place == slot_ref[0:1, :]
    for k in range(1, slot_ref.shape[0]):
        chosen = chosen | (place == slot_ref[k : k + 1, :])
    spread = jnp.where(chosen, 1.0, 0.0).astype(jnp.bfloat16)
    rows = jnp.dot(spread, state.astype(jnp.bfloat16), preferred_element_type=jnp.float32)
    for block in range(blocks):
        out_ref[block] = rows[block * stride : block * stride + share].astype(out_ref.dtype)


def dispatch(own, other, slots, blocks, capacity):
    def kernel(*refs):
        dispatch_kernel(padded(capacity), *refs)

    return pl.pallas_call(
        kernel,
        out_shape=jax.ShapeDtypeStruct((blocks, capacity // 2, 2 * own.shape[1]), jnp.bfloat16),
        compiler_params=vmem(12),
        name="dispatch",
    )(own, other, slots)


def compact_kernel(arrived_ref, own_ref, other_ref, out_ref, rows_ref):
    blocks, share, width = arrived_ref.shape
    rows = blocks * share
    first = lax.axis_index("core") == 0
    for block in range(blocks):
        rows_ref[block * share : (block + 1) * share] = arrived_ref[block].astype(jnp.float32)
    own, other = own_ref[...].astype(jnp.float32), other_ref[...].astype(jnp.float32)
    rows_ref[rows:, : width // 2] = jnp.where(first, own, other)
    rows_ref[rows:, width // 2 :] = jnp.where(first, other, own)
    out_ref[...] = rows_ref[...].astype(out_ref.dtype)


def compact(arrived, own_gains, other_gains):
    shape = (arrived.shape[0] * arrived.shape[1] + GAIN_ROWS, arrived.shape[2])
    return pl.pallas_call(
        compact_kernel,
        out_shape=jax.ShapeDtypeStruct(shape, jnp.bfloat16),
        scratch_shapes=[pltpu.VMEM(shape, jnp.float32)],
        compiler_params=vmem(8),
        name="compact",
    )(arrived, own_gains, other_gains)


def tiles(rows, limit):
    size = -(-rows // -(-rows // limit) // 16) * 16
    return [(first, min(size, rows - first)) for first in range(0, rows, size)]


def begin_ahead(copies, ahead):
    for copy in sum(copies[:ahead], []):
        copy.start()


def turn_over(copies, chunk, ahead):
    for copy in copies[chunk]:
        copy.wait()
    for copy in sum(copies[chunk + ahead : chunk + ahead + 1], []):
        copy.start()


def hidden_kernel(x_hbm, gate_hbm, up_hbm, gate2_hbm, up2_hbm, out_ref, x_ref, gate_ref, up_ref, squares_ref, gate_sum, up_sum, x_sems, w_sems):
    parts, rows, width = x_ref.shape
    rows -= GAIN_ROWS
    units = gate_ref.shape[2]
    depth = TOGETHER * width
    core = lax.axis_index("core")
    copies = []
    for chunk in range(parts // TOGETHER):
        deep = pl.ds(chunk * depth, depth)
        here = [
            pltpu.make_async_copy(hbm.at[deep], ref.at[which, deep], w_sems.at[chunk, k])
            for k, (hbm, ref, which) in enumerate(
                (
                    (gate_hbm, gate_ref, core),
                    (up_hbm, up_ref, core),
                    (gate2_hbm, gate_ref, 1 - core),
                    (up2_hbm, up_ref, 1 - core),
                )
            )
        ]
        for part in range(chunk * TOGETHER, (chunk + 1) * TOGETHER):
            here.append(pltpu.make_async_copy(x_hbm.at[part], x_ref.at[part], x_sems.at[part]))
        copies.append(here)
    begin_ahead(copies, AHEAD)
    for chunk in range(len(copies)):
        turn_over(copies, chunk, AHEAD)
        mine = range(chunk * TOGETHER, (chunk + 1) * TOGETHER)
        deep = pl.ds(chunk * depth, depth)
        gains = []
        for part in mine:
            extra = x_ref[part, pl.ds(rows, GAIN_ROWS), :].astype(jnp.float32)
            gains.append(extra[0:1] + extra[1:2] + extra[2:3])
        for first, count in tiles(rows, ROWS):
            here = pl.ds(first, count)
            squares, scaled = None, []
            for part, gain in zip(mine, gains):
                state = x_ref[part, here, :].astype(jnp.float32)
                squares = state * state if squares is None else squares + state * state
                scaled.append((state * gain).astype(jnp.bfloat16))
            rows_in = jnp.concatenate(scaled, axis=1)
            if chunk == 0:
                squares_ref[here, :] = squares
            else:
                squares_ref[here, :] += squares
            for which in range(2):
                there = pl.ds(which * units, units)
                gate = jnp.dot(rows_in, gate_ref[which, deep, :], preferred_element_type=jnp.float32)
                up = jnp.dot(rows_in, up_ref[which, deep, :], preferred_element_type=jnp.float32)
                if chunk == 0:
                    gate_sum[here, there], up_sum[here, there] = gate, up
                else:
                    gate_sum[here, there] += gate
                    up_sum[here, there] += up
    for first, count in tiles(rows, ROWS):
        here = pl.ds(first, count)
        mean = jnp.sum(squares_ref[here, :], axis=1, keepdims=True) / (parts * width)
        factor = lax.rsqrt(mean + epsilon)
        gate, up = gate_sum[here, :] * factor, up_sum[here, :] * factor
        out_ref[here, :] = (jax.nn.silu(gate) * up).astype(out_ref.dtype)


def hidden(everyone, w_gate, w_up, other_gate, other_up):
    parts, extended, width = everyone.shape
    rows, units = extended - GAIN_ROWS, w_gate.shape[1]
    return pl.pallas_call(
        hidden_kernel,
        out_shape=jax.ShapeDtypeStruct((rows, 2 * units), jnp.bfloat16),
        in_specs=[pl.BlockSpec(memory_space=pltpu.HBM)] * 5,
        scratch_shapes=[
            pltpu.VMEM(everyone.shape, everyone.dtype),
            pltpu.VMEM((2, *w_gate.shape), w_gate.dtype),
            pltpu.VMEM((2, *w_up.shape), w_up.dtype),
            pltpu.VMEM((rows, width), jnp.float32),
            pltpu.VMEM((rows, 2 * units), jnp.float32),
            pltpu.VMEM((rows, 2 * units), jnp.float32),
            pltpu.SemaphoreType.DMA((parts,)),
            pltpu.SemaphoreType.DMA((parts // TOGETHER, 4)),
        ],
        name="hidden",
    )(everyone, w_gate, w_up, other_gate, other_up)


def down_kernel(u_hbm, own_hbm, other_hbm, own_out, other_out, u_ref, own_ref, other_ref, total_ref, u_sems, w_sems):
    parts, rows, units = u_ref.shape
    width = own_ref.shape[1]
    copies = []
    for part in range(parts):
        deep = pl.ds(part * units, units)
        copies.append(
            [
                pltpu.make_async_copy(own_hbm.at[deep], own_ref.at[deep], w_sems.at[part, 0]),
                pltpu.make_async_copy(other_hbm.at[deep], other_ref.at[deep], w_sems.at[part, 1]),
                pltpu.make_async_copy(u_hbm.at[part], u_ref.at[part], u_sems.at[part]),
            ]
        )
    begin_ahead(copies, DOWN_AHEAD)
    for part in range(parts):
        turn_over(copies, part, DOWN_AHEAD)
        deep = pl.ds(part * units, units)
        columns = jnp.concatenate([own_ref[deep, :], other_ref[deep, :]], axis=1)
        for first, count in tiles(rows, ROWS):
            here = pl.ds(first, count)
            product = jnp.dot(u_ref[part, here, :], columns, preferred_element_type=jnp.float32)
            if part == 0:
                total_ref[here, :] = product
            else:
                total_ref[here, :] += product
    own_out[...] = total_ref[:, :width].astype(own_out.dtype)
    other_out[...] = total_ref[:, width:].astype(other_out.dtype)


def down(everyone, own, other):
    parts, rows, units = everyone.shape
    width = own.shape[1]
    half = jax.ShapeDtypeStruct((rows, width), jnp.bfloat16)
    return pl.pallas_call(
        down_kernel,
        out_shape=[half, half],
        in_specs=[pl.BlockSpec(memory_space=pltpu.HBM)] * 3,
        scratch_shapes=[
            pltpu.VMEM(everyone.shape, everyone.dtype),
            pltpu.VMEM(own.shape, own.dtype),
            pltpu.VMEM(other.shape, other.dtype),
            pltpu.VMEM((rows, 2 * width), jnp.float32),
            pltpu.SemaphoreType.DMA((parts,)),
            pltpu.SemaphoreType.DMA((parts, 2)),
        ],
        name="down",
    )(everyone, own, other)


def unfold_kernel(own_ref, other_ref, out_ref, wide_ref):
    blocks, capacity, _ = out_ref.shape
    share = capacity // 2
    first = lax.axis_index("core") == 0
    own, other = own_ref[...].astype(jnp.float32), other_ref[...].astype(jnp.float32)
    lower, upper = jnp.where(first, own, other), jnp.where(first, other, own)
    for block in range(blocks):
        here = slice(block * share, (block + 1) * share)
        wide_ref[block, 0:share] = lower[here]
        wide_ref[block, share:capacity] = upper[here]
    out_ref[...] = wide_ref[...].astype(out_ref.dtype)


def unfold(own, other, blocks, capacity):
    shape = (blocks, capacity, own.shape[1])
    return pl.pallas_call(
        unfold_kernel,
        out_shape=jax.ShapeDtypeStruct(shape, own.dtype),
        scratch_shapes=[pltpu.VMEM(shape, jnp.float32)],
        compiler_params=vmem(8),
        name="unfold",
    )(own, other)


def combine_kernel(state_ref, slot_ref, weight_ref, returned_ref, out_ref, rows_ref):
    blocks, capacity, _ = returned_ref.shape
    pitch = padded(capacity)
    rows_ref[...] = jnp.zeros_like(rows_ref)
    for block in range(blocks):
        rows_ref[block * pitch : block * pitch + capacity] = returned_ref[block].astype(jnp.float32)
    rows = rows_ref[...].astype(jnp.bfloat16)
    place = lax.broadcasted_iota(jnp.int32, (state_ref.shape[0], blocks * pitch), 1)
    total = jnp.zeros(out_ref.shape, jnp.float32)
    for choice in range(slot_ref.shape[1]):
        pick = jnp.where(place == slot_ref[:, choice : choice + 1], 1.0, 0.0).astype(jnp.bfloat16)
        picked = jnp.dot(pick, rows, preferred_element_type=jnp.float32)
        total += weight_ref[:, choice : choice + 1] * picked
    out_ref[...] = (state_ref[...].astype(jnp.float32) + total).astype(out_ref.dtype)


def combine(state, slots, weights, returned):
    blocks, capacity, width = returned.shape
    return pl.pallas_call(
        combine_kernel,
        out_shape=jax.ShapeDtypeStruct(state.shape, jnp.bfloat16),
        scratch_shapes=[pltpu.VMEM((blocks * padded(capacity), width), jnp.float32)],
        compiler_params=vmem(12),
        name="combine",
    )(state, slots, weights, returned)


def route_weights(routes, group_logits, expert_scores, per_group):
    raised = jnp.exp(group_logits)
    group_prob = raised / jnp.sum(raised, axis=1, keepdims=True)
    owning_group = routes // per_group
    groups_iota = jnp.arange(group_logits.shape[1], dtype=jnp.int32)
    picked = jnp.sum(
        jnp.where(owning_group[:, :, None] == groups_iota[None, None, :], group_prob[:, None, :], 0.0),
        axis=2,
    )
    lifted = jnp.exp(expert_scores)
    return picked * lifted / jnp.sum(lifted, axis=1, keepdims=True)


def to_travel(values):
    wide = values.astype(jnp.float32)
    root = jnp.sqrt(jnp.abs(wide))
    return jnp.where(wide < 0, -root, root).astype(jnp.float16)


def from_travel(roots):
    wide = roots.astype(jnp.float32)
    return (wide * jnp.abs(wide)).astype(jnp.bfloat16)


def to_line(values):
    return from_travel(lax.all_gather(to_travel(values), LINE, axis=0, tiled=False))


def swap(values):
    return lax.ppermute(values, "core", [(0, 1), (1, 0)])


def gain_rows(gain):
    row = lax.broadcasted_iota(jnp.int32, (GAIN_ROWS, gain.shape[0]), 0)
    rows, rest = jnp.zeros(row.shape, jnp.float32), gain[None, :]
    for k in range(3):
        head = lax.reduce_precision(rest, 8, 7)
        rows = jnp.where(row == k, head, rows)
        rest = rest - head
    return rows.astype(jnp.bfloat16)


def per_device(
    pool_input,
    pool_gate,
    pool_mix,
    pool_scale,
    out_proj,
    residual,
    norm_gain,
    routes,
    group_logits,
    expert_scores,
    w_gate,
    w_up,
    w_down,
):
    channels, length = pool_input.shape
    blocks = lax.axis_size("sp")
    experts = blocks * w_gate.shape[0]
    capacity = 3 * routes.shape[1] * length // (2 * experts)
    scale, quarter = lax.axis_index("tg"), lax.axis_index(SCALE)
    own_first = (scale * lax.axis_size(SCALE) + quarter) * channels
    edge = lax.ppermute(
        pool_input[:, length - SPAN :], "sp", [(i, i + 1) for i in range(blocks - 1)]
    )
    slots = slot_table(routes.T, experts, padded(capacity))
    gains = gain_rows(norm_gain)
    pooled = pool(edge, pool_input)
    group = lax.all_gather(pooled, SCALE, axis=0, tiled=True)
    mix = lax.dynamic_slice(
        pool_mix, (scale, 0, quarter * channels), (1, pool_mix.shape[1], channels)
    )[0]
    mixed = lax.dot_general(mix, group, (((0,), (0,)), ((), ())), preferred_element_type=jnp.float32)
    own_scale = lax.dynamic_slice(pool_scale, (own_first,), (channels,))
    branch = (jax.nn.sigmoid(pool_gate.astype(jnp.float32)) * mixed * own_scale[:, None]).astype(jnp.bfloat16)
    branches = lax.all_gather(branch, TP, axis=0, tiled=True)
    product = lax.dot_general(
        branches, out_proj, (((0,), (0,)), ((), ())), preferred_element_type=jnp.float32
    )
    state = (residual.astype(jnp.float32) + product).astype(jnp.bfloat16)

    other_state = swap(state)
    sent = dispatch(state, other_state, slots, blocks, capacity)
    w_gate, w_up, w_down = w_gate[0], w_up[0], w_down[0]
    other_gate, other_up, other_down, other_gains = swap(w_gate), swap(w_up), swap(w_down), swap(gains)
    arrived = lax.all_to_all(sent, "sp", split_axis=0, concat_axis=0, tiled=True)
    everyone = to_line(compact(arrived, gains, other_gains))
    activated = hidden(everyone, w_gate, w_up, other_gate, other_up)
    own_result, other_result = down(to_line(activated), w_down, other_down)
    result = unfold(own_result, swap(other_result), blocks, capacity)
    returned = lax.all_to_all(result, "sp", split_axis=0, concat_axis=0, tiled=True)
    weights = route_weights(routes, group_logits, expert_scores, experts // group_logits.shape[1])
    return combine(state, slots.T, weights, returned)


def solution(mesh):
    fine = Mesh(mesh.devices.reshape(mesh.devices.shape[0], 4, -1, 2), ("sp", *TP))
    placed = (
        P(TP, "sp"),
        P(TP, "sp"),
        P(),
        P(),
        P(None, TP),
        P("sp", TP),
        P(TP),
        P("sp", None),
        P("sp", None),
        P("sp", None),
        P("sp", None, TP),
        P("sp", None, TP),
        P("sp", None, TP),
    )
    return jax.shard_map(
        per_device, mesh=fine, in_specs=placed, out_specs=P("sp", TP), check_vma=False
    )
```

time: 218 us -> 191 us (0.88)
  waiting for transfers between devices: 76.7 us -> 18.7 us
  blocking collectives: 72.5 us -> 94 us
  starting transfers between devices: 28.1 us -> 44.1 us
  between operations: 13.6 us -> 0.21 us
  other arithmetic: 0.97 us -> 9.83 us
  Pallas kernels: 19.6 us -> 14.1 us
  local copies, waits for them, and re-layouts: 3.33 us -> 6.23 us
    all_gather x2 -> x0, waiting for transfers between devices: 52 us -> none  [per_device(): lax.all_gather(piece, TP, axis=0, tiled=False)]
    ppermute x0 -> x6, starting transfers between devices: none -> 21.6 us  [swap(): return lax.ppermute(values, 'core', [(0, 1), (1, 0)])]
    all_gather x3, blocking collectives: 55.9 us -> 77.4 us  [the longest x2 67.7 us: to_line(): lax.all_gather(to_travel(values), LINE, axis=0, tiled=False)]
    all_to_all x1, waiting for transfers between devices: 12.1 us -> 4.02 us  [per_device(): lax.all_to_all(sent, 'sp', split_axis=0, concat_axis=0, tiled=True)]
    convert_element_type x0 -> x4, other arithmetic: none -> 7.47 us  [the longest x2 5.6 us: from_travel(): return (wide * jnp.abs(wide)).astype(jnp.bfloat16)]
    pallas_call x4 -> x5, Pallas kernels: 17.6 us -> 12.1 us  [the longest x1 5.39 us: hidden(): pl.pallas_call(hidden_kernel, out_shape=jax.ShapeDtypeStruct((rows, 2 * u...]
    all_to_all x1, starting transfers between devices: 9.91 us -> 5.09 us  [per_device(): lax.all_to_all(result, 'sp', split_axis=0, concat_axis=0, tiled=True)]
    unnamed x12 -> x16, local copies, waits for them, and re-layouts: 1.5 us -> 4.42 us
  transfers between devices with their start and end apart: 5 -> 9, of which waited for: 4 -> 4; matrix products, arithmetic and copies ran while one was open for 1% -> 6% of each run, Pallas kernels for 0% -> 3%
where the time goes in v5:
time: 191 us; the launch traced here: 190 us
  blocking collectives  94 us (49%)
  starting transfers between devices  44.1 us (23%)
  waiting for transfers between devices  18.7 us (10%)
  Pallas kernels  14.1 us (7%)
  other arithmetic  9.83 us (5%)
  local copies, waits for them, and re-layouts  6.23 us (3%)
  matrix products  2.46 us (1%)
    all_gather x2, blocking collectives, to_line(): lax.all_gather(to_travel(values), LINE, axis=0, tiled=False)  67.7 us
    ppermute x6, starting transfers between devices, swap(): return lax.ppermute(values, 'core', [(0, 1), (1, 0)])  21.6 us
    all_gather x1, blocking collectives, per_device(): branches = lax.all_gather(branch, TP, axis=0, tiled=True)  16.6 us
    all_to_all x1, starting transfers between devices, per_device(): lax.all_to_all(sent, 'sp', split_axis=0, concat_axis=0, tiled=True)  13.5 us
    all_to_all x1, waiting for transfers between devices, per_device(): lax.all_to_all(result, 'sp', split_axis=0, concat_axis=0, tiled=True)  12.4 us
    all_gather x1, blocking collectives, per_device(): group = lax.all_gather(pooled, SCALE, axis=0, tiled=True)  9.63 us
    convert_element_type x2, other arithmetic, from_travel(): return (wide * jnp.abs(wide)).astype(jnp.bfloat16)  5.6 us
    pallas_call x1, Pallas kernels, hidden(): pl.pallas_call(hidden_kernel, out_shape=jax.ShapeDtypeStruct((rows, 2 * u...  5.39 us
  transfers between devices with their start and end apart: 9, of which 4 were waited for; matrix products, arithmetic and copies ran while one was open for 6% of the time, Pallas kernels for 3%

profile of v5, /device:TPU:1, one launch (start us, length us, event | category | flops | bytes accessed | tf_op | source)
XLA Modules:
  0.0 189.7 jit_solution(16233628283572950134)
XLA Ops:
  0.0 0.8 slice.3
  0.8 3.9 %collective-permute-start = (bf16[64,128]{1,0:T(8,128)(2,1)S(1)}, bf16[64,128]{1,0:T(8,128)(2,1)S(1)}, u32[]{:S(2)}, u32[]{:S(2)}) collective-permute-start(bf16[64,128]{1,0:T(8,128)(2,1)S(1)} %slice.3), channel_id=1, source_target_pairs={{0,16},{16,32},{32,48},{48,64},{64,80},{80,96},{96,112},{112,128},... | collective-permute-start | bytes 49160 | tf_op jit(solution)/shard_map/ppermute | solution.py:400
  4.7 0.7 subtract_reduce-precision_fusion
  5.4 0.7 copy-done.3
  6.1 0.2 slots.1.refs_2_
  6.2 0.8 dynamic_slice.7
  7.0 0.8 copy-done.2
  7.8 0.4 pool.1
  8.2 9.6 %all_gather.18 = bf16[256,384]{1,0:T(8,128)(2,1)S(1)} all-gather(bf16[64,384]{1,0:T(8,128)(2,1)S(1)} %pool.1), channel_id=1, replica_groups=mesh['sp'=32,'tg'=4,'yl'=2,'core'=2] {'yl','core'}, dimensions={0}, use_global_device_ids=true | all-gather | bytes 245760 | tf_op jit(solution)/shard_map/all_gather | solution.py:406
  17.8 1.1 fusion.6
  18.9 16.6 %all_gather.19 = bf16[1024,384]{1,0:T(8,128)(2,1)S(1)} all-gather(bf16[64,384]{1,0:T(8,128)(2,1)S(1)} %fusion.6), channel_id=1, replica_groups=mesh['sp'=32,'tg'=4,'yl'=2,'core'=2] {'tg','yl','core'}, dimensions={0}, use_global_device_ids=true | all-gather | bytes 835584 | tf_op jit(solution)/shard_map/all_gather | solution.py:413
  35.5 1.4 fusion.4.refs_0_.state_ref
  36.9 2.1 %collective-permute-start.1 = (bf16[384,128]{1,0:T(8,128)(2,1)S(1)}, bf16[384,128]{1,0:T(8,128)(2,1)S(1)}, u32[]{:S(2)}, u32[]{:S(2)}) collective-permute-start(bf16[384,128]{1,0:T(8,128)(2,1)S(1)} %fusion.4.refs_0_.state_ref), channel_id=1, source_target_pairs={{0,1},{1,0},{2,3},{3,2},{4,5},{5,4},{6,7},{7,6},{8,9},{9,8},{10,11... | collective-permute-start | bytes 294920 | tf_op jit(solution)/shard_map/ppermute | solution.py:366
  39.0 1.1 collective-permute-done.1.refs_1_
  40.1 1.2 dispatch.1
  41.3 13.5 %all-to-all-start = ((bf16[32,18,256]{2,1,0:T(8,128)(2,1)}), bf16[32,18,256]{2,1,0:T(8,128)(2,1)S(1)}, u32[]{:S(2)}, u32[]{:S(2)}) async-start(bf16[32,18,256]{2,1,0:T(8,128)(2,1)} %dispatch.1), calls=%async_computation | async-start | bytes 786432 | tf_op jit(solution)/shard_map/all_to_all | solution.py:423
  54.8 0.1 select_convert_fusion.own_ref
  54.9 2.3 %collective-permute-start.2 = (bf16[16,128]{1,0:T(8,128)(2,1)S(1)}, bf16[16,128]{1,0:T(8,128)(2,1)S(1)}, u32[]{:S(2)}, u32[]{:S(2)}) collective-permute-start(bf16[16,128]{1,0:T(8,128)(2,1)S(1)} %select_convert_fusion.own_ref), channel_id=1, source_target_pairs={{0,1},{1,0},{2,3},{3,2},{4,5},{5,4},{6,7},{7,6},{8,9},{9,8},{10,11... | collective-permute-start | bytes 12296 | tf_op jit(solution)/shard_map/ppermute | solution.py:366
  57.2 2.0 %collective-permute-start.3 = (bf16[2048,256]{1,0:T(8,128)(2,1)}, bf16[2048,256]{1,0:T(8,128)(2,1)S(1)}, u32[]{:S(2)}, u32[]{:S(2)}) collective-permute-start(bf16[2048,256]{1,0:T(8,128)(2,1)} %bitcast.19), channel_id=1, source_target_pairs={{0,1},{1,0},{2,3},{3,2},{4,5},{5,4},{6,7},{7,6},{8,9},{9,8},{10,11... | collective-permute-start | bytes 3145736 | tf_op jit(solution)/shard_map/ppermute | solution.py:366
  59.2 2.4 %collective-permute-start.4 = (bf16[2048,256]{1,0:T(8,128)(2,1)}, bf16[2048,256]{1,0:T(8,128)(2,1)S(1)}, u32[]{:S(2)}, u32[]{:S(2)}) collective-permute-start(bf16[2048,256]{1,0:T(8,128)(2,1)} %bitcast.21), channel_id=1, source_target_pairs={{0,1},{1,0},{2,3},{3,2},{4,5},{5,4},{6,7},{7,6},{8,9},{9,8},{10,11... | collective-permute-start | bytes 3145736 | tf_op jit(solution)/shard_map/ppermute | solution.py:366
  61.6 2.0 %collective-permute-start.5 = (bf16[4096,128]{1,0:T(8,128)(2,1)}, bf16[4096,128]{1,0:T(8,128)(2,1)}, u32[]{:S(2)}, u32[]{:S(2)}) collective-permute-start(bf16[4096,128]{1,0:T(8,128)(2,1)} %bitcast.23), channel_id=1, source_target_pairs={{0,1},{1,0},{2,3},{3,2},{4,5},{5,4},{6,7},{7,6},{8,9},{9,8},{10,11... | collective-permute-start | bytes 3145736 | tf_op jit(solution)/shard_map/ppermute | solution.py:366
  63.6 0.7 exponential_reduce_fusion
  64.3 0.7 exponential_divide_fusion
  65.0 0.1 copy.24
  65.2 4.0 %all-to-all-done.arrived_ref = bf16[32,18,256]{2,1,0:T(8,128)(2,1)S(1)} async-done(((bf16[32,18,256]{2,1,0:T(8,128)(2,1)}), bf16[32,18,256]{2,1,0:T(8,128)(2,1)S(1)}, u32[]{:S(2)}, u32[]{:S(2)}) %all-to-all-start) | async-done | bytes 294944 | tf_op jit(solution)/shard_map/all_to_all | solution.py:423
  69.2 0.1 compact.1
  69.3 0.3 fusion.8
  69.5 25.9 %all-gather.4 = f16[4736,256]{1,0:T(8,128)(2,1)S(1)} all-gather(f16[592,256]{1,0:T(8,128)(2,1)S(1)} %fusion.8), channel_id=2, replica_groups=mesh['sp'=32,'tg'=4,'yl'=2,'core'=2] {'tg','yl'}, dimensions={0}, use_global_device_ids=true | all-gather | bytes 2727936 | tf_op jit(solution)/shard_map/all_gather | solution.py:362
  95.5 2.1 %fusion.1.x_hbm = bf16[8,592,256]{2,1,0:T(8,128)(2,1)} fusion(f16[8,592,256]{2,1,0:T(8,128)(2,1)S(1)} %bitcast.18), kind=kLoop, calls=%fused_computation.3 | loop fusion | flops 4849664 | bytes 4849664 | tf_op jit(solution)/shard_map/convert_element_type | solution.py:358
  97.6 0.0 collective-permute-done.3.gate2_hbm
  97.6 0.0 collective-permute-done.4.up2_hbm
  97.6 1.0 copy-done.5
  98.5 1.0 copy-done.6
  99.6 5.4 %hidden.1 = bf16[576,512]{1,0:T(8,128)(2,1)} custom-call(bf16[8,592,256]{2,1,0:T(8,128)(2,1)} %fusion.1.x_hbm, bf16[2048,256]{1,0:T(8,128)(2,1)} %bitcast.20, bf16[2048,256]{1,0:T(8,128)(2,1)} %bitcast.22, bf16[2048,256]{1,0:T(8,128)(2,1)} %copy-done.5, bf16[2048,256]{1,0:T(8,128)(2,1)} %copy-done.6), custom_call_target="tpu_custom_call" | custom-call | tf_op jit(solution)/shard_map/hidden/pallas_call | solution.py:219
  105.0 1.6 fusion.3
  106.6 41.8 %all-gather.5 = f16[4608,512]{1,0:T(8,128)(2,1)S(1)} all-gather(f16[576,512]{1,0:T(8,128)(2,1)S(1)} %fusion.3), channel_id=3, replica_groups=mesh['sp'=32,'tg'=4,'yl'=2,'core'=2] {'tg','yl'}, dimensions={0}, use_global_device_ids=true | all-gather | bytes 5308416 | tf_op jit(solution)/shard_map/all_gather | solution.py:362
  148.4 3.5 %fusion.u_hbm = bf16[8,576,512]{2,1,0:T(8,128)(2,1)} fusion(f16[8,576,512]{2,1,0:T(8,128)(2,1)S(1)} %bitcast.17), kind=kLoop, calls=%fused_computation.1 | loop fusion | flops 9437184 | bytes 9437184 | tf_op jit(solution)/shard_map/convert_element_type | solution.py:358
  151.9 0.0 collective-permute-done.5.other_hbm
  151.9 4.7 %down.1 = (bf16[576,128]{1,0:T(8,128)(2,1)}, bf16[576,128]{1,0:T(8,128)(2,1)}) custom-call(bf16[8,576,512]{2,1,0:T(8,128)(2,1)} %fusion.u_hbm, bf16[4096,128]{1,0:T(8,128)(2,1)} %bitcast.24, bf16[4096,128]{1,0:T(8,128)(2,1)} %collective-permute-done.5.other_hbm), custom_call_target="tpu_custom_call" | custom-call | tf_op jit(solution)/shard_map/down/pallas_call | solution.py:270
  156.6 10.9 %collective-permute-start.6 = (bf16[576,128]{1,0:T(8,128)(2,1)}, bf16[576,128]{1,0:T(8,128)(2,1)S(1)}, u32[]{:S(2)}, u32[]{:S(2)}) collective-permute-start(bf16[576,128]{1,0:T(8,128)(2,1)} %get-tuple-element.8), channel_id=1, source_target_pairs={{0,1},{1,0},{2,3},{3,2},{4,5},{5,4},{6,7},{7,6},{8,9},{9,8},{10,11... | collective-permute-start | bytes 442376 | tf_op jit(solution)/shard_map/ppermute | solution.py:366
  167.5 1.2 collective-permute-done.6.other_ref
  168.6 0.9 copy-done.1
  169.5 0.8 unfold.1
  170.4 5.1 %all-to-all-start.1 = ((bf16[32,36,128]{2,1,0:T(8,128)(2,1)}), bf16[32,36,128]{2,1,0:T(8,128)(2,1)S(1)}, u32[]{:S(2)}, u32[]{:S(2)}) async-start(bf16[32,36,128]{2,1,0:T(8,128)(2,1)} %unfold.1), calls=%async_computation.1 | async-start | bytes 655360 | tf_op jit(solution)/shard_map/all_to_all | solution.py:428
  175.5 0.1 copy.25
  175.7 0.1 broadcast_divide_fusion.weight_ref
  175.8 12.4 %all-to-all-done.1.returned_ref = bf16[32,36,128]{2,1,0:T(8,128)(2,1)S(1)} async-done(((bf16[32,36,128]{2,1,0:T(8,128)(2,1)}), bf16[32,36,128]{2,1,0:T(8,128)(2,1)S(1)}, u32[]{:S(2)}, u32[]{:S(2)}) %all-to-all-start.1) | async-done | bytes 294944 | tf_op jit(solution)/shard_map/all_to_all | solution.py:428
  188.2 1.4 combine.1
  (18 shorter events, 0.1 us)
Async XLA Ops:
  0.0 17.8 %copy-start = (bf16[4,256,256]{2,1,0:T(8,128)(2,1)S(1)}, bf16[4,256,256]{2,1,0:T(8,128)(2,1)}, u32[]{:S(2)}) copy-start(bf16[4,256,256]{2,1,0:T(8,128)(2,1)} %param.15) | copy-start | bytes 1572868
  0.8 6.2 %collective-permute-start = (bf16[64,128]{1,0:T(8,128)(2,1)S(1)}, bf16[64,128]{1,0:T(8,128)(2,1)S(1)}, u32[]{:S(2)}, u32[]{:S(2)}) collective-permute-start(bf16[64,128]{1,0:T(8,128)(2,1)S(1)} %slice.3), channel_id=1, source_target_pairs={{0,16},{16,32},{32,48},{48,64},{64,80},{80,96},{96,112},{112,128},... | collective-permute-start | bytes 49160 | tf_op jit(solution)/shard_map/ppermute | solution.py:400
  5.4 0.7 copy-start.3
  7.0 0.8 copy-start.2
  36.9 3.2 %collective-permute-start.1 = (bf16[384,128]{1,0:T(8,128)(2,1)S(1)}, bf16[384,128]{1,0:T(8,128)(2,1)S(1)}, u32[]{:S(2)}, u32[]{:S(2)}) collective-permute-start(bf16[384,128]{1,0:T(8,128)(2,1)S(1)} %fusion.4.refs_0_.state_ref), channel_id=1, source_target_pairs={{0,1},{1,0},{2,3},{3,2},{4,5},{5,4},{6,7},{7,6},{8,9},{9,8},{10,11... | collective-permute-start | bytes 294920 | tf_op jit(solution)/shard_map/ppermute | solution.py:366
  41.3 27.9 %all-to-all-start = ((bf16[32,18,256]{2,1,0:T(8,128)(2,1)}), bf16[32,18,256]{2,1,0:T(8,128)(2,1)S(1)}, u32[]{:S(2)}, u32[]{:S(2)}) async-start(bf16[32,18,256]{2,1,0:T(8,128)(2,1)} %dispatch.1), calls=%async_computation | async-start | bytes 786432 | tf_op jit(solution)/shard_map/all_to_all | solution.py:423
  54.9 10.2 %collective-permute-start.2 = (bf16[16,128]{1,0:T(8,128)(2,1)S(1)}, bf16[16,128]{1,0:T(8,128)(2,1)S(1)}, u32[]{:S(2)}, u32[]{:S(2)}) collective-permute-start(bf16[16,128]{1,0:T(8,128)(2,1)S(1)} %select_convert_fusion.own_ref), channel_id=1, source_target_pairs={{0,1},{1,0},{2,3},{3,2},{4,5},{5,4},{6,7},{7,6},{8,9},{9,8},{10,11... | collective-permute-start | bytes 12296 | tf_op jit(solution)/shard_map/ppermute | solution.py:366
  57.2 40.3 %collective-permute-start.3 = (bf16[2048,256]{1,0:T(8,128)(2,1)}, bf16[2048,256]{1,0:T(8,128)(2,1)S(1)}, u32[]{:S(2)}, u32[]{:S(2)}) collective-permute-start(bf16[2048,256]{1,0:T(8,128)(2,1)} %bitcast.19), channel_id=1, source_target_pairs={{0,1},{1,0},{2,3},{3,2},{4,5},{5,4},{6,7},{7,6},{8,9},{9,8},{10,11... | collective-permute-start | bytes 3145736 | tf_op jit(solution)/shard_map/ppermute | solution.py:366
  59.2 38.3 %collective-permute-start.4 = (bf16[2048,256]{1,0:T(8,128)(2,1)}, bf16[2048,256]{1,0:T(8,128)(2,1)S(1)}, u32[]{:S(2)}, u32[]{:S(2)}) collective-permute-start(bf16[2048,256]{1,0:T(8,128)(2,1)} %bitcast.21), channel_id=1, source_target_pairs={{0,1},{1,0},{2,3},{3,2},{4,5},{5,4},{6,7},{7,6},{8,9},{9,8},{10,11... | collective-permute-start | bytes 3145736 | tf_op jit(solution)/shard_map/ppermute | solution.py:366
  61.6 90.3 %collective-permute-start.5 = (bf16[4096,128]{1,0:T(8,128)(2,1)}, bf16[4096,128]{1,0:T(8,128)(2,1)}, u32[]{:S(2)}, u32[]{:S(2)}) collective-permute-start(bf16[4096,128]{1,0:T(8,128)(2,1)} %bitcast.23), channel_id=1, source_target_pairs={{0,1},{1,0},{2,3},{3,2},{4,5},{5,4},{6,7},{7,6},{8,9},{9,8},{10,11... | collective-permute-start | bytes 3145736 | tf_op jit(solution)/shard_map/ppermute | solution.py:366
  97.6 1.0 copy-start.5
  98.5 1.0 copy-start.6
  151.9 15.5 %copy-start.4 = (s32[384,2]{0,1:T(2,128)S(1)}, s32[384,2]{0,1:T(2,128)}, u32[]{:S(2)}) copy-start(s32[384,2]{0,1:T(2,128)} %param.20) | copy-start | bytes 9220
  151.9 23.6 %copy-start.7 = (f32[384,2]{0,1:T(2,128)S(1)}, f32[384,2]{0,1:T(2,128)}, u32[]{:S(2)}) copy-start(f32[384,2]{0,1:T(2,128)} %param.22) | copy-start | bytes 9220
  156.6 12.1 %collective-permute-start.6 = (bf16[576,128]{1,0:T(8,128)(2,1)}, bf16[576,128]{1,0:T(8,128)(2,1)S(1)}, u32[]{:S(2)}, u32[]{:S(2)}) collective-permute-start(bf16[576,128]{1,0:T(8,128)(2,1)} %get-tuple-element.8), channel_id=1, source_target_pairs={{0,1},{1,0},{2,3},{3,2},{4,5},{5,4},{6,7},{7,6},{8,9},{9,8},{10,11... | collective-permute-start | bytes 442376 | tf_op jit(solution)/shard_map/ppermute | solution.py:366
  168.6 0.9 copy-start.1
  170.4 17.9 %all-to-all-start.1 = ((bf16[32,36,128]{2,1,0:T(8,128)(2,1)}), bf16[32,36,128]{2,1,0:T(8,128)(2,1)S(1)}, u32[]{:S(2)}, u32[]{:S(2)}) async-start(bf16[32,36,128]{2,1,0:T(8,128)(2,1)} %unfold.1), calls=%async_computation.1 | async-start | bytes 655360 | tf_op jit(solution)/shard_map/all_to_all | solution.py:428

commit v6 on v5

--- a/solution.py
+++ b/solution.py
@@ -10,6 +10,8 @@
 TOGETHER = 2
 AHEAD = 2
 DOWN_AHEAD = 4
+HIDDEN_MIB = 20
+DOWN_MIB = 16
 ROWS = 288
 epsilon = 1e-06
 
@@ -26,7 +28,7 @@
     return -(-rows // 8) * 8
 
 
-def pool_kernel(edge_ref, own_ref, out_ref):
+def pool_kernel(edge_ref, own_ref, gain_ref, out_ref):
     length = own_ref.shape[1]
     scale = lax.axis_index("tg")
     first = lax.axis_index("sp") * length
@@ -42,16 +44,19 @@
     position = first + 1 + lax.broadcasted_iota(jnp.int32, own.shape, 1)
     counted = jnp.minimum(position, window).astype(jnp.float32)
     pooled = chosen[:, SPAN : SPAN + length] / counted - own
-    out_ref[...] = pooled.astype(out_ref.dtype)
-
-
-def pool(edge, own):
+    out_ref[:, :length] = pooled.astype(out_ref.dtype)
+    out_ref[:, length:] = jnp.zeros((own.shape[0], SPAN), out_ref.dtype)
+    out_ref[0:GAIN_ROWS, length:] = gain_ref[...]
+
+
+def pool(edge, own, gains):
+    channels, length = own.shape
     return pl.pallas_call(
         pool_kernel,
-        out_shape=jax.ShapeDtypeStruct(own.shape, jnp.bfloat16),
+        out_shape=jax.ShapeDtypeStruct((channels, length + SPAN), jnp.bfloat16),
         compiler_params=vmem(4),
         name="pool",
-    )(edge, own)
+    )(edge, own, gains)
 
 
 def slot_kernel(experts, pitch, routes_ref, out_ref):
@@ -152,31 +157,24 @@
         copy.start()
 
 
-def hidden_kernel(x_hbm, gate_hbm, up_hbm, gate2_hbm, up2_hbm, out_ref, x_ref, gate_ref, up_ref, squares_ref, gate_sum, up_sum, x_sems, w_sems):
+def hidden_kernel(x_ref, gate_ref, up_ref, gate2_hbm, up2_hbm, out_ref, gate2_ref, up2_ref, squares_ref, *refs):
+    sums, w_sems = refs[:4], refs[4]
     parts, rows, width = x_ref.shape
     rows -= GAIN_ROWS
-    units = gate_ref.shape[2]
+    units = gate_ref.shape[1]
     depth = TOGETHER * width
-    core = lax.axis_index("core")
+    chunks = parts // TOGETHER
     copies = []
-    for chunk in range(parts // TOGETHER):
+    for chunk in range(chunks):
         deep = pl.ds(chunk * depth, depth)
-        here = [
-            pltpu.make_async_copy(hbm.at[deep], ref.at[which, deep], w_sems.at[chunk, k])
-            for k, (hbm, ref, which) in enumerate(
-                (
-                    (gate_hbm, gate_ref, core),
-                    (up_hbm, up_ref, core),
-                    (gate2_hbm, gate_ref, 1 - core),
-                    (up2_hbm, up_ref, 1 - core),
-                )
-            )
-        ]
-        for part in range(chunk * TOGETHER, (chunk + 1) * TOGETHER):
-            here.append(pltpu.make_async_copy(x_hbm.at[part], x_ref.at[part], x_sems.at[part]))
-        copies.append(here)
+        copies.append(
+            [
+                pltpu.make_async_copy(hbm.at[deep], ref.at[deep], w_sems.at[chunk, k])
+                for k, (hbm, ref) in enumerate(((gate2_hbm, gate2_ref), (up2_hbm, up2_ref)))
+            ]
+        )
     begin_ahead(copies, AHEAD)
-    for chunk in range(len(copies)):
+    for chunk in range(chunks):
         turn_over(copies, chunk, AHEAD)
         mine = range(chunk * TOGETHER, (chunk + 1) * TOGETHER)
         deep = pl.ds(chunk * depth, depth)
@@ -196,45 +194,44 @@
                 squares_ref[here, :] = squares
             else:
                 squares_ref[here, :] += squares
-            for which in range(2):
-                there = pl.ds(which * units, units)
-                gate = jnp.dot(rows_in, gate_ref[which, deep, :], preferred_element_type=jnp.float32)
-                up = jnp.dot(rows_in, up_ref[which, deep, :], preferred_element_type=jnp.float32)
+            for total_ref, weight_ref in zip(sums, (gate_ref, up_ref, gate2_ref, up2_ref)):
+                product = jnp.dot(rows_in, weight_ref[deep, :], preferred_element_type=jnp.float32)
                 if chunk == 0:
-                    gate_sum[here, there], up_sum[here, there] = gate, up
+                    total_ref[here, :] = product
                 else:
-                    gate_sum[here, there] += gate
-                    up_sum[here, there] += up
+                    total_ref[here, :] += product
+    lower = lax.axis_index("core") == 0
     for first, count in tiles(rows, ROWS):
         here = pl.ds(first, count)
         mean = jnp.sum(squares_ref[here, :], axis=1, keepdims=True) / (parts * width)
         factor = lax.rsqrt(mean + epsilon)
-        gate, up = gate_sum[here, :] * factor, up_sum[here, :] * factor
-        out_ref[here, :] = (jax.nn.silu(gate) * up).astype(out_ref.dtype)
+        gate, up, gate2, up2 = [total_ref[here, :] * factor for total_ref in sums]
+        own, other = jax.nn.silu(gate) * up, jax.nn.silu(gate2) * up2
+        out_ref[here, :units] = jnp.where(lower, own, other).astype(out_ref.dtype)
+        out_ref[here, units:] = jnp.where(lower, other, own).astype(out_ref.dtype)
 
 
 def hidden(everyone, w_gate, w_up, other_gate, other_up):
     parts, extended, width = everyone.shape
     rows, units = extended - GAIN_ROWS, w_gate.shape[1]
+    hbm, near = pl.BlockSpec(memory_space=pltpu.HBM), pl.BlockSpec(memory_space=pltpu.VMEM)
     return pl.pallas_call(
         hidden_kernel,
         out_shape=jax.ShapeDtypeStruct((rows, 2 * units), jnp.bfloat16),
-        in_specs=[pl.BlockSpec(memory_space=pltpu.HBM)] * 5,
+        in_specs=[near, near, near, hbm, hbm],
         scratch_shapes=[
-            pltpu.VMEM(everyone.shape, everyone.dtype),
-            pltpu.VMEM((2, *w_gate.shape), w_gate.dtype),
-            pltpu.VMEM((2, *w_up.shape), w_up.dtype),
+            pltpu.VMEM(w_gate.shape, w_gate.dtype),
+            pltpu.VMEM(w_up.shape, w_up.dtype),
             pltpu.VMEM((rows, width), jnp.float32),
-            pltpu.VMEM((rows, 2 * units), jnp.float32),
-            pltpu.VMEM((rows, 2 * units), jnp.float32),
-            pltpu.SemaphoreType.DMA((parts,)),
-            pltpu.SemaphoreType.DMA((parts // TOGETHER, 4)),
+            *[pltpu.VMEM((rows, units), jnp.float32)] * 4,
+            pltpu.SemaphoreType.DMA((parts // TOGETHER, 2)),
         ],
+        compiler_params=vmem(HIDDEN_MIB),
         name="hidden",
     )(everyone, w_gate, w_up, other_gate, other_up)
 
 
-def down_kernel(u_hbm, own_hbm, other_hbm, own_out, other_out, u_ref, own_ref, other_ref, total_ref, u_sems, w_sems):
+def down_kernel(u_ref, own_hbm, other_hbm, own_out, other_out, own_ref, other_ref, total_ref, w_sems):
     parts, rows, units = u_ref.shape
     width = own_ref.shape[1]
     copies = []
@@ -244,7 +241,6 @@
             [
                 pltpu.make_async_copy(own_hbm.at[deep], own_ref.at[deep], w_sems.at[part, 0]),
                 pltpu.make_async_copy(other_hbm.at[deep], other_ref.at[deep], w_sems.at[part, 1]),
-                pltpu.make_async_copy(u_hbm.at[part], u_ref.at[part], u_sems.at[part]),
             ]
         )
     begin_ahead(copies, DOWN_AHEAD)
@@ -267,18 +263,18 @@
     parts, rows, units = everyone.shape
     width = own.shape[1]
     half = jax.ShapeDtypeStruct((rows, width), jnp.bfloat16)
+    hbm, near = pl.BlockSpec(memory_space=pltpu.HBM), pl.BlockSpec(memory_space=pltpu.VMEM)
     return pl.pallas_call(
         down_kernel,
         out_shape=[half, half],
-        in_specs=[pl.BlockSpec(memory_space=pltpu.HBM)] * 3,
+        in_specs=[near, hbm, hbm],
         scratch_shapes=[
-            pltpu.VMEM(everyone.shape, everyone.dtype),
             pltpu.VMEM(own.shape, own.dtype),
             pltpu.VMEM(other.shape, other.dtype),
             pltpu.VMEM((rows, 2 * width), jnp.float32),
-            pltpu.SemaphoreType.DMA((parts,)),
             pltpu.SemaphoreType.DMA((parts, 2)),
         ],
+        compiler_params=vmem(DOWN_MIB),
         name="down",
     )(everyone, own, other)
 
@@ -396,37 +392,53 @@
     experts = blocks * w_gate.shape[0]
     capacity = 3 * routes.shape[1] * length // (2 * experts)
     scale, quarter = lax.axis_index("tg"), lax.axis_index(SCALE)
+    core = lax.axis_index("core")
     own_first = (scale * lax.axis_size(SCALE) + quarter) * channels
     edge = lax.ppermute(
         pool_input[:, length - SPAN :], "sp", [(i, i + 1) for i in range(blocks - 1)]
     )
     slots = slot_table(routes.T, experts, padded(capacity))
     gains = gain_rows(norm_gain)
-    pooled = pool(edge, pool_input)
+    pooled = pool(edge, pool_input, gains)
     group = lax.all_gather(pooled, SCALE, axis=0, tiled=True)
     mix = lax.dynamic_slice(
         pool_mix, (scale, 0, quarter * channels), (1, pool_mix.shape[1], channels)
     )[0]
-    mixed = lax.dot_general(mix, group, (((0,), (0,)), ((), ())), preferred_element_type=jnp.float32)
+    mixed = lax.dot_general(mix, group[:, :length], (((0,), (0,)), ((), ())), preferred_element_type=jnp.float32)
+    other_gains = lax.dynamic_slice(group, ((quarter + 1 - 2 * core) * channels, length), (GAIN_ROWS, SPAN))
     own_scale = lax.dynamic_slice(pool_scale, (own_first,), (channels,))
     branch = (jax.nn.sigmoid(pool_gate.astype(jnp.float32)) * mixed * own_scale[:, None]).astype(jnp.bfloat16)
-    branches = lax.all_gather(branch, TP, axis=0, tiled=True)
-    product = lax.dot_general(
-        branches, out_proj, (((0,), (0,)), ((), ())), preferred_element_type=jnp.float32
+    branches = lax.all_gather(branch, LINE, axis=0, tiled=True)
+    proj = out_proj.reshape(lax.axis_size(LINE), 2, channels, -1)
+    own_proj, other_proj = lax.optimization_barrier(
+        tuple(lax.dynamic_index_in_dim(proj, which, 1, keepdims=False) for which in (core, 1 - core))
+    )
+    swapped, other_gains = lax.optimization_barrier((swap(branches), other_gains))
+    product = sum(
+        lax.dot_general(
+            rows,
+            columns.reshape(rows.shape[0], -1),
+            (((0,), (0,)), ((), ())),
+            preferred_element_type=jnp.float32,
+        )
+        for rows, columns in ((branches, own_proj), (swapped, other_proj))
     )
     state = (residual.astype(jnp.float32) + product).astype(jnp.bfloat16)
 
     other_state = swap(state)
     sent = dispatch(state, other_state, slots, blocks, capacity)
     w_gate, w_up, w_down = w_gate[0], w_up[0], w_down[0]
-    other_gate, other_up, other_down, other_gains = swap(w_gate), swap(w_up), swap(w_down), swap(gains)
+    other_gate, other_up, other_down = swap(w_gate), swap(w_up), swap(w_down)
     arrived = lax.all_to_all(sent, "sp", split_axis=0, concat_axis=0, tiled=True)
     everyone = to_line(compact(arrived, gains, other_gains))
     activated = hidden(everyone, w_gate, w_up, other_gate, other_up)
     own_result, other_result = down(to_line(activated), w_down, other_down)
     result = unfold(own_result, swap(other_result), blocks, capacity)
+    result, routes, group_logits, expert_scores = lax.optimization_barrier(
+        (result, routes, group_logits, expert_scores)
+    )
+    weights = route_weights(routes, group_logits, expert_scores, experts // group_logits.shape[1])
     returned = lax.all_to_all(result, "sp", split_axis=0, concat_axis=0, tiled=True)
-    weights = route_weights(routes, group_logits, expert_scores, experts // group_logits.shape[1])
     return combine(state, slots.T, weights, returned)
 
 

time: 191 us -> 192 us (level)
  other arithmetic: 9.83 us -> 3.78 us
  starting transfers between devices: 44.1 us -> 48.4 us
  blocking collectives: 94 us -> 97.3 us
  waiting for transfers between devices: 18.7 us -> 21.3 us
  Pallas kernels: 14.1 us -> 11.8 us
    ppermute x6, starting transfers between devices: 21.6 us -> 27.4 us  [swap(): return lax.ppermute(values, 'core', [(0, 1), (1, 0)])]
    all_to_all x1, waiting for transfers between devices: 4.02 us -> 7.65 us  [per_device(): lax.all_to_all(sent, 'sp', split_axis=0, concat_axis=0, tiled=True)]
    convert_element_type x2, other arithmetic: 5.6 us -> 1.99 us  [from_travel(): return (wide * jnp.abs(wide)).astype(jnp.bfloat16)]
    unnamed x16 -> x20, local copies, waits for them, and re-layouts: 4.42 us -> 1.52 us
    all_gather x1, blocking collectives: 16.6 us -> 18.9 us  [per_device(): branches = lax.all_gather(branch, LINE, axis=0, tiled=True)]
  transfers between devices with their start and end apart: 9 -> 9, of which waited for: 4 -> 4; matrix products, arithmetic and copies ran while one was open for 6% -> 4% of each run, Pallas kernels for 3% -> 2%
where the time goes in v6:
time: 192 us; the launch traced here: 191 us
  blocking collectives  97.3 us (51%)
  starting transfers between devices  48.4 us (25%)
  waiting for transfers between devices  21.3 us (11%)
  Pallas kernels  11.8 us (6%)
  local copies, waits for them, and re-layouts  5.11 us (3%)
  other arithmetic  3.78 us (2%)
  matrix products  2.71 us (1%)
    all_gather x2, blocking collectives, to_line(): lax.all_gather(to_travel(values), LINE, axis=0, tiled=False)  68.6 us
    ppermute x6, starting transfers between devices, swap(): return lax.ppermute(values, 'core', [(0, 1), (1, 0)])  27.4 us
    all_gather x1, blocking collectives, per_device(): branches = lax.all_gather(branch, LINE, axis=0, tiled=True)  18.9 us
    all_to_all x1, starting transfers between devices, per_device(): lax.all_to_all(sent, 'sp', split_axis=0, concat_axis=0, tiled=True)  12.8 us
    all_to_all x1, waiting for transfers between devices, per_device(): lax.all_to_all(result, 'sp', split_axis=0, concat_axis=0, tiled=True)  12.4 us
    all_gather x1, blocking collectives, per_device(): group = lax.all_gather(pooled, SCALE, axis=0, tiled=True)  9.8 us
    all_to_all x1, waiting for transfers between devices, per_device(): lax.all_to_all(sent, 'sp', split_axis=0, concat_axis=0, tiled=True)  7.65 us
    all_to_all x1, starting transfers between devices, per_device(): lax.all_to_all(result, 'sp', split_axis=0, concat_axis=0, tiled=True)  4.34 us
  transfers between devices with their start and end apart: 9, of which 4 were waited for; matrix products, arithmetic and copies ran while one was open for 4% of the time, Pallas kernels for 2%

profile of v6, /device:TPU:1, one launch (start us, length us, event | category | flops | bytes accessed | tf_op | source)
XLA Modules:
  0.0 190.8 jit_solution(13411820812223477166)
XLA Ops:
  0.0 0.9 slice.6
  0.9 3.9 %collective-permute-start = (bf16[64,128]{1,0:T(8,128)(2,1)S(1)}, bf16[64,128]{1,0:T(8,128)(2,1)S(1)}, u32[]{:S(2)}, u32[]{:S(2)}) collective-permute-start(bf16[64,128]{1,0:T(8,128)(2,1)S(1)} %slice.6), channel_id=1, source_target_pairs={{0,16},{16,32},{32,48},{48,64},{64,80},{80,96},{96,112},{112,128},... | collective-permute-start | bytes 49160 | tf_op jit(solution)/shard_map/ppermute | solution.py:397
  4.8 0.7 subtract_reduce-precision_fusion
  5.5 0.1 select_convert_fusion.gain_ref.own_ref
  5.6 0.8 dynamic_slice.17
  6.3 0.0 collective-permute-done.edge_ref
  6.3 0.8 copy-done.4
  7.1 0.4 pool.1
  7.5 9.8 %all_gather.18 = bf16[256,512]{1,0:T(8,128)(2,1)S(1)} all-gather(bf16[64,512]{1,0:T(8,128)(2,1)S(1)} %pool.1), channel_id=1, replica_groups=mesh['sp'=32,'tg'=4,'yl'=2,'core'=2] {'yl','core'}, dimensions={0}, use_global_device_ids=true | all-gather | bytes 327680 | tf_op jit(solution)/shard_map/all_gather | solution.py:403
  17.3 1.1 fusion.7
  18.4 18.9 %all_gather.19 = bf16[512,384]{1,0:T(8,128)(2,1)S(1)} all-gather(bf16[64,384]{1,0:T(8,128)(2,1)S(1)} %fusion.7), channel_id=1, replica_groups=mesh['sp'=32,'tg'=4,'yl'=2,'core'=2] {'tg','yl'}, dimensions={0}, use_global_device_ids=true | all-gather | bytes 442368 | tf_op jit(solution)/shard_map/all_gather | solution.py:411
  37.4 8.2 %collective-permute-start.1 = (bf16[512,384]{1,0:T(8,128)(2,1)S(1)}, bf16[512,384]{1,0:T(8,128)(2,1)}, u32[]{:S(2)}, u32[]{:S(2)}) collective-permute-start(bf16[512,384]{1,0:T(8,128)(2,1)S(1)} %all_gather.19), channel_id=1, source_target_pairs={{0,1},{1,0},{2,3},{3,2},{4,5},{5,4},{6,7},{7,6},{8,9},{9,8},{10,11... | collective-permute-start | bytes 1179656 | tf_op jit(solution)/shard_map/ppermute | solution.py:362
  45.5 1.0 dynamic-slice_bitcast_fusion
  46.5 0.7 constant_dynamic-slice_fusion.other_ref
  47.2 0.3 fusion.14
  47.5 1.3 fusion.5.refs_0_.state_ref
  48.9 1.9 %collective-permute-start.2 = (bf16[384,128]{1,0:T(8,128)(2,1)S(1)}, bf16[384,128]{1,0:T(8,128)(2,1)S(1)}, u32[]{:S(2)}, u32[]{:S(2)}) collective-permute-start(bf16[384,128]{1,0:T(8,128)(2,1)S(1)} %fusion.5.refs_0_.state_ref), channel_id=1, source_target_pairs={{0,1},{1,0},{2,3},{3,2},{4,5},{5,4},{6,7},{7,6},{8,9},{9,8},{10,11... | collective-permute-start | bytes 294920 | tf_op jit(solution)/shard_map/ppermute | solution.py:362
  50.8 0.0 copy-start.5
  50.8 0.7 copy-done.5
  51.5 0.2 slots.1.refs_2_
  51.7 0.4 collective-permute-done.2.refs_1_
  52.1 1.2 dispatch.1
  53.2 12.8 %all-to-all-start = ((bf16[32,18,256]{2,1,0:T(8,128)(2,1)}), bf16[32,18,256]{2,1,0:T(8,128)(2,1)S(1)}, u32[]{:S(2)}, u32[]{:S(2)}) async-start(bf16[32,18,256]{2,1,0:T(8,128)(2,1)} %dispatch.1), calls=%async_computation | async-start | bytes 786432 | tf_op jit(solution)/shard_map/all_to_all | solution.py:432
  66.0 2.3 %collective-permute-start.3 = (bf16[2048,256]{1,0:T(8,128)(2,1)S(1)}, bf16[2048,256]{1,0:T(8,128)(2,1)}, u32[]{:S(2)}, u32[]{:S(2)}) collective-permute-start(bf16[2048,256]{1,0:T(8,128)(2,1)S(1)} %bitcast.23), channel_id=1, source_target_pairs={{0,1},{1,0},{2,3},{3,2},{4,5},{5,4},{6,7},{7,6},{8,9},{9,8},{10,11... | collective-permute-start | bytes 3145736 | tf_op jit(solution)/shard_map/ppermute | solution.py:362
  68.4 2.0 %collective-permute-start.4 = (bf16[2048,256]{1,0:T(8,128)(2,1)S(1)}, bf16[2048,256]{1,0:T(8,128)(2,1)}, u32[]{:S(2)}, u32[]{:S(2)}) collective-permute-start(bf16[2048,256]{1,0:T(8,128)(2,1)S(1)} %bitcast.25), channel_id=1, source_target_pairs={{0,1},{1,0},{2,3},{3,2},{4,5},{5,4},{6,7},{7,6},{8,9},{9,8},{10,11... | collective-permute-start | bytes 3145736 | tf_op jit(solution)/shard_map/ppermute | solution.py:362
  70.4 2.3 %collective-permute-start.5 = (bf16[4096,128]{1,0:T(8,128)(2,1)}, bf16[4096,128]{1,0:T(8,128)(2,1)}, u32[]{:S(2)}, u32[]{:S(2)}) collective-permute-start(bf16[4096,128]{1,0:T(8,128)(2,1)} %bitcast.27), channel_id=1, source_target_pairs={{0,1},{1,0},{2,3},{3,2},{4,5},{5,4},{6,7},{7,6},{8,9},{9,8},{10,11... | collective-permute-start | bytes 3145736 | tf_op jit(solution)/shard_map/ppermute | solution.py:362
  72.7 7.6 %all-to-all-done.arrived_ref = bf16[32,18,256]{2,1,0:T(8,128)(2,1)S(1)} async-done(((bf16[32,18,256]{2,1,0:T(8,128)(2,1)}), bf16[32,18,256]{2,1,0:T(8,128)(2,1)S(1)}, u32[]{:S(2)}, u32[]{:S(2)}) %all-to-all-start) | async-done | bytes 294944 | tf_op jit(solution)/shard_map/all_to_all | solution.py:432
  80.4 0.1 compact.1
  80.4 0.3 fusion.9
  80.7 25.9 %all-gather.4 = f16[4736,256]{1,0:T(8,128)(2,1)S(1)} all-gather(f16[592,256]{1,0:T(8,128)(2,1)S(1)} %fusion.9), channel_id=2, replica_groups=mesh['sp'=32,'tg'=4,'yl'=2,'core'=2] {'tg','yl'}, dimensions={0}, use_global_device_ids=true | all-gather | bytes 2727936 | tf_op jit(solution)/shard_map/all_gather | solution.py:358
  106.7 0.7 fusion.1.x_ref
  107.4 4.1 %hidden.1 = bf16[576,512]{1,0:T(8,128)(2,1)S(1)} custom-call(bf16[8,592,256]{2,1,0:T(8,128)(2,1)S(1)} %fusion.1.x_ref, bf16[2048,256]{1,0:T(8,128)(2,1)S(1)} %bitcast.24, bf16[2048,256]{1,0:T(8,128)(2,1)S(1)} %bitcast.26, bf16[2048,256]{1,0:T(8,128)(2,1)} %collective-permute-done.3.gate2_hbm, bf16[2048,256]{1,0:T(8,128)(2,1)} %collective-permute-done.4.up2_hbm), custom_call_target="tpu_custom_call" | custom-call | tf_op jit(solution)/shard_map/hidden/pallas_call | solution.py:218
  111.5 0.5 fusion.3
  112.0 42.6 %all-gather.5 = f16[4608,512]{1,0:T(8,128)(2,1)S(1)} all-gather(f16[576,512]{1,0:T(8,128)(2,1)S(1)} %fusion.3), channel_id=3, replica_groups=mesh['sp'=32,'tg'=4,'yl'=2,'core'=2] {'tg','yl'}, dimensions={0}, use_global_device_ids=true | all-gather | bytes 5308416 | tf_op jit(solution)/shard_map/all_gather | solution.py:358
  154.7 1.3 fusion.u_ref
  156.0 0.0 copy-start.8
  156.0 0.0 copy-start.6
  156.0 0.0 copy-start.9
  156.1 3.7 %down.1 = (bf16[576,128]{1,0:T(8,128)(2,1)S(1)}, bf16[576,128]{1,0:T(8,128)(2,1)S(1)}) custom-call(bf16[8,576,512]{2,1,0:T(8,128)(2,1)S(1)} %fusion.u_ref, bf16[4096,128]{1,0:T(8,128)(2,1)S(1)} %bitcast.28, bf16[4096,128]{1,0:T(8,128)(2,1)} %collective-permute-done.5.other_hbm), custom_call_target="tpu_custom_call" | custom-call | tf_op jit(solution)/shard_map/down/pallas_call | solution.py:267
  159.7 10.6 %collective-permute-start.6 = (bf16[576,128]{1,0:T(8,128)(2,1)S(1)}, bf16[576,128]{1,0:T(8,128)(2,1)S(1)}, u32[]{:S(2)}, u32[]{:S(2)}) collective-permute-start(bf16[576,128]{1,0:T(8,128)(2,1)S(1)} %get-tuple-element.20), channel_id=1, source_target_pairs={{0,1},{1,0},{2,3},{3,2},{4,5},{5,4},{6,7},{7,6},{8,9},{9,8},{10,11... | collective-permute-start | bytes 442376 | tf_op jit(solution)/shard_map/ppermute | solution.py:362
  170.4 0.1 copy.24
  170.5 0.8 collective-permute-done.6.other_ref
  171.4 0.8 unfold.1
  172.3 4.3 %all-to-all-start.1 = ((bf16[32,36,128]{2,1,0:T(8,128)(2,1)}), bf16[32,36,128]{2,1,0:T(8,128)(2,1)S(1)}, u32[]{:S(2)}, u32[]{:S(2)}) async-start(bf16[32,36,128]{2,1,0:T(8,128)(2,1)} %unfold.1), calls=%async_computation.1 | async-start | bytes 655360 | tf_op jit(solution)/shard_map/all_to_all | solution.py:441
  176.7 0.1 copy.25
  176.8 0.1 broadcast_divide_fusion.weight_ref
  177.0 12.4 %all-to-all-done.1.returned_ref = bf16[32,36,128]{2,1,0:T(8,128)(2,1)S(1)} async-done(((bf16[32,36,128]{2,1,0:T(8,128)(2,1)}), bf16[32,36,128]{2,1,0:T(8,128)(2,1)S(1)}, u32[]{:S(2)}, u32[]{:S(2)}) %all-to-all-start.1) | async-done | bytes 294944 | tf_op jit(solution)/shard_map/all_to_all | solution.py:441
  189.4 1.4 combine.1
  (25 shorter events, 0.1 us)
Async XLA Ops:
  0.0 17.3 %copy-start = (bf16[4,256,256]{2,1,0:T(8,128)(2,1)S(1)}, bf16[4,256,256]{2,1,0:T(8,128)(2,1)}, u32[]{:S(2)}) copy-start(bf16[4,256,256]{2,1,0:T(8,128)(2,1)} %param.15) | copy-start | bytes 1572868
  0.0 66.0 %copy-start.1 = (bf16[1,2048,256]{2,1,0:T(8,128)(2,1)S(1)}, bf16[1,2048,256]{2,1,0:T(8,128)(2,1)}, u32[]{:S(2)}) copy-start(bf16[1,2048,256]{2,1,0:T(8,128)(2,1)} %param.23) | copy-start | bytes 3145732
  0.0 68.4 %copy-start.2 = (bf16[1,2048,256]{2,1,0:T(8,128)(2,1)S(1)}, bf16[1,2048,256]{2,1,0:T(8,128)(2,1)}, u32[]{:S(2)}) copy-start(bf16[1,2048,256]{2,1,0:T(8,128)(2,1)} %param.24) | copy-start | bytes 3145732
  0.9 5.5 %collective-permute-start = (bf16[64,128]{1,0:T(8,128)(2,1)S(1)}, bf16[64,128]{1,0:T(8,128)(2,1)S(1)}, u32[]{:S(2)}, u32[]{:S(2)}) collective-permute-start(bf16[64,128]{1,0:T(8,128)(2,1)S(1)} %slice.6), channel_id=1, source_target_pairs={{0,16},{16,32},{32,48},{48,64},{64,80},{80,96},{96,112},{112,128},... | collective-permute-start | bytes 49160 | tf_op jit(solution)/shard_map/ppermute | solution.py:397
  6.3 0.8 copy-start.4
  17.3 28.2 %copy-start.7 = (bf16[256,512]{1,0:T(8,128)(2,1)}, bf16[256,512]{1,0:T(8,128)(2,1)S(1)}, u32[]{:S(2)}) copy-start(bf16[256,512]{1,0:T(8,128)(2,1)S(1)} %all_gather.18) | copy-start | bytes 786436
  37.4 10.2 %collective-permute-start.1 = (bf16[512,384]{1,0:T(8,128)(2,1)S(1)}, bf16[512,384]{1,0:T(8,128)(2,1)}, u32[]{:S(2)}, u32[]{:S(2)}) collective-permute-start(bf16[512,384]{1,0:T(8,128)(2,1)S(1)} %all_gather.19), channel_id=1, source_target_pairs={{0,1},{1,0},{2,3},{3,2},{4,5},{5,4},{6,7},{7,6},{8,9},{9,8},{10,11... | collective-permute-start | bytes 1179656 | tf_op jit(solution)/shard_map/ppermute | solution.py:362
  48.9 3.2 %collective-permute-start.2 = (bf16[384,128]{1,0:T(8,128)(2,1)S(1)}, bf16[384,128]{1,0:T(8,128)(2,1)S(1)}, u32[]{:S(2)}, u32[]{:S(2)}) collective-permute-start(bf16[384,128]{1,0:T(8,128)(2,1)S(1)} %fusion.5.refs_0_.state_ref), channel_id=1, source_target_pairs={{0,1},{1,0},{2,3},{3,2},{4,5},{5,4},{6,7},{7,6},{8,9},{9,8},{10,11... | collective-permute-start | bytes 294920 | tf_op jit(solution)/shard_map/ppermute | solution.py:362
  50.8 0.7 copy-start.5
  53.2 27.1 %all-to-all-start = ((bf16[32,18,256]{2,1,0:T(8,128)(2,1)}), bf16[32,18,256]{2,1,0:T(8,128)(2,1)S(1)}, u32[]{:S(2)}, u32[]{:S(2)}) async-start(bf16[32,18,256]{2,1,0:T(8,128)(2,1)} %dispatch.1), calls=%async_computation | async-start | bytes 786432 | tf_op jit(solution)/shard_map/all_to_all | solution.py:432
  66.0 41.3 %collective-permute-start.3 = (bf16[2048,256]{1,0:T(8,128)(2,1)S(1)}, bf16[2048,256]{1,0:T(8,128)(2,1)}, u32[]{:S(2)}, u32[]{:S(2)}) collective-permute-start(bf16[2048,256]{1,0:T(8,128)(2,1)S(1)} %bitcast.23), channel_id=1, source_target_pairs={{0,1},{1,0},{2,3},{3,2},{4,5},{5,4},{6,7},{7,6},{8,9},{9,8},{10,11... | collective-permute-start | bytes 3145736 | tf_op jit(solution)/shard_map/ppermute | solution.py:362
  68.4 39.0 %collective-permute-start.4 = (bf16[2048,256]{1,0:T(8,128)(2,1)S(1)}, bf16[2048,256]{1,0:T(8,128)(2,1)}, u32[]{:S(2)}, u32[]{:S(2)}) collective-permute-start(bf16[2048,256]{1,0:T(8,128)(2,1)S(1)} %bitcast.25), channel_id=1, source_target_pairs={{0,1},{1,0},{2,3},{3,2},{4,5},{5,4},{6,7},{7,6},{8,9},{9,8},{10,11... | collective-permute-start | bytes 3145736 | tf_op jit(solution)/shard_map/ppermute | solution.py:362
  70.4 85.7 %collective-permute-start.5 = (bf16[4096,128]{1,0:T(8,128)(2,1)}, bf16[4096,128]{1,0:T(8,128)(2,1)}, u32[]{:S(2)}, u32[]{:S(2)}) collective-permute-start(bf16[4096,128]{1,0:T(8,128)(2,1)} %bitcast.27), channel_id=1, source_target_pairs={{0,1},{1,0},{2,3},{3,2},{4,5},{5,4},{6,7},{7,6},{8,9},{9,8},{10,11... | collective-permute-start | bytes 3145736 | tf_op jit(solution)/shard_map/ppermute | solution.py:362
  154.7 1.4 copy-start.3
  156.0 16.2 %copy-start.8 = (f32[384,4]{0,1:T(4,128)S(1)}, f32[384,4]{0,1:T(4,128)}, u32[]{:S(2)}) copy-start(f32[384,4]{0,1:T(4,128)} %param.21) | copy-start | bytes 18436
  156.0 16.2 %copy-start.6 = (s32[384,2]{0,1:T(2,128)S(1)}, s32[384,2]{0,1:T(2,128)}, u32[]{:S(2)}) copy-start(s32[384,2]{0,1:T(2,128)} %param.20) | copy-start | bytes 9220
  156.0 20.6 %copy-start.9 = (f32[384,2]{0,1:T(2,128)S(1)}, f32[384,2]{0,1:T(2,128)}, u32[]{:S(2)}) copy-start(f32[384,2]{0,1:T(2,128)} %param.22) | copy-start | bytes 9220
  159.7 11.6 %collective-permute-start.6 = (bf16[576,128]{1,0:T(8,128)(2,1)S(1)}, bf16[576,128]{1,0:T(8,128)(2,1)S(1)}, u32[]{:S(2)}, u32[]{:S(2)}) collective-permute-start(bf16[576,128]{1,0:T(8,128)(2,1)S(1)} %get-tuple-element.20), channel_id=1, source_target_pairs={{0,1},{1,0},{2,3},{3,2},{4,5},{5,4},{6,7},{7,6},{8,9},{9,8},{10,11... | collective-permute-start | bytes 442376 | tf_op jit(solution)/shard_map/ppermute | solution.py:362
  172.3 17.1 %all-to-all-start.1 = ((bf16[32,36,128]{2,1,0:T(8,128)(2,1)}), bf16[32,36,128]{2,1,0:T(8,128)(2,1)S(1)}, u32[]{:S(2)}, u32[]{:S(2)}) async-start(bf16[32,36,128]{2,1,0:T(8,128)(2,1)} %unfold.1), calls=%async_computation.1 | async-start | bytes 655360 | tf_op jit(solution)/shard_map/all_to_all | solution.py:441

commit v7 on v6

--- a/solution.py
+++ b/solution.py
@@ -408,24 +408,13 @@
     other_gains = lax.dynamic_slice(group, ((quarter + 1 - 2 * core) * channels, length), (GAIN_ROWS, SPAN))
     own_scale = lax.dynamic_slice(pool_scale, (own_first,), (channels,))
     branch = (jax.nn.sigmoid(pool_gate.astype(jnp.float32)) * mixed * own_scale[:, None]).astype(jnp.bfloat16)
-    branches = lax.all_gather(branch, LINE, axis=0, tiled=True)
-    proj = out_proj.reshape(lax.axis_size(LINE), 2, channels, -1)
-    own_proj, other_proj = lax.optimization_barrier(
-        tuple(lax.dynamic_index_in_dim(proj, which, 1, keepdims=False) for which in (core, 1 - core))
-    )
-    swapped, other_gains = lax.optimization_barrier((swap(branches), other_gains))
-    product = sum(
-        lax.dot_general(
-            rows,
-            columns.reshape(rows.shape[0], -1),
-            (((0,), (0,)), ((), ())),
-            preferred_element_type=jnp.float32,
-        )
-        for rows, columns in ((branches, own_proj), (swapped, other_proj))
+    branches = lax.all_gather(branch, TP, axis=0, tiled=True)
+    product = lax.dot_general(
+        branches, out_proj, (((0,), (0,)), ((), ())), preferred_element_type=jnp.float32
     )
     state = (residual.astype(jnp.float32) + product).astype(jnp.bfloat16)
 
-    other_state = swap(state)
+    other_state, other_gains = lax.optimization_barrier((swap(state), other_gains))
     sent = dispatch(state, other_state, slots, blocks, capacity)
     w_gate, w_up, w_down = w_gate[0], w_up[0], w_down[0]
     other_gate, other_up, other_down = swap(w_gate), swap(w_up), swap(w_down)

time: 192 us -> 180 us (0.938)
  starting transfers between devices: 48.4 us -> 41.2 us
  blocking collectives: 97.3 us -> 94.3 us
    ppermute x6 -> x5, starting transfers between devices: 27.4 us -> 19.6 us  [swap(): return lax.ppermute(values, 'core', [(0, 1), (1, 0)])]
    all_gather x1, blocking collectives: 18.9 us -> 16.8 us  [per_device(): branches = lax.all_gather(branch, TP, axis=0, tiled=True)]
  transfers between devices with their start and end apart: 9 -> 8, of which waited for: 4 -> 4; matrix products, arithmetic and copies ran while one was open for 4% -> 3% of each run, Pallas kernels for 2% -> 2%
where the time goes in v7:
time: 180 us; the launch traced here: 179 us
  blocking collectives  94.3 us (52%)
  starting transfers between devices  41.2 us (23%)
  waiting for transfers between devices  22 us (12%)
  Pallas kernels  11.8 us (7%)
  other arithmetic  3.82 us (2%)
  local copies, waits for them, and re-layouts  3.44 us (2%)
  matrix products  2.46 us (1%)
    all_gather x2, blocking collectives, to_line(): lax.all_gather(to_travel(values), LINE, axis=0, tiled=False)  67.7 us
    ppermute x5, starting transfers between devices, swap(): return lax.ppermute(values, 'core', [(0, 1), (1, 0)])  19.6 us
    all_gather x1, blocking collectives, per_device(): branches = lax.all_gather(branch, TP, axis=0, tiled=True)  16.8 us
    all_to_all x1, starting transfers between devices, per_device(): lax.all_to_all(sent, 'sp', split_axis=0, concat_axis=0, tiled=True)  13.3 us
    all_to_all x1, waiting for transfers between devices, per_device(): lax.all_to_all(result, 'sp', split_axis=0, concat_axis=0, tiled=True)  12.4 us
    all_gather x1, blocking collectives, per_device(): group = lax.all_gather(pooled, SCALE, axis=0, tiled=True)  9.8 us
    all_to_all x1, waiting for transfers between devices, per_device(): lax.all_to_all(sent, 'sp', split_axis=0, concat_axis=0, tiled=True)  7.64 us
    all_to_all x1, starting transfers between devices, per_device(): lax.all_to_all(result, 'sp', split_axis=0, concat_axis=0, tiled=True)  4.41 us
  transfers between devices with their start and end apart: 8, of which 4 were waited for; matrix products, arithmetic and copies ran while one was open for 3% of the time, Pallas kernels for 2%

profile of v7, /device:TPU:1, one launch (start us, length us, event | category | flops | bytes accessed | tf_op | source)
XLA Modules:
  0.0 179.4 jit_solution(14545125927752475075)
XLA Ops:
  0.0 0.0 copy-start
  0.0 0.9 slice.6
  0.9 3.9 %collective-permute-start = (bf16[64,128]{1,0:T(8,128)(2,1)S(1)}, bf16[64,128]{1,0:T(8,128)(2,1)S(1)}, u32[]{:S(2)}, u32[]{:S(2)}) collective-permute-start(bf16[64,128]{1,0:T(8,128)(2,1)S(1)} %slice.6), channel_id=1, source_target_pairs={{0,16},{16,32},{32,48},{48,64},{64,80},{80,96},{96,112},{112,128},... | collective-permute-start | bytes 49160 | tf_op jit(solution)/shard_map/ppermute | solution.py:397
  4.8 0.7 subtract_reduce-precision_fusion
  5.5 0.1 select_convert_fusion.gain_ref.own_ref
  5.6 0.7 copy-done.5
  6.3 0.2 slots.1.refs_2_
  6.4 0.8 dynamic_slice.10
  7.2 0.0 collective-permute-done.edge_ref
  7.2 0.8 copy-done.4
  8.0 0.4 pool.1
  8.4 9.8 %all_gather.18 = bf16[256,512]{1,0:T(8,128)(2,1)S(1)} all-gather(bf16[64,512]{1,0:T(8,128)(2,1)S(1)} %pool.1), channel_id=1, replica_groups=mesh['sp'=32,'tg'=4,'yl'=2,'core'=2] {'yl','core'}, dimensions={0}, use_global_device_ids=true | all-gather | bytes 327680 | tf_op jit(solution)/shard_map/all_gather | solution.py:403
  18.2 1.1 fusion.6
  19.3 16.8 %all_gather.19 = bf16[1024,384]{1,0:T(8,128)(2,1)S(1)} all-gather(bf16[64,384]{1,0:T(8,128)(2,1)S(1)} %fusion.6), channel_id=1, replica_groups=mesh['sp'=32,'tg'=4,'yl'=2,'core'=2] {'tg','yl','core'}, dimensions={0}, use_global_device_ids=true | all-gather | bytes 835584 | tf_op jit(solution)/shard_map/all_gather | solution.py:411
  36.1 1.4 fusion.4.refs_0_.state_ref
  37.4 2.1 %collective-permute-start.1 = (bf16[384,128]{1,0:T(8,128)(2,1)S(1)}, bf16[384,128]{1,0:T(8,128)(2,1)S(1)}, u32[]{:S(2)}, u32[]{:S(2)}) collective-permute-start(bf16[384,128]{1,0:T(8,128)(2,1)S(1)} %fusion.4.refs_0_.state_ref), channel_id=1, source_target_pairs={{0,1},{1,0},{2,3},{3,2},{4,5},{5,4},{6,7},{7,6},{8,9},{9,8},{10,11... | collective-permute-start | bytes 294920 | tf_op jit(solution)/shard_map/ppermute | solution.py:362
  39.5 1.1 collective-permute-done.1.refs_1_
  40.6 1.2 dispatch.1
  41.8 13.3 %all-to-all-start = ((bf16[32,18,256]{2,1,0:T(8,128)(2,1)}), bf16[32,18,256]{2,1,0:T(8,128)(2,1)S(1)}, u32[]{:S(2)}, u32[]{:S(2)}) async-start(bf16[32,18,256]{2,1,0:T(8,128)(2,1)} %dispatch.1), calls=%async_computation | async-start | bytes 786432 | tf_op jit(solution)/shard_map/all_to_all | solution.py:421
  55.1 2.3 %collective-permute-start.2 = (bf16[2048,256]{1,0:T(8,128)(2,1)S(1)}, bf16[2048,256]{1,0:T(8,128)(2,1)}, u32[]{:S(2)}, u32[]{:S(2)}) collective-permute-start(bf16[2048,256]{1,0:T(8,128)(2,1)S(1)} %bitcast.14), channel_id=1, source_target_pairs={{0,1},{1,0},{2,3},{3,2},{4,5},{5,4},{6,7},{7,6},{8,9},{9,8},{10,11... | collective-permute-start | bytes 3145736 | tf_op jit(solution)/shard_map/ppermute | solution.py:362
  57.5 2.0 %collective-permute-start.3 = (bf16[2048,256]{1,0:T(8,128)(2,1)S(1)}, bf16[2048,256]{1,0:T(8,128)(2,1)}, u32[]{:S(2)}, u32[]{:S(2)}) collective-permute-start(bf16[2048,256]{1,0:T(8,128)(2,1)S(1)} %bitcast.16), channel_id=1, source_target_pairs={{0,1},{1,0},{2,3},{3,2},{4,5},{5,4},{6,7},{7,6},{8,9},{9,8},{10,11... | collective-permute-start | bytes 3145736 | tf_op jit(solution)/shard_map/ppermute | solution.py:362
  59.4 2.4 %collective-permute-start.4 = (bf16[4096,128]{1,0:T(8,128)(2,1)}, bf16[4096,128]{1,0:T(8,128)(2,1)}, u32[]{:S(2)}, u32[]{:S(2)}) collective-permute-start(bf16[4096,128]{1,0:T(8,128)(2,1)} %bitcast.18), channel_id=1, source_target_pairs={{0,1},{1,0},{2,3},{3,2},{4,5},{5,4},{6,7},{7,6},{8,9},{9,8},{10,11... | collective-permute-start | bytes 3145736 | tf_op jit(solution)/shard_map/ppermute | solution.py:362
  61.8 7.6 %all-to-all-done.arrived_ref = bf16[32,18,256]{2,1,0:T(8,128)(2,1)S(1)} async-done(((bf16[32,18,256]{2,1,0:T(8,128)(2,1)}), bf16[32,18,256]{2,1,0:T(8,128)(2,1)S(1)}, u32[]{:S(2)}, u32[]{:S(2)}) %all-to-all-start) | async-done | bytes 294944 | tf_op jit(solution)/shard_map/all_to_all | solution.py:421
  69.5 0.1 compact.1
  69.5 0.3 fusion.8
  69.8 25.9 %all-gather.4 = f16[4736,256]{1,0:T(8,128)(2,1)S(1)} all-gather(f16[592,256]{1,0:T(8,128)(2,1)S(1)} %fusion.8), channel_id=2, replica_groups=mesh['sp'=32,'tg'=4,'yl'=2,'core'=2] {'tg','yl'}, dimensions={0}, use_global_device_ids=true | all-gather | bytes 2727936 | tf_op jit(solution)/shard_map/all_gather | solution.py:358
  95.7 0.7 fusion.1.x_ref
  96.4 0.0 collective-permute-done.2.gate2_hbm
  96.5 0.0 collective-permute-done.3.up2_hbm
  96.5 4.1 %hidden.1 = bf16[576,512]{1,0:T(8,128)(2,1)S(1)} custom-call(bf16[8,592,256]{2,1,0:T(8,128)(2,1)S(1)} %fusion.1.x_ref, bf16[2048,256]{1,0:T(8,128)(2,1)S(1)} %bitcast.15, bf16[2048,256]{1,0:T(8,128)(2,1)S(1)} %bitcast.17, bf16[2048,256]{1,0:T(8,128)(2,1)} %collective-permute-done.2.gate2_hbm, bf16[2048,256]{1,0:T(8,128)(2,1)} %collective-permute-done.3.up2_hbm), custom_call_target="tpu_custom_call" | custom-call | tf_op jit(solution)/shard_map/hidden/pallas_call | solution.py:218
  100.6 0.5 fusion.3
  101.1 41.8 %all-gather.5 = f16[4608,512]{1,0:T(8,128)(2,1)S(1)} all-gather(f16[576,512]{1,0:T(8,128)(2,1)S(1)} %fusion.3), channel_id=3, replica_groups=mesh['sp'=32,'tg'=4,'yl'=2,'core'=2] {'tg','yl'}, dimensions={0}, use_global_device_ids=true | all-gather | bytes 5308416 | tf_op jit(solution)/shard_map/all_gather | solution.py:358
  142.9 1.3 fusion.u_ref
  144.3 0.0 copy-start.7
  144.3 0.0 copy-start.6
  144.3 0.0 copy-start.8
  144.3 0.0 collective-permute-done.4.other_hbm
  144.3 3.7 %down.1 = (bf16[576,128]{1,0:T(8,128)(2,1)S(1)}, bf16[576,128]{1,0:T(8,128)(2,1)S(1)}) custom-call(bf16[8,576,512]{2,1,0:T(8,128)(2,1)S(1)} %fusion.u_ref, bf16[4096,128]{1,0:T(8,128)(2,1)S(1)} %bitcast.19, bf16[4096,128]{1,0:T(8,128)(2,1)} %collective-permute-done.4.other_hbm), custom_call_target="tpu_custom_call" | custom-call | tf_op jit(solution)/shard_map/down/pallas_call | solution.py:267
  148.0 10.8 %collective-permute-start.5 = (bf16[576,128]{1,0:T(8,128)(2,1)S(1)}, bf16[576,128]{1,0:T(8,128)(2,1)S(1)}, u32[]{:S(2)}, u32[]{:S(2)}) collective-permute-start(bf16[576,128]{1,0:T(8,128)(2,1)S(1)} %get-tuple-element.16), channel_id=1, source_target_pairs={{0,1},{1,0},{2,3},{3,2},{4,5},{5,4},{6,7},{7,6},{8,9},{9,8},{10,11... | collective-permute-start | bytes 442376 | tf_op jit(solution)/shard_map/ppermute | solution.py:362
  158.9 0.1 copy.24
  159.0 0.8 collective-permute-done.5.other_ref
  159.9 0.8 unfold.1
  160.8 4.4 %all-to-all-start.1 = ((bf16[32,36,128]{2,1,0:T(8,128)(2,1)}), bf16[32,36,128]{2,1,0:T(8,128)(2,1)S(1)}, u32[]{:S(2)}, u32[]{:S(2)}) async-start(bf16[32,36,128]{2,1,0:T(8,128)(2,1)} %unfold.1), calls=%async_computation.1 | async-start | bytes 655360 | tf_op jit(solution)/shard_map/all_to_all | solution.py:430
  165.2 0.0 copy-done.8
  165.2 0.1 copy.25
  165.4 0.1 broadcast_divide_fusion.weight_ref
  165.5 12.4 %all-to-all-done.1.returned_ref = bf16[32,36,128]{2,1,0:T(8,128)(2,1)S(1)} async-done(((bf16[32,36,128]{2,1,0:T(8,128)(2,1)}), bf16[32,36,128]{2,1,0:T(8,128)(2,1)S(1)}, u32[]{:S(2)}, u32[]{:S(2)}) %all-to-all-start.1) | async-done | bytes 294944 | tf_op jit(solution)/shard_map/all_to_all | solution.py:430
  178.0 1.4 combine.1
  (19 shorter events, 0.1 us)
Async XLA Ops:
  0.0 18.2 %copy-start = (bf16[4,256,256]{2,1,0:T(8,128)(2,1)S(1)}, bf16[4,256,256]{2,1,0:T(8,128)(2,1)}, u32[]{:S(2)}) copy-start(bf16[4,256,256]{2,1,0:T(8,128)(2,1)} %param.15) | copy-start | bytes 1572868
  0.0 55.1 %copy-start.1 = (bf16[1,2048,256]{2,1,0:T(8,128)(2,1)S(1)}, bf16[1,2048,256]{2,1,0:T(8,128)(2,1)}, u32[]{:S(2)}) copy-start(bf16[1,2048,256]{2,1,0:T(8,128)(2,1)} %param.23) | copy-start | bytes 3145732
  0.0 57.4 %copy-start.2 = (bf16[1,2048,256]{2,1,0:T(8,128)(2,1)S(1)}, bf16[1,2048,256]{2,1,0:T(8,128)(2,1)}, u32[]{:S(2)}) copy-start(bf16[1,2048,256]{2,1,0:T(8,128)(2,1)} %param.24) | copy-start | bytes 3145732
  0.9 6.3 %collective-permute-start = (bf16[64,128]{1,0:T(8,128)(2,1)S(1)}, bf16[64,128]{1,0:T(8,128)(2,1)S(1)}, u32[]{:S(2)}, u32[]{:S(2)}) collective-permute-start(bf16[64,128]{1,0:T(8,128)(2,1)S(1)} %slice.6), channel_id=1, source_target_pairs={{0,16},{16,32},{32,48},{48,64},{64,80},{80,96},{96,112},{112,128},... | collective-permute-start | bytes 49160 | tf_op jit(solution)/shard_map/ppermute | solution.py:397
  5.6 0.7 copy-start.5
  7.2 0.8 copy-start.4
  37.4 3.2 %collective-permute-start.1 = (bf16[384,128]{1,0:T(8,128)(2,1)S(1)}, bf16[384,128]{1,0:T(8,128)(2,1)S(1)}, u32[]{:S(2)}, u32[]{:S(2)}) collective-permute-start(bf16[384,128]{1,0:T(8,128)(2,1)S(1)} %fusion.4.refs_0_.state_ref), channel_id=1, source_target_pairs={{0,1},{1,0},{2,3},{3,2},{4,5},{5,4},{6,7},{7,6},{8,9},{9,8},{10,11... | collective-permute-start | bytes 294920 | tf_op jit(solution)/shard_map/ppermute | solution.py:362
  41.8 27.7 %all-to-all-start = ((bf16[32,18,256]{2,1,0:T(8,128)(2,1)}), bf16[32,18,256]{2,1,0:T(8,128)(2,1)S(1)}, u32[]{:S(2)}, u32[]{:S(2)}) async-start(bf16[32,18,256]{2,1,0:T(8,128)(2,1)} %dispatch.1), calls=%async_computation | async-start | bytes 786432 | tf_op jit(solution)/shard_map/all_to_all | solution.py:421
  55.1 41.3 %collective-permute-start.2 = (bf16[2048,256]{1,0:T(8,128)(2,1)S(1)}, bf16[2048,256]{1,0:T(8,128)(2,1)}, u32[]{:S(2)}, u32[]{:S(2)}) collective-permute-start(bf16[2048,256]{1,0:T(8,128)(2,1)S(1)} %bitcast.14), channel_id=1, source_target_pairs={{0,1},{1,0},{2,3},{3,2},{4,5},{5,4},{6,7},{7,6},{8,9},{9,8},{10,11... | collective-permute-start | bytes 3145736 | tf_op jit(solution)/shard_map/ppermute | solution.py:362
  57.5 39.0 %collective-permute-start.3 = (bf16[2048,256]{1,0:T(8,128)(2,1)S(1)}, bf16[2048,256]{1,0:T(8,128)(2,1)}, u32[]{:S(2)}, u32[]{:S(2)}) collective-permute-start(bf16[2048,256]{1,0:T(8,128)(2,1)S(1)} %bitcast.16), channel_id=1, source_target_pairs={{0,1},{1,0},{2,3},{3,2},{4,5},{5,4},{6,7},{7,6},{8,9},{9,8},{10,11... | collective-permute-start | bytes 3145736 | tf_op jit(solution)/shard_map/ppermute | solution.py:362
  59.4 84.9 %collective-permute-start.4 = (bf16[4096,128]{1,0:T(8,128)(2,1)}, bf16[4096,128]{1,0:T(8,128)(2,1)}, u32[]{:S(2)}, u32[]{:S(2)}) collective-permute-start(bf16[4096,128]{1,0:T(8,128)(2,1)} %bitcast.18), channel_id=1, source_target_pairs={{0,1},{1,0},{2,3},{3,2},{4,5},{5,4},{6,7},{7,6},{8,9},{9,8},{10,11... | collective-permute-start | bytes 3145736 | tf_op jit(solution)/shard_map/ppermute | solution.py:362
  142.9 1.4 copy-start.3
  144.3 16.4 %copy-start.7 = (f32[384,4]{0,1:T(4,128)S(1)}, f32[384,4]{0,1:T(4,128)}, u32[]{:S(2)}) copy-start(f32[384,4]{0,1:T(4,128)} %param.21) | copy-start | bytes 18436
  144.3 16.4 %copy-start.6 = (s32[384,2]{0,1:T(2,128)S(1)}, s32[384,2]{0,1:T(2,128)}, u32[]{:S(2)}) copy-start(s32[384,2]{0,1:T(2,128)} %param.20) | copy-start | bytes 9220
  144.3 20.9 %copy-start.8 = (f32[384,2]{0,1:T(2,128)S(1)}, f32[384,2]{0,1:T(2,128)}, u32[]{:S(2)}) copy-start(f32[384,2]{0,1:T(2,128)} %param.22) | copy-start | bytes 9220
  148.0 11.8 %collective-permute-start.5 = (bf16[576,128]{1,0:T(8,128)(2,1)S(1)}, bf16[576,128]{1,0:T(8,128)(2,1)S(1)}, u32[]{:S(2)}, u32[]{:S(2)}) collective-permute-start(bf16[576,128]{1,0:T(8,128)(2,1)S(1)} %get-tuple-element.16), channel_id=1, source_target_pairs={{0,1},{1,0},{2,3},{3,2},{4,5},{5,4},{6,7},{7,6},{8,9},{9,8},{10,11... | collective-permute-start | bytes 442376 | tf_op jit(solution)/shard_map/ppermute | solution.py:362
  160.8 17.2 %all-to-all-start.1 = ((bf16[32,36,128]{2,1,0:T(8,128)(2,1)}), bf16[32,36,128]{2,1,0:T(8,128)(2,1)S(1)}, u32[]{:S(2)}, u32[]{:S(2)}) async-start(bf16[32,36,128]{2,1,0:T(8,128)(2,1)} %unfold.1), calls=%async_computation.1 | async-start | bytes 655360 | tf_op jit(solution)/shard_map/all_to_all | solution.py:430

commit v8 on v7

--- a/solution.py
+++ b/solution.py
@@ -399,7 +399,10 @@
     )
     slots = slot_table(routes.T, experts, padded(capacity))
     gains = gain_rows(norm_gain)
-    pooled = pool(edge, pool_input, gains)
+    own, opened = lax.optimization_barrier(
+        (pool_input.astype(jnp.float32), jax.nn.sigmoid(pool_gate.astype(jnp.float32)))
+    )
+    pooled = pool(edge, own, gains)
     group = lax.all_gather(pooled, SCALE, axis=0, tiled=True)
     mix = lax.dynamic_slice(
         pool_mix, (scale, 0, quarter * channels), (1, pool_mix.shape[1], channels)
@@ -407,7 +410,7 @@
     mixed = lax.dot_general(mix, group[:, :length], (((0,), (0,)), ((), ())), preferred_element_type=jnp.float32)
     other_gains = lax.dynamic_slice(group, ((quarter + 1 - 2 * core) * channels, length), (GAIN_ROWS, SPAN))
     own_scale = lax.dynamic_slice(pool_scale, (own_first,), (channels,))
-    branch = (jax.nn.sigmoid(pool_gate.astype(jnp.float32)) * mixed * own_scale[:, None]).astype(jnp.bfloat16)
+    branch = (opened * mixed * own_scale[:, None]).astype(jnp.bfloat16)
     branches = lax.all_gather(branch, TP, axis=0, tiled=True)
     product = lax.dot_general(
         branches, out_proj, (((0,), (0,)), ((), ())), preferred_element_type=jnp.float32

time: 180 us -> 179 us (level)
  transfers between devices with their start and end apart: 8 -> 8, of which waited for: 4 -> 4; matrix products, arithmetic and copies ran while one was open for 3% -> 4% of each run, Pallas kernels for 2% -> 2%
where the time goes in v8:
time: 179 us; the launch traced here: 178 us
  blocking collectives  94.3 us (53%)
  starting transfers between devices  40.3 us (23%)
  waiting for transfers between devices  22 us (12%)
  Pallas kernels  11.8 us (7%)
  other arithmetic  5.46 us (3%)
  local copies, waits for them, and re-layouts  2.63 us (1%)
    all_gather x2, blocking collectives, to_line(): lax.all_gather(to_travel(values), LINE, axis=0, tiled=False)  67.7 us
    ppermute x5, starting transfers between devices, swap(): return lax.ppermute(values, 'core', [(0, 1), (1, 0)])  19.6 us
    all_gather x1, blocking collectives, per_device(): branches = lax.all_gather(branch, TP, axis=0, tiled=True)  16.8 us
    all_to_all x1, waiting for transfers between devices, per_device(): lax.all_to_all(result, 'sp', split_axis=0, concat_axis=0, tiled=True)  12.4 us
    all_to_all x1, starting transfers between devices, per_device(): lax.all_to_all(sent, 'sp', split_axis=0, concat_axis=0, tiled=True)  12.3 us
    all_gather x1, blocking collectives, per_device(): group = lax.all_gather(pooled, SCALE, axis=0, tiled=True)  9.8 us
    all_to_all x1, waiting for transfers between devices, per_device(): lax.all_to_all(sent, 'sp', split_axis=0, concat_axis=0, tiled=True)  7.64 us
    all_to_all x1, starting transfers between devices, per_device(): lax.all_to_all(result, 'sp', split_axis=0, concat_axis=0, tiled=True)  4.41 us
  transfers between devices with their start and end apart: 8, of which 4 were waited for; matrix products, arithmetic and copies ran while one was open for 4% of the time, Pallas kernels for 2%

profile of v8, /device:TPU:1, one launch (start us, length us, event | category | flops | bytes accessed | tf_op | source)
XLA Modules:
  0.0 178.4 jit_solution(5372512617588588324)
XLA Ops:
  0.0 0.0 copy-start
  0.0 0.9 slice.6
  0.9 3.9 %collective-permute-start = (bf16[64,128]{1,0:T(8,128)(2,1)S(1)}, bf16[64,128]{1,0:T(8,128)(2,1)S(1)}, u32[]{:S(2)}, u32[]{:S(2)}) collective-permute-start(bf16[64,128]{1,0:T(8,128)(2,1)S(1)} %slice.6), channel_id=1, source_target_pairs={{0,16},{16,32},{32,48},{48,64},{64,80},{80,96},{96,112},{112,128},... | collective-permute-start | bytes 49160 | tf_op jit(solution)/shard_map/ppermute | solution.py:397
  4.8 0.7 subtract_reduce-precision_fusion
  5.5 0.8 add_divide_fusion
  6.3 0.1 select_convert_fusion.gain_ref.own_ref
  6.4 0.8 convert_element_type.43.own_ref
  7.2 0.7 copy-done.4
  7.9 0.2 slots.1.refs_2_
  8.1 0.8 dynamic_slice.10
  8.9 0.0 collective-permute-done.edge_ref
  8.9 0.4 pool.1
  9.2 9.8 %all_gather.18 = bf16[256,512]{1,0:T(8,128)(2,1)S(1)} all-gather(bf16[64,512]{1,0:T(8,128)(2,1)S(1)} %pool.1), channel_id=1, replica_groups=mesh['sp'=32,'tg'=4,'yl'=2,'core'=2] {'yl','core'}, dimensions={0}, use_global_device_ids=true | all-gather | bytes 327680 | tf_op jit(solution)/shard_map/all_gather | solution.py:406
  19.0 0.3 fusion.6
  19.3 16.8 %all_gather.19 = bf16[1024,384]{1,0:T(8,128)(2,1)S(1)} all-gather(bf16[64,384]{1,0:T(8,128)(2,1)S(1)} %fusion.6), channel_id=1, replica_groups=mesh['sp'=32,'tg'=4,'yl'=2,'core'=2] {'tg','yl','core'}, dimensions={0}, use_global_device_ids=true | all-gather | bytes 835584 | tf_op jit(solution)/shard_map/all_gather | solution.py:414
  36.1 1.4 fusion.4.refs_0_.state_ref
  37.5 2.1 %collective-permute-start.1 = (bf16[384,128]{1,0:T(8,128)(2,1)S(1)}, bf16[384,128]{1,0:T(8,128)(2,1)S(1)}, u32[]{:S(2)}, u32[]{:S(2)}) collective-permute-start(bf16[384,128]{1,0:T(8,128)(2,1)S(1)} %fusion.4.refs_0_.state_ref), channel_id=1, source_target_pairs={{0,1},{1,0},{2,3},{3,2},{4,5},{5,4},{6,7},{7,6},{8,9},{9,8},{10,11... | collective-permute-start | bytes 294920 | tf_op jit(solution)/shard_map/ppermute | solution.py:362
  39.6 1.1 collective-permute-done.1.refs_1_
  40.7 1.2 dispatch.1
  41.8 12.3 %all-to-all-start = ((bf16[32,18,256]{2,1,0:T(8,128)(2,1)}), bf16[32,18,256]{2,1,0:T(8,128)(2,1)S(1)}, u32[]{:S(2)}, u32[]{:S(2)}) async-start(bf16[32,18,256]{2,1,0:T(8,128)(2,1)} %dispatch.1), calls=%async_computation | async-start | bytes 786432 | tf_op jit(solution)/shard_map/all_to_all | solution.py:424
  54.2 2.3 %collective-permute-start.2 = (bf16[2048,256]{1,0:T(8,128)(2,1)S(1)}, bf16[2048,256]{1,0:T(8,128)(2,1)}, u32[]{:S(2)}, u32[]{:S(2)}) collective-permute-start(bf16[2048,256]{1,0:T(8,128)(2,1)S(1)} %bitcast.14), channel_id=1, source_target_pairs={{0,1},{1,0},{2,3},{3,2},{4,5},{5,4},{6,7},{7,6},{8,9},{9,8},{10,11... | collective-permute-start | bytes 3145736 | tf_op jit(solution)/shard_map/ppermute | solution.py:362
  56.5 2.0 %collective-permute-start.3 = (bf16[2048,256]{1,0:T(8,128)(2,1)S(1)}, bf16[2048,256]{1,0:T(8,128)(2,1)}, u32[]{:S(2)}, u32[]{:S(2)}) collective-permute-start(bf16[2048,256]{1,0:T(8,128)(2,1)S(1)} %bitcast.16), channel_id=1, source_target_pairs={{0,1},{1,0},{2,3},{3,2},{4,5},{5,4},{6,7},{7,6},{8,9},{9,8},{10,11... | collective-permute-start | bytes 3145736 | tf_op jit(solution)/shard_map/ppermute | solution.py:362
  58.5 2.4 %collective-permute-start.4 = (bf16[4096,128]{1,0:T(8,128)(2,1)}, bf16[4096,128]{1,0:T(8,128)(2,1)}, u32[]{:S(2)}, u32[]{:S(2)}) collective-permute-start(bf16[4096,128]{1,0:T(8,128)(2,1)} %bitcast.18), channel_id=1, source_target_pairs={{0,1},{1,0},{2,3},{3,2},{4,5},{5,4},{6,7},{7,6},{8,9},{9,8},{10,11... | collective-permute-start | bytes 3145736 | tf_op jit(solution)/shard_map/ppermute | solution.py:362
  60.9 7.6 %all-to-all-done.arrived_ref = bf16[32,18,256]{2,1,0:T(8,128)(2,1)S(1)} async-done(((bf16[32,18,256]{2,1,0:T(8,128)(2,1)}), bf16[32,18,256]{2,1,0:T(8,128)(2,1)S(1)}, u32[]{:S(2)}, u32[]{:S(2)}) %all-to-all-start) | async-done | bytes 294944 | tf_op jit(solution)/shard_map/all_to_all | solution.py:424
  68.5 0.1 compact.1
  68.6 0.3 fusion.8
  68.9 25.9 %all-gather.4 = f16[4736,256]{1,0:T(8,128)(2,1)S(1)} all-gather(f16[592,256]{1,0:T(8,128)(2,1)S(1)} %fusion.8), channel_id=2, replica_groups=mesh['sp'=32,'tg'=4,'yl'=2,'core'=2] {'tg','yl'}, dimensions={0}, use_global_device_ids=true | all-gather | bytes 2727936 | tf_op jit(solution)/shard_map/all_gather | solution.py:358
  94.8 0.7 fusion.1.x_ref
  95.5 0.0 collective-permute-done.2.gate2_hbm
  95.5 0.0 collective-permute-done.3.up2_hbm
  95.5 4.1 %hidden.1 = bf16[576,512]{1,0:T(8,128)(2,1)S(1)} custom-call(bf16[8,592,256]{2,1,0:T(8,128)(2,1)S(1)} %fusion.1.x_ref, bf16[2048,256]{1,0:T(8,128)(2,1)S(1)} %bitcast.15, bf16[2048,256]{1,0:T(8,128)(2,1)S(1)} %bitcast.17, bf16[2048,256]{1,0:T(8,128)(2,1)} %collective-permute-done.2.gate2_hbm, bf16[2048,256]{1,0:T(8,128)(2,1)} %collective-permute-done.3.up2_hbm), custom_call_target="tpu_custom_call" | custom-call | tf_op jit(solution)/shard_map/hidden/pallas_call | solution.py:218
  99.7 0.5 fusion.3
  100.2 41.8 %all-gather.5 = f16[4608,512]{1,0:T(8,128)(2,1)S(1)} all-gather(f16[576,512]{1,0:T(8,128)(2,1)S(1)} %fusion.3), channel_id=3, replica_groups=mesh['sp'=32,'tg'=4,'yl'=2,'core'=2] {'tg','yl'}, dimensions={0}, use_global_device_ids=true | all-gather | bytes 5308416 | tf_op jit(solution)/shard_map/all_gather | solution.py:358
  142.0 1.3 fusion.u_ref
  143.4 0.0 copy-start.6
  143.4 0.0 copy-start.5
  143.4 0.0 copy-start.7
  143.4 0.0 collective-permute-done.4.other_hbm
  143.4 3.7 %down.1 = (bf16[576,128]{1,0:T(8,128)(2,1)S(1)}, bf16[576,128]{1,0:T(8,128)(2,1)S(1)}) custom-call(bf16[8,576,512]{2,1,0:T(8,128)(2,1)S(1)} %fusion.u_ref, bf16[4096,128]{1,0:T(8,128)(2,1)S(1)} %bitcast.19, bf16[4096,128]{1,0:T(8,128)(2,1)} %collective-permute-done.4.other_hbm), custom_call_target="tpu_custom_call" | custom-call | tf_op jit(solution)/shard_map/down/pallas_call | solution.py:267
  147.1 10.9 %collective-permute-start.5 = (bf16[576,128]{1,0:T(8,128)(2,1)S(1)}, bf16[576,128]{1,0:T(8,128)(2,1)S(1)}, u32[]{:S(2)}, u32[]{:S(2)}) collective-permute-start(bf16[576,128]{1,0:T(8,128)(2,1)S(1)} %get-tuple-element.20), channel_id=1, source_target_pairs={{0,1},{1,0},{2,3},{3,2},{4,5},{5,4},{6,7},{7,6},{8,9},{9,8},{10,11... | collective-permute-start | bytes 442376 | tf_op jit(solution)/shard_map/ppermute | solution.py:362
  158.0 0.1 copy.24
  158.1 0.8 collective-permute-done.5.other_ref
  158.9 0.8 unfold.1
  159.8 4.4 %all-to-all-start.1 = ((bf16[32,36,128]{2,1,0:T(8,128)(2,1)}), bf16[32,36,128]{2,1,0:T(8,128)(2,1)S(1)}, u32[]{:S(2)}, u32[]{:S(2)}) async-start(bf16[32,36,128]{2,1,0:T(8,128)(2,1)} %unfold.1), calls=%async_computation.1 | async-start | bytes 655360 | tf_op jit(solution)/shard_map/all_to_all | solution.py:433
  164.3 0.1 copy.25
  164.5 0.1 broadcast_divide_fusion.weight_ref
  164.6 12.4 %all-to-all-done.1.returned_ref = bf16[32,36,128]{2,1,0:T(8,128)(2,1)S(1)} async-done(((bf16[32,36,128]{2,1,0:T(8,128)(2,1)}), bf16[32,36,128]{2,1,0:T(8,128)(2,1)S(1)}, u32[]{:S(2)}, u32[]{:S(2)}) %all-to-all-start.1) | async-done | bytes 294944 | tf_op jit(solution)/shard_map/all_to_all | solution.py:433
  177.0 1.4 combine.1
  (19 shorter events, 0.1 us)
Async XLA Ops:
  0.0 19.0 %copy-start = (bf16[4,256,256]{2,1,0:T(8,128)(2,1)S(1)}, bf16[4,256,256]{2,1,0:T(8,128)(2,1)}, u32[]{:S(2)}) copy-start(bf16[4,256,256]{2,1,0:T(8,128)(2,1)} %param.15) | copy-start | bytes 1572868
  0.0 54.2 %copy-start.1 = (bf16[1,2048,256]{2,1,0:T(8,128)(2,1)S(1)}, bf16[1,2048,256]{2,1,0:T(8,128)(2,1)}, u32[]{:S(2)}) copy-start(bf16[1,2048,256]{2,1,0:T(8,128)(2,1)} %param.23) | copy-start | bytes 3145732
  0.0 56.5 %copy-start.2 = (bf16[1,2048,256]{2,1,0:T(8,128)(2,1)S(1)}, bf16[1,2048,256]{2,1,0:T(8,128)(2,1)}, u32[]{:S(2)}) copy-start(bf16[1,2048,256]{2,1,0:T(8,128)(2,1)} %param.24) | copy-start | bytes 3145732
  0.9 8.0 %collective-permute-start = (bf16[64,128]{1,0:T(8,128)(2,1)S(1)}, bf16[64,128]{1,0:T(8,128)(2,1)S(1)}, u32[]{:S(2)}, u32[]{:S(2)}) collective-permute-start(bf16[64,128]{1,0:T(8,128)(2,1)S(1)} %slice.6), channel_id=1, source_target_pairs={{0,16},{16,32},{32,48},{48,64},{64,80},{80,96},{96,112},{112,128},... | collective-permute-start | bytes 49160 | tf_op jit(solution)/shard_map/ppermute | solution.py:397
  7.2 0.7 copy-start.4
  37.5 3.2 %collective-permute-start.1 = (bf16[384,128]{1,0:T(8,128)(2,1)S(1)}, bf16[384,128]{1,0:T(8,128)(2,1)S(1)}, u32[]{:S(2)}, u32[]{:S(2)}) collective-permute-start(bf16[384,128]{1,0:T(8,128)(2,1)S(1)} %fusion.4.refs_0_.state_ref), channel_id=1, source_target_pairs={{0,1},{1,0},{2,3},{3,2},{4,5},{5,4},{6,7},{7,6},{8,9},{9,8},{10,11... | collective-permute-start | bytes 294920 | tf_op jit(solution)/shard_map/ppermute | solution.py:362
  41.8 26.7 %all-to-all-start = ((bf16[32,18,256]{2,1,0:T(8,128)(2,1)}), bf16[32,18,256]{2,1,0:T(8,128)(2,1)S(1)}, u32[]{:S(2)}, u32[]{:S(2)}) async-start(bf16[32,18,256]{2,1,0:T(8,128)(2,1)} %dispatch.1), calls=%async_computation | async-start | bytes 786432 | tf_op jit(solution)/shard_map/all_to_all | solution.py:424
  54.2 41.3 %collective-permute-start.2 = (bf16[2048,256]{1,0:T(8,128)(2,1)S(1)}, bf16[2048,256]{1,0:T(8,128)(2,1)}, u32[]{:S(2)}, u32[]{:S(2)}) collective-permute-start(bf16[2048,256]{1,0:T(8,128)(2,1)S(1)} %bitcast.14), channel_id=1, source_target_pairs={{0,1},{1,0},{2,3},{3,2},{4,5},{5,4},{6,7},{7,6},{8,9},{9,8},{10,11... | collective-permute-start | bytes 3145736 | tf_op jit(solution)/shard_map/ppermute | solution.py:362
  56.5 39.0 %collective-permute-start.3 = (bf16[2048,256]{1,0:T(8,128)(2,1)S(1)}, bf16[2048,256]{1,0:T(8,128)(2,1)}, u32[]{:S(2)}, u32[]{:S(2)}) collective-permute-start(bf16[2048,256]{1,0:T(8,128)(2,1)S(1)} %bitcast.16), channel_id=1, source_target_pairs={{0,1},{1,0},{2,3},{3,2},{4,5},{5,4},{6,7},{7,6},{8,9},{9,8},{10,11... | collective-permute-start | bytes 3145736 | tf_op jit(solution)/shard_map/ppermute | solution.py:362
  58.5 84.9 %collective-permute-start.4 = (bf16[4096,128]{1,0:T(8,128)(2,1)}, bf16[4096,128]{1,0:T(8,128)(2,1)}, u32[]{:S(2)}, u32[]{:S(2)}) collective-permute-start(bf16[4096,128]{1,0:T(8,128)(2,1)} %bitcast.18), channel_id=1, source_target_pairs={{0,1},{1,0},{2,3},{3,2},{4,5},{5,4},{6,7},{7,6},{8,9},{9,8},{10,11... | collective-permute-start | bytes 3145736 | tf_op jit(solution)/shard_map/ppermute | solution.py:362
  142.0 1.4 copy-start.3
  143.4 16.4 %copy-start.6 = (f32[384,4]{0,1:T(4,128)S(1)}, f32[384,4]{0,1:T(4,128)}, u32[]{:S(2)}) copy-start(f32[384,4]{0,1:T(4,128)} %param.21) | copy-start | bytes 18436
  143.4 16.4 %copy-start.5 = (s32[384,2]{0,1:T(2,128)S(1)}, s32[384,2]{0,1:T(2,128)}, u32[]{:S(2)}) copy-start(s32[384,2]{0,1:T(2,128)} %param.20) | copy-start | bytes 9220
  143.4 20.9 %copy-start.7 = (f32[384,2]{0,1:T(2,128)S(1)}, f32[384,2]{0,1:T(2,128)}, u32[]{:S(2)}) copy-start(f32[384,2]{0,1:T(2,128)} %param.22) | copy-start | bytes 9220
  147.1 11.8 %collective-permute-start.5 = (bf16[576,128]{1,0:T(8,128)(2,1)S(1)}, bf16[576,128]{1,0:T(8,128)(2,1)S(1)}, u32[]{:S(2)}, u32[]{:S(2)}) collective-permute-start(bf16[576,128]{1,0:T(8,128)(2,1)S(1)} %get-tuple-element.20), channel_id=1, source_target_pairs={{0,1},{1,0},{2,3},{3,2},{4,5},{5,4},{6,7},{7,6},{8,9},{9,8},{10,11... | collective-permute-start | bytes 442376 | tf_op jit(solution)/shard_map/ppermute | solution.py:362
  159.8 17.2 %all-to-all-start.1 = ((bf16[32,36,128]{2,1,0:T(8,128)(2,1)}), bf16[32,36,128]{2,1,0:T(8,128)(2,1)S(1)}, u32[]{:S(2)}, u32[]{:S(2)}) async-start(bf16[32,36,128]{2,1,0:T(8,128)(2,1)} %unfold.1), calls=%async_computation.1 | async-start | bytes 655360 | tf_op jit(solution)/shard_map/all_to_all | solution.py:433
